TPU v7x, 512 devices: a whole 4x8x8 slice. The times are simulated.
512 devices in a mesh: rep: 2 (over z_hi), fs: 32 (over z_lo, y), tp: 8 (over x, core).
Axes of the slice: x: 4, y: 8, z: 8 (z_hi: 2, z_lo: 4; z = z_hi * 4 + z_lo), core: 2. Of those that a mesh axis runs over, the one named last changes fastest.
Arguments:
- tokens: bfloat16 [65536, 1536], P(('rep', 'fs', 'tp')), may hold values from -6 to 6
- norm_gain: float32 [1536], replicated, may hold values from 0.1 to 1.9
- up_weight: float32 [1536, 6144], P('fs', 'tp'), may hold values from -0.15625 to 0.15625
- up_scale: float32 [1, 6144], P(None, 'tp'), may hold values from 0.5 to 2
- down_weight: float32 [6144, 1536], P('tp', 'fs'), may hold values from -0.078125 to 0.078125
- down_scale: float32 [1, 1536], P(None, 'fs'), may hold values from 0.5 to 2
Outputs:
- mixed: bfloat16 [65536, 1536], P(('rep', 'fs', 'tp'))
All inputs are finite; a program needn't handle non-finite values.
Results may differ from a plain program's by a relative error of at most 0.015.
Values may be sent and summed in bfloat16 or wider, within the bound.
No kernel may reach another device: no remote copies, remote signals or barrier semaphores. Data moves between devices by JAX's collectives and lax.ppermute only.
A program may use at most 64 MiB of HBM per device.

v0:
```python
import jax
import jax.numpy as jnp
from jax import lax
from jax.sharding import PartitionSpec as P


Z, ZLO, Y, X = 8, 4, 8, 4
ROW_GROUPS = [[z * Y + y for y in range(Y)] for z in range(ZLO)]
X_GROUPS = [[2 * x + c for x in range(X)] for c in range(2)]
OTHER_CORE = [(i, i ^ 1) for i in range(2 * X)]
PLANE = ("rep", "fs")
F32, BF16 = jnp.float32, jnp.bfloat16


def z_shift(by):
    return [(z * Y + y, (z + by(z)) % Z * Y + y) for z in range(Z) for y in range(Y)]


def x_shift(by):
    return [(2 * x + c, (x + by(x)) % X * 2 + c) for x in range(X) for c in range(2)]


FROM_NEXT = z_shift(lambda z: -1)
FROM_LAST = z_shift(lambda z: 1)
FROM_TWO = z_shift(lambda z: 2 if z % 2 == 0 else -2)
X_NEXT = x_shift(lambda x: -1)
X_LAST = x_shift(lambda x: 1)
X_TWO = x_shift(lambda x: 2)


def swapped(blocks, axis, groups):
    return lax.all_to_all(blocks, axis, 0, 0, axis_index_groups=groups, tiled=True)


def spread(shard, axis, groups):
    return swapped(jnp.broadcast_to(shard[None], (len(groups[0]), *shard.shape)), axis, groups)


def rolled(a, by, width):
    n = a.shape[1] // width
    out = a
    for k in range(1, n):
        out = jnp.where(by == k, jnp.concatenate([a[:, width * k :], a[:, : width * k]], 1), out)
    return out


def body(tokens, norm_gain, up_weight, up_scale, down_weight, down_scale):
    z = lax.axis_index("fs") // Y
    x = lax.axis_index("tp") // 2
    rows, d = tokens.shape
    width = d // ZLO
    hidden_width = up_weight.shape[1]

    up_own = spread(up_weight.astype(BF16), "fs", ROW_GROUPS).reshape(width, hidden_width)
    down_piece = (down_weight * down_scale).T.astype(BF16)
    down_two = lax.ppermute(down_piece, PLANE, FROM_TWO)

    values = tokens.astype(F32)
    normed = (
        values * lax.rsqrt(jnp.mean(values * values, axis=-1, keepdims=True) + 1e-06) * norm_gain
    ).astype(BF16)
    normed = rolled(normed, z, width)
    near = [
        normed,
        lax.ppermute(normed, "tp", X_NEXT),
        lax.ppermute(normed, "tp", X_TWO),
        lax.ppermute(normed, "tp", X_LAST),
    ]
    own = jnp.zeros((X * rows, d), BF16)
    for k, block in enumerate(near):
        own = lax.dynamic_update_slice(own, block, (rows * ((x + k) % X), 0))
    other = lax.ppermute(own, "tp", OTHER_CORE)

    up_next = lax.ppermute(up_own, PLANE, FROM_NEXT)
    up_last = lax.ppermute(up_own, PLANE, FROM_LAST)
    half = width // 2
    up_two = jnp.concatenate(
        [lax.ppermute(up_next[:half], PLANE, FROM_NEXT), lax.ppermute(up_last[half:], PLANE, FROM_LAST)],
        0,
    )

    pieces, up_own = lax.optimization_barrier((jnp.stack([down_piece, down_two]), up_own))
    copies = jnp.broadcast_to(pieces[None], (Y, *pieces.shape))
    down_a = swapped(copies, "fs", ROW_GROUPS)
    first = lax.ppermute(down_a[: Y // 2], PLANE, FROM_NEXT)
    second = lax.ppermute(down_a[Y // 2 :], PLANE, FROM_LAST)
    down_b = jnp.stack(
        [jnp.concatenate([first[:, 0], second[:, 1]], 0), jnp.concatenate([first[:, 1], second[:, 0]], 0)]
    )
    down_b = down_b.reshape(2 * width, hidden_width)
    down_a = down_a.transpose(1, 0, 2, 3).reshape(2 * width, hidden_width)

    def hidden_of(t):
        pre = 0.0
        for k, block in enumerate([up_own, up_next, up_last, up_two]):
            place = (0, 1, 3, 2)[k]
            pre += jnp.dot(t[:, place * width : (place + 1) * width], block, preferred_element_type=F32)
        return jnp.square(jnp.maximum(pre * up_scale, 0.0)).astype(BF16)

    hidden_own, hidden_other = hidden_of(own), hidden_of(other)

    def chunk(down):
        def terms(hidden):
            return lax.dot_general(hidden, down, (((1,), (1,)), ((), ())), preferred_element_type=F32)

        arrived = lax.ppermute(terms(hidden_other).astype(BF16), "tp", OTHER_CORE)
        pair = (terms(hidden_own) + arrived.astype(F32)).astype(BF16)
        arrived = swapped(pair.reshape(X, rows, -1), "tp", X_GROUPS)
        return arrived.astype(F32).sum(axis=0).astype(BF16)

    out_a = chunk(down_a)
    out_b = chunk(down_b)
    summed = jnp.concatenate(
        [out_a[:, :width], out_b[:, :width], out_a[:, width:], out_b[:, width:]], 1
    )
    return rolled(summed, (ZLO - z) % ZLO, width)


def solution(mesh):
    return jax.shard_map(
        body,
        mesh=mesh,
        in_specs=(
            P(("rep", "fs", "tp"), None),
            P(),
            P("fs", "tp"),
            P(None, "tp"),
            P("tp", "fs"),
            P(None, "fs"),
        ),
        out_specs=P(("rep", "fs", "tp"), None),
        check_vma=False,
    )
```

profile of v0, /device:TPU:1, one launch (start us, length us, event | category | flops | bytes accessed | tf_op | source)
XLA Modules:
  0.0 171.1 jit_solution(4835719499602726995)
XLA Ops:
  4.5 5.2 %collective-permute-start = (bf16[128,1536]{1,0:T(8,128)(2,1)}, bf16[128,1536]{1,0:T(8,128)(2,1)S(1)}, u32[]{:S(2)}, u32[]{:S(2)}) collective-permute-start(bf16[128,1536]{1,0:T(8,128)(2,1)} %get-tuple-element.10), channel_id=1, source_target_pairs={{0,6},{1,7},{2,0},{3,1},{4,2},{5,3},{6,4},{7,5},{8,14},{9,15},{10,... | collective-permute-start | bytes 1179656 | tf_op jit(solution)/shard_map/ppermute | solution.py:65
  10.6 7.0 %all-to-all-start = ((bf16[8,48,768]{2,1,0:T(8,128)(2,1)}), bf16[8,48,768]{2,1,0:T(8,128)(2,1)S(1)}, u32[]{:S(2)}, u32[]{:S(2)}) async-start(bf16[8,48,768]{2,1,0:T(8,128)(2,1)} %broadcast_in_dim.7), calls=%async_computation | async-start | bytes 1179648 | tf_op jit(solution)/shard_map/all_to_all | solution.py:32
  17.5 2.4 %collective-permute-start.1 = (bf16[128,1536]{1,0:T(8,128)(2,1)}, bf16[128,1536]{1,0:T(8,128)(2,1)S(1)}, u32[]{:S(2)}, u32[]{:S(2)}) collective-permute-start(bf16[128,1536]{1,0:T(8,128)(2,1)} %get-tuple-element.10), channel_id=1, source_target_pairs={{0,4},{1,5},{2,6},{3,7},{4,0},{5,1},{6,2},{7,3},{8,12},{9,13},{10,... | collective-permute-start | bytes 1179656 | tf_op jit(solution)/shard_map/ppermute | solution.py:66
  19.9 2.5 %collective-permute-start.2 = (bf16[128,1536]{1,0:T(8,128)(2,1)}, bf16[128,1536]{1,0:T(8,128)(2,1)S(1)}, u32[]{:S(2)}, u32[]{:S(2)}) collective-permute-start(bf16[128,1536]{1,0:T(8,128)(2,1)} %get-tuple-element.10), channel_id=1, source_target_pairs={{0,2},{1,3},{2,4},{3,5},{4,6},{5,7},{6,0},{7,1},{8,10},{9,11},{10,... | collective-permute-start | bytes 1179656 | tf_op jit(solution)/shard_map/ppermute | solution.py:67
  22.6 8.0 %collective-permute-done.1 = bf16[128,1536]{1,0:T(8,128)(2,1)S(1)} collective-permute-done((bf16[128,1536]{1,0:T(8,128)(2,1)}, bf16[128,1536]{1,0:T(8,128)(2,1)S(1)}, u32[]{:S(2)}, u32[]{:S(2)}) %collective-permute-start.1) | collective-permute-done | bytes 393248 | tf_op jit(solution)/shard_map/ppermute | solution.py:66
  30.6 10.0 %collective-permute-done.2 = bf16[128,1536]{1,0:T(8,128)(2,1)S(1)} collective-permute-done((bf16[128,1536]{1,0:T(8,128)(2,1)}, bf16[128,1536]{1,0:T(8,128)(2,1)S(1)}, u32[]{:S(2)}, u32[]{:S(2)}) %collective-permute-start.2) | collective-permute-done | bytes 393248 | tf_op jit(solution)/shard_map/ppermute | solution.py:67
  40.6 2.4 %collective-permute-start.10 = (bf16[512,1536]{1,0:T(8,128)(2,1)S(1)}, bf16[512,1536]{1,0:T(8,128)(2,1)}, u32[]{:S(2)}, u32[]{:S(2)}) collective-permute-start(bf16[512,1536]{1,0:T(8,128)(2,1)S(1)} %constant_dynamic-update-slice_fusion.2), channel_id=1, source_target_pairs={{0,1},{1,0},{2,3},{3,2},{4,5},{5,4},{6,7},{7,6},{8,9},{9,8},{10,11... | collective-permute-start | bytes 4718600 | tf_op jit(solution)/shard_map/ppermute | solution.py:72
  43.0 10.7 %collective-permute-start.4 = (bf16[384,768]{1,0:T(8,128)(2,1)S(1)}, bf16[384,768]{1,0:T(8,128)(2,1)}, u32[]{:S(2)}, u32[]{:S(2)}) collective-permute-start(bf16[384,768]{1,0:T(8,128)(2,1)S(1)} %bitcast.44), channel_id=1, source_target_pairs={{0,448},{8,456},{16,464},{24,472},{32,480},{40,488},{48,496},{56,5... | collective-permute-start | bytes 1769480 | tf_op jit(solution)/shard_map/ppermute | solution.py:74
  53.7 1.9 %collective-permute-start.5 = (bf16[384,768]{1,0:T(8,128)(2,1)S(1)}, bf16[384,768]{1,0:T(8,128)(2,1)}, u32[]{:S(2)}, u32[]{:S(2)}) collective-permute-start(bf16[384,768]{1,0:T(8,128)(2,1)S(1)} %bitcast.45), channel_id=1, source_target_pairs={{0,64},{8,72},{16,80},{24,88},{32,96},{40,104},{48,112},{56,120},{... | collective-permute-start | bytes 1769480 | tf_op jit(solution)/shard_map/ppermute | solution.py:75
  55.7 1.9 %collective-permute-start.3 = (bf16[48,768]{1,0:T(8,128)(2,1)S(1)}, bf16[48,768]{1,0:T(8,128)(2,1)S(1)}, u32[]{:S(2)}, u32[]{:S(2)}) collective-permute-start(bf16[48,768]{1,0:T(8,128)(2,1)S(1)} %get-tuple-element.26), channel_id=1, source_target_pairs={{0,128},{8,136},{16,144},{24,152},{32,160},{40,168},{48,176},{56,1... | collective-permute-start | bytes 221192 | tf_op jit(solution)/shard_map/ppermute | solution.py:56
  57.7 14.1 %collective-permute-done.3 = bf16[48,768]{1,0:T(8,128)(2,1)S(1)} collective-permute-done((bf16[48,768]{1,0:T(8,128)(2,1)S(1)}, bf16[48,768]{1,0:T(8,128)(2,1)S(1)}, u32[]{:S(2)}, u32[]{:S(2)}) %collective-permute-start.3) | collective-permute-done | bytes 73760 | tf_op jit(solution)/shard_map/ppermute | solution.py:56
  72.9 6.6 %all-to-all-start.1 = ((bf16[8,2,48,768]{3,2,1,0:T(8,128)(2,1)}), bf16[8,2,48,768]{3,2,1,0:T(8,128)(2,1)S(1)}, u32[]{:S(2)}, u32[]{:S(2)}) async-start(bf16[8,2,48,768]{3,2,1,0:T(8,128)(2,1)} %broadcast_in_dim.8), calls=%async_computation.1 | async-start | bytes 2359296 | tf_op jit(solution)/shard_map/all_to_all | solution.py:32
  82.3 1.9 %collective-permute-start.6 = (bf16[192,768]{1,0:T(8,128)(2,1)S(1)}, bf16[192,768]{1,0:T(8,128)(2,1)S(1)}, u32[]{:S(2)}, u32[]{:S(2)}) collective-permute-start(bf16[192,768]{1,0:T(8,128)(2,1)S(1)} %slice.122), channel_id=1, source_target_pairs={{0,448},{8,456},{16,464},{24,472},{32,480},{40,488},{48,496},{56,5... | collective-permute-start | bytes 884744 | tf_op jit(solution)/shard_map/ppermute | solution.py:78
  85.2 3.4 %collective-permute-start.7 = (bf16[192,768]{1,0:T(8,128)(2,1)S(1)}, bf16[192,768]{1,0:T(8,128)(2,1)S(1)}, u32[]{:S(2)}, u32[]{:S(2)}) collective-permute-start(bf16[192,768]{1,0:T(8,128)(2,1)S(1)} %slice.123), channel_id=1, source_target_pairs={{0,64},{8,72},{16,80},{24,88},{32,96},{40,104},{48,112},{56,120},{... | collective-permute-start | bytes 884744 | tf_op jit(solution)/shard_map/ppermute | solution.py:78
  88.6 2.8 %fusion.17 = f32[512,768]{1,0:T(8,128)} fusion(bf16[384,768]{1,0:T(8,128)(2,1)} %collective-permute-done.5, bf16[512,1536]{1,0:T(8,128)(2,1)S(1)} %constant_dynamic-update-slice_fusion.2), kind=kOutput, calls=%fused_computation.24 | convolution fusion | flops 301989888 | bytes 2555904 | tf_op jit(solution)/shard_map/dot_general | solution.py:97
  91.4 2.8 %fusion.19 = f32[512,768]{1,0:T(8,128)} fusion(bf16[384,768]{1,0:T(8,128)(2,1)} %collective-permute-done.4, bf16[512,1536]{1,0:T(8,128)(2,1)S(1)} %constant_dynamic-update-slice_fusion.2), kind=kOutput, calls=%fused_computation.26 | convolution fusion | flops 301989888 | bytes 2555904 | tf_op jit(solution)/shard_map/dot_general | solution.py:97
  95.4 3.1 %fusion.9 = f32[512,768]{1,0:T(8,128)} fusion(bf16[384,768]{1,0:T(8,128)(2,1)} %collective-permute-done.4, bf16[512,1536]{1,0:T(8,128)(2,1)} %collective-permute-done.10), kind=kOutput, calls=%fused_computation.18 | convolution fusion | flops 301989888 | bytes 2555904 | tf_op jit(solution)/shard_map/dot_general | solution.py:97
  98.5 2.7 %fusion.11 = f32[512,768]{1,0:T(8,128)} fusion(bf16[384,768]{1,0:T(8,128)(2,1)S(1)} %bitcast.47, bf16[512,1536]{1,0:T(8,128)(2,1)} %collective-permute-done.10), kind=kOutput, calls=%fused_computation.20 | convolution fusion | flops 301989888 | bytes 2555904 | tf_op jit(solution)/shard_map/dot_general | solution.py:97
  101.3 3.0 %fusion.7 = f32[512,768]{1,0:T(8,128)} fusion(bf16[384,768]{1,0:T(8,128)(2,1)} %collective-permute-done.5, bf16[512,1536]{1,0:T(8,128)(2,1)} %collective-permute-done.10), kind=kOutput, calls=%fused_computation.16 | convolution fusion | flops 301989888 | bytes 2555904 | tf_op jit(solution)/shard_map/dot_general | solution.py:97
  104.2 7.3 %all-to-all-done.1 = bf16[8,2,48,768]{3,2,1,0:T(8,128)(2,1)S(1)} async-done(((bf16[8,2,48,768]{3,2,1,0:T(8,128)(2,1)}), bf16[8,2,48,768]{3,2,1,0:T(8,128)(2,1)S(1)}, u32[]{:S(2)}, u32[]{:S(2)}) %all-to-all-start.1) | async-done | bytes 1179680 | tf_op jit(solution)/shard_map/all_to_all | solution.py:32
  111.7 2.2 %collective-permute-start.8 = (bf16[4,2,48,768]{3,2,0,1:T(8,128)(2,1)S(1)}, bf16[4,2,48,768]{3,2,0,1:T(8,128)(2,1)S(1)}, u32[]{:S(2)}, u32[]{:S(2)}) collective-permute-start(bf16[4,2,48,768]{3,2,0,1:T(8,128)(2,1)S(1)} %slice.124), channel_id=1, source_target_pairs={{0,448},{8,456},{16,464},{24,472},{32,480},{40,488},{48,496},{56,5... | collective-permute-start | bytes 1769480 | tf_op jit(solution)/shard_map/ppermute | solution.py:85
  114.0 3.4 %collective-permute-start.9 = (bf16[4,2,48,768]{3,2,1,0:T(8,128)(2,1)S(1)}, bf16[4,2,48,768]{3,2,1,0:T(8,128)(2,1)S(1)}, u32[]{:S(2)}, u32[]{:S(2)}) collective-permute-start(bf16[4,2,48,768]{3,2,1,0:T(8,128)(2,1)S(1)} %slice.126), channel_id=1, source_target_pairs={{0,64},{8,72},{16,80},{24,88},{32,96},{40,104},{48,112},{56,120},{... | collective-permute-start | bytes 1769480 | tf_op jit(solution)/shard_map/ppermute | solution.py:86
  117.4 1.8 %multiply_convert_fusion = bf16[512,768]{1,0:T(8,128)(2,1)S(1)} fusion(f32[512,768]{1,0:T(8,128)S(1)} %copy-done.5, f32[512,768]{1,0:T(8,128)S(1)} %copy-done.4, f32[512,768]{1,0:T(8,128)S(1)} %copy-done.3, f32[768]{0:T(1024)S(1)} %reduce.2, bf16[384,768]{1,0:T(8,128)(2,1)} %copy-done.6, bf16[512,1536]{1,0:T(8,128)(2,1)} %collective-permute-done.10), kind=kOutput, calls=%fused_computation.2 | convolution fusion | flops 304742400 | bytes 6491136 | tf_op jit(solution)/shard_map/dot_general | solution.py:97
  120.0 3.0 %collective-permute-start.12 = (bf16[512,768]{1,0:T(8,128)(2,1)S(1)}, bf16[512,768]{1,0:T(8,128)(2,1)S(1)}, u32[]{:S(2)}, u32[]{:S(2)}) collective-permute-start(bf16[512,768]{1,0:T(8,128)(2,1)S(1)} %convolution_convert_fusion), channel_id=1, source_target_pairs={{0,1},{1,0},{2,3},{3,2},{4,5},{5,4},{6,7},{7,6},{8,9},{9,8},{10,11... | collective-permute-start | bytes 2359304 | tf_op jit(solution)/shard_map/ppermute | solution.py:106
  123.0 5.3 %collective-permute-done.8 = bf16[4,2,48,768]{3,2,0,1:T(8,128)(2,1)S(1)} collective-permute-done((bf16[4,2,48,768]{3,2,0,1:T(8,128)(2,1)S(1)}, bf16[4,2,48,768]{3,2,0,1:T(8,128)(2,1)S(1)}, u32[]{:S(2)}, u32[]{:S(2)}) %collective-permute-start.8) | collective-permute-done | bytes 589856 | tf_op jit(solution)/shard_map/ppermute | solution.py:85
  128.3 3.1 %collective-permute-done.9 = bf16[4,2,48,768]{3,2,1,0:T(8,128)(2,1)S(1)} collective-permute-done((bf16[4,2,48,768]{3,2,1,0:T(8,128)(2,1)S(1)}, bf16[4,2,48,768]{3,2,1,0:T(8,128)(2,1)S(1)}, u32[]{:S(2)}, u32[]{:S(2)}) %collective-permute-start.9) | collective-permute-done | bytes 589856 | tf_op jit(solution)/shard_map/ppermute | solution.py:86
  133.5 3.2 %collective-permute-start.11 = (bf16[512,768]{1,0:T(8,128)(2,1)}, bf16[512,768]{1,0:T(8,128)(2,1)}, u32[]{:S(2)}, u32[]{:S(2)}) collective-permute-start(bf16[512,768]{1,0:T(8,128)(2,1)} %convolution_convert_fusion.1), channel_id=1, source_target_pairs={{0,1},{1,0},{2,3},{3,2},{4,5},{5,4},{6,7},{7,6},{8,9},{9,8},{10,11... | collective-permute-start | bytes 2359304 | tf_op jit(solution)/shard_map/ppermute | solution.py:106
  139.2 3.5 %all-to-all-start.3 = ((bf16[4,128,768]{2,1,0:T(8,128)(2,1)}), bf16[4,128,768]{2,1,0:T(8,128)(2,1)S(1)}, u32[]{:S(2)}, u32[]{:S(2)}) async-start(bf16[4,128,768]{2,1,0:T(8,128)(2,1)} %bitcast.16), calls=%async_computation.3 | async-start | bytes 1572864 | tf_op jit(solution)/shard_map/all_to_all | solution.py:32
  142.7 2.9 %add_convert_fusion.1 = bf16[512,768]{1,0:T(8,128)(2,1)} fusion(bf16[512,768]{1,0:T(8,128)(2,1)} %collective-permute-done.11, bf16[512,768]{1,0:T(8,128)(2,1)S(1)} %multiply_convert_fusion.1, bf16[768,768]{1,0:T(8,128)(2,1)S(1)} %bitcast.51), kind=kOutput, calls=%fused_computation.1 | convolution fusion | flops 605159424 | bytes 3538944 | tf_op jit(solution)/shard_map/dot_general | solution.py:104
  145.6 9.5 %all-to-all-done.3 = bf16[4,128,768]{2,1,0:T(8,128)(2,1)S(1)} async-done(((bf16[4,128,768]{2,1,0:T(8,128)(2,1)}), bf16[4,128,768]{2,1,0:T(8,128)(2,1)S(1)}, u32[]{:S(2)}, u32[]{:S(2)}) %all-to-all-start.3) | async-done | bytes 786464 | tf_op jit(solution)/shard_map/all_to_all | solution.py:32
  155.1 3.5 %all-to-all-start.2 = ((bf16[4,128,768]{2,1,0:T(8,128)(2,1)}), bf16[4,128,768]{2,1,0:T(8,128)(2,1)S(1)}, u32[]{:S(2)}, u32[]{:S(2)}) async-start(bf16[4,128,768]{2,1,0:T(8,128)(2,1)} %bitcast.12), calls=%async_computation.2 | async-start | bytes 1572864 | tf_op jit(solution)/shard_map/all_to_all | solution.py:32
  158.7 11.3 %all-to-all-done.2 = bf16[4,128,768]{2,1,0:T(8,128)(2,1)S(1)} async-done(((bf16[4,128,768]{2,1,0:T(8,128)(2,1)}), bf16[4,128,768]{2,1,0:T(8,128)(2,1)S(1)}, u32[]{:S(2)}, u32[]{:S(2)}) %all-to-all-start.2) | async-done | bytes 786464 | tf_op jit(solution)/shard_map/all_to_all | solution.py:32
  (75 shorter events, 18.1 us)
Async XLA Ops:
  2.4 1.0 copy-start.8
  2.4 1.0 copy-start.11
  3.4 6.3 %copy-start.9 = (f32[48,768]{1,0:T(8,128)S(1)}, f32[48,768]{1,0:T(8,128)}, u32[]{:S(2)}) copy-start(f32[48,768]{1,0:T(8,128)} %param.8) | copy-start | bytes 442372
  4.5 18.0 %collective-permute-start = (bf16[128,1536]{1,0:T(8,128)(2,1)}, bf16[128,1536]{1,0:T(8,128)(2,1)S(1)}, u32[]{:S(2)}, u32[]{:S(2)}) collective-permute-start(bf16[128,1536]{1,0:T(8,128)(2,1)} %get-tuple-element.10), channel_id=1, source_target_pairs={{0,6},{1,7},{2,0},{3,1},{4,2},{5,3},{6,4},{7,5},{8,14},{9,15},{10,... | collective-permute-start | bytes 1179656 | tf_op jit(solution)/shard_map/ppermute | solution.py:65
  10.6 45.1 %copy-start.10 = (f32[768,48]{0,1:T(8,128)S(1)}, f32[768,48]{0,1:T(8,128)}, u32[]{:S(2)}) copy-start(f32[768,48]{0,1:T(8,128)} %param.10) | copy-start | bytes 442372
  10.6 45.1 %copy-start.13 = (f32[1,48]{1,0:T(1,128)S(1)}, f32[1,48]{1,0:T(1,128)}, u32[]{:S(2)}) copy-start(f32[1,48]{1,0:T(1,128)} %param.11) | copy-start | bytes 580
  10.6 32.5 %all-to-all-start = ((bf16[8,48,768]{2,1,0:T(8,128)(2,1)}), bf16[8,48,768]{2,1,0:T(8,128)(2,1)S(1)}, u32[]{:S(2)}, u32[]{:S(2)}) async-start(bf16[8,48,768]{2,1,0:T(8,128)(2,1)} %broadcast_in_dim.7), calls=%async_computation | async-start | bytes 1179648 | tf_op jit(solution)/shard_map/all_to_all | solution.py:32
  17.5 13.1 %collective-permute-start.1 = (bf16[128,1536]{1,0:T(8,128)(2,1)}, bf16[128,1536]{1,0:T(8,128)(2,1)S(1)}, u32[]{:S(2)}, u32[]{:S(2)}) collective-permute-start(bf16[128,1536]{1,0:T(8,128)(2,1)} %get-tuple-element.10), channel_id=1, source_target_pairs={{0,4},{1,5},{2,6},{3,7},{4,0},{5,1},{6,2},{7,3},{8,12},{9,13},{10,... | collective-permute-start | bytes 1179656 | tf_op jit(solution)/shard_map/ppermute | solution.py:66
  19.9 20.6 %collective-permute-start.2 = (bf16[128,1536]{1,0:T(8,128)(2,1)}, bf16[128,1536]{1,0:T(8,128)(2,1)S(1)}, u32[]{:S(2)}, u32[]{:S(2)}) collective-permute-start(bf16[128,1536]{1,0:T(8,128)(2,1)} %get-tuple-element.10), channel_id=1, source_target_pairs={{0,2},{1,3},{2,4},{3,5},{4,6},{5,7},{6,0},{7,1},{8,10},{9,11},{10,... | collective-permute-start | bytes 1179656 | tf_op jit(solution)/shard_map/ppermute | solution.py:67
  40.6 54.8 %collective-permute-start.10 = (bf16[512,1536]{1,0:T(8,128)(2,1)S(1)}, bf16[512,1536]{1,0:T(8,128)(2,1)}, u32[]{:S(2)}, u32[]{:S(2)}) collective-permute-start(bf16[512,1536]{1,0:T(8,128)(2,1)S(1)} %constant_dynamic-update-slice_fusion.2), channel_id=1, source_target_pairs={{0,1},{1,0},{2,3},{3,2},{4,5},{5,4},{6,7},{7,6},{8,9},{9,8},{10,11... | collective-permute-start | bytes 4718600 | tf_op jit(solution)/shard_map/ppermute | solution.py:72
  43.0 38.3 %collective-permute-start.4 = (bf16[384,768]{1,0:T(8,128)(2,1)S(1)}, bf16[384,768]{1,0:T(8,128)(2,1)}, u32[]{:S(2)}, u32[]{:S(2)}) collective-permute-start(bf16[384,768]{1,0:T(8,128)(2,1)S(1)} %bitcast.44), channel_id=1, source_target_pairs={{0,448},{8,456},{16,464},{24,472},{32,480},{40,488},{48,496},{56,5... | collective-permute-start | bytes 1769480 | tf_op jit(solution)/shard_map/ppermute | solution.py:74
  53.7 30.5 %collective-permute-start.5 = (bf16[384,768]{1,0:T(8,128)(2,1)S(1)}, bf16[384,768]{1,0:T(8,128)(2,1)}, u32[]{:S(2)}, u32[]{:S(2)}) collective-permute-start(bf16[384,768]{1,0:T(8,128)(2,1)S(1)} %bitcast.45), channel_id=1, source_target_pairs={{0,64},{8,72},{16,80},{24,88},{32,96},{40,104},{48,112},{56,120},{... | collective-permute-start | bytes 1769480 | tf_op jit(solution)/shard_map/ppermute | solution.py:75
  55.7 16.0 %collective-permute-start.3 = (bf16[48,768]{1,0:T(8,128)(2,1)S(1)}, bf16[48,768]{1,0:T(8,128)(2,1)S(1)}, u32[]{:S(2)}, u32[]{:S(2)}) collective-permute-start(bf16[48,768]{1,0:T(8,128)(2,1)S(1)} %get-tuple-element.26), channel_id=1, source_target_pairs={{0,128},{8,136},{16,144},{24,152},{32,160},{40,168},{48,176},{56,1... | collective-permute-start | bytes 221192 | tf_op jit(solution)/shard_map/ppermute | solution.py:56
  71.8 7.8 %copy-start.12 = (f32[1,768]{1,0:T(1,128)S(1)}, f32[1,768]{1,0:T(1,128)}, u32[]{:S(2)}) copy-start(f32[1,768]{1,0:T(1,128)} %param.9) | copy-start | bytes 9220
  72.9 38.6 %all-to-all-start.1 = ((bf16[8,2,48,768]{3,2,1,0:T(8,128)(2,1)}), bf16[8,2,48,768]{3,2,1,0:T(8,128)(2,1)S(1)}, u32[]{:S(2)}, u32[]{:S(2)}) async-start(bf16[8,2,48,768]{3,2,1,0:T(8,128)(2,1)} %broadcast_in_dim.8), calls=%async_computation.1 | async-start | bytes 2359296 | tf_op jit(solution)/shard_map/all_to_all | solution.py:32
  82.3 11.9 %collective-permute-start.6 = (bf16[192,768]{1,0:T(8,128)(2,1)S(1)}, bf16[192,768]{1,0:T(8,128)(2,1)S(1)}, u32[]{:S(2)}, u32[]{:S(2)}) collective-permute-start(bf16[192,768]{1,0:T(8,128)(2,1)S(1)} %slice.122), channel_id=1, source_target_pairs={{0,448},{8,456},{16,464},{24,472},{32,480},{40,488},{48,496},{56,5... | collective-permute-start | bytes 884744 | tf_op jit(solution)/shard_map/ppermute | solution.py:78
  85.2 10.1 %collective-permute-start.7 = (bf16[192,768]{1,0:T(8,128)(2,1)S(1)}, bf16[192,768]{1,0:T(8,128)(2,1)S(1)}, u32[]{:S(2)}, u32[]{:S(2)}) collective-permute-start(bf16[192,768]{1,0:T(8,128)(2,1)S(1)} %slice.123), channel_id=1, source_target_pairs={{0,64},{8,72},{16,80},{24,88},{32,96},{40,104},{48,112},{56,120},{... | collective-permute-start | bytes 884744 | tf_op jit(solution)/shard_map/ppermute | solution.py:78
  95.4 5.9 %copy-start.6 = (bf16[384,768]{1,0:T(8,128)(2,1)}, bf16[384,768]{1,0:T(8,128)(2,1)S(1)}, u32[]{:S(2)}) copy-start(bf16[384,768]{1,0:T(8,128)(2,1)S(1)} %constant_dynamic-update-slice_fusion) | copy-start | bytes 1769476
  111.6 5.8 %copy-start.4 = (f32[512,768]{1,0:T(8,128)S(1)}, f32[512,768]{1,0:T(8,128)}, u32[]{:S(2)}) copy-start(f32[512,768]{1,0:T(8,128)} %fusion.11) | copy-start | bytes 4718596
  111.6 5.8 %copy-start.5 = (f32[512,768]{1,0:T(8,128)S(1)}, f32[512,768]{1,0:T(8,128)}, u32[]{:S(2)}) copy-start(f32[512,768]{1,0:T(8,128)} %fusion.7) | copy-start | bytes 4718596
  111.7 5.7 %copy-start.3 = (f32[512,768]{1,0:T(8,128)S(1)}, f32[512,768]{1,0:T(8,128)}, u32[]{:S(2)}) copy-start(f32[512,768]{1,0:T(8,128)} %fusion.9) | copy-start | bytes 4718596
  111.7 16.6 %collective-permute-start.8 = (bf16[4,2,48,768]{3,2,0,1:T(8,128)(2,1)S(1)}, bf16[4,2,48,768]{3,2,0,1:T(8,128)(2,1)S(1)}, u32[]{:S(2)}, u32[]{:S(2)}) collective-permute-start(bf16[4,2,48,768]{3,2,0,1:T(8,128)(2,1)S(1)} %slice.124), channel_id=1, source_target_pairs={{0,448},{8,456},{16,464},{24,472},{32,480},{40,488},{48,496},{56,5... | collective-permute-start | bytes 1769480 | tf_op jit(solution)/shard_map/ppermute | solution.py:85
  114.0 17.5 %collective-permute-start.9 = (bf16[4,2,48,768]{3,2,1,0:T(8,128)(2,1)S(1)}, bf16[4,2,48,768]{3,2,1,0:T(8,128)(2,1)S(1)}, u32[]{:S(2)}, u32[]{:S(2)}) collective-permute-start(bf16[4,2,48,768]{3,2,1,0:T(8,128)(2,1)S(1)} %slice.126), channel_id=1, source_target_pairs={{0,64},{8,72},{16,80},{24,88},{32,96},{40,104},{48,112},{56,120},{... | collective-permute-start | bytes 1769480 | tf_op jit(solution)/shard_map/ppermute | solution.py:86
  120.0 17.4 %collective-permute-start.12 = (bf16[512,768]{1,0:T(8,128)(2,1)S(1)}, bf16[512,768]{1,0:T(8,128)(2,1)S(1)}, u32[]{:S(2)}, u32[]{:S(2)}) collective-permute-start(bf16[512,768]{1,0:T(8,128)(2,1)S(1)} %convolution_convert_fusion), channel_id=1, source_target_pairs={{0,1},{1,0},{2,3},{3,2},{4,5},{5,4},{6,7},{7,6},{8,9},{9,8},{10,11... | collective-permute-start | bytes 2359304 | tf_op jit(solution)/shard_map/ppermute | solution.py:106
  131.6 5.2 %copy-start.2 = (f32[512,768]{1,0:T(8,128)S(1)}, f32[512,768]{1,0:T(8,128)}, u32[]{:S(2)}) copy-start(f32[512,768]{1,0:T(8,128)} %fusion.19) | copy-start | bytes 4718596
  131.6 5.2 %copy-start.7 = (bf16[384,768]{1,0:T(8,128)(2,1)S(1)}, bf16[384,768]{1,0:T(8,128)(2,1)}, u32[]{:S(2)}) copy-start(bf16[384,768]{1,0:T(8,128)(2,1)} %copy-done.6) | copy-start | bytes 1769476
  131.7 5.0 %copy-start = (f32[512,768]{1,0:T(8,128)S(1)}, f32[512,768]{1,0:T(8,128)}, u32[]{:S(2)}) copy-start(f32[512,768]{1,0:T(8,128)} %fusion.21) | copy-start | bytes 4718596
  131.8 5.0 %copy-start.1 = (f32[512,768]{1,0:T(8,128)S(1)}, f32[512,768]{1,0:T(8,128)}, u32[]{:S(2)}) copy-start(f32[512,768]{1,0:T(8,128)} %fusion.17) | copy-start | bytes 4718596
  133.5 9.2 %collective-permute-start.11 = (bf16[512,768]{1,0:T(8,128)(2,1)}, bf16[512,768]{1,0:T(8,128)(2,1)}, u32[]{:S(2)}, u32[]{:S(2)}) collective-permute-start(bf16[512,768]{1,0:T(8,128)(2,1)} %convolution_convert_fusion.1), channel_id=1, source_target_pairs={{0,1},{1,0},{2,3},{3,2},{4,5},{5,4},{6,7},{7,6},{8,9},{9,8},{10,11... | collective-permute-start | bytes 2359304 | tf_op jit(solution)/shard_map/ppermute | solution.py:106
  139.2 15.8 %all-to-all-start.3 = ((bf16[4,128,768]{2,1,0:T(8,128)(2,1)}), bf16[4,128,768]{2,1,0:T(8,128)(2,1)S(1)}, u32[]{:S(2)}, u32[]{:S(2)}) async-start(bf16[4,128,768]{2,1,0:T(8,128)(2,1)} %bitcast.16), calls=%async_computation.3 | async-start | bytes 1572864 | tf_op jit(solution)/shard_map/all_to_all | solution.py:32
  155.1 15.0 %all-to-all-start.2 = ((bf16[4,128,768]{2,1,0:T(8,128)(2,1)}), bf16[4,128,768]{2,1,0:T(8,128)(2,1)S(1)}, u32[]{:S(2)}, u32[]{:S(2)}) async-start(bf16[4,128,768]{2,1,0:T(8,128)(2,1)} %bitcast.12), calls=%async_computation.2 | async-start | bytes 1572864 | tf_op jit(solution)/shard_map/all_to_all | solution.py:32
where the time goes:
time: 172 us; the launch traced here: 171 us
  waiting for transfers between devices  69.7 us (41%)
  starting transfers between devices  64.7 us (38%)
  matrix products  25.8 us (15%)
  local copies, waits for them, and re-layouts  5.39 us (3%)
  other arithmetic  4.94 us (3%)
    all_to_all x4, waiting for transfers between devices, swapped(): lax.all_to_all(blocks, axis, 0, 0, axis_index_groups=groups, tiled=True)  28.1 us
    all_to_all x4, starting transfers between devices, swapped(): lax.all_to_all(blocks, axis, 0, 0, axis_index_groups=groups, tiled=True)  20.6 us
    dot_general x8, matrix products, hidden_of(): jnp.dot(t[:, place * width:(place + 1) * width], block, preferred_element...  18.7 us
    ppermute x1, waiting for transfers between devices, body(): down_two = lax.ppermute(down_piece, PLANE, FROM_TWO)  14.1 us
    ppermute x1, starting transfers between devices, body(): up_next = lax.ppermute(up_own, PLANE, FROM_NEXT)  10.7 us
    ppermute x1, waiting for transfers between devices, body(): lax.ppermute(normed, 'tp', X_LAST)  9.95 us
    ppermute x1, waiting for transfers between devices, body(): lax.ppermute(normed, 'tp', X_TWO)  8.01 us
    dot_general x4, matrix products, terms(): lax.dot_general(hidden, down, (((1,), (1,)), ((), ())), preferred_element...  7.15 us
  transfers between devices with their start and end apart: 17, of which 9 were waited for; matrix products, arithmetic and copies ran while one was open for 18% of the time, Pallas kernels for 0%

commit v1 on v0

--- a/solution.py
+++ b/solution.py
@@ -33,7 +33,8 @@
 
 
 def spread(shard, axis, groups):
-    return swapped(jnp.broadcast_to(shard[None], (len(groups[0]), *shard.shape)), axis, groups)
+    copies = jnp.broadcast_to(shard[None], (len(groups[0]), *shard.shape))
+    return swapped(copies, axis, groups).reshape(-1, shard.shape[1])
 
 
 def rolled(a, by, width):
@@ -49,9 +50,8 @@
     x = lax.axis_index("tp") // 2
     rows, d = tokens.shape
     width = d // ZLO
-    hidden_width = up_weight.shape[1]
 
-    up_own = spread(up_weight.astype(BF16), "fs", ROW_GROUPS).reshape(width, hidden_width)
+    up_own = spread(up_weight.astype(BF16), "fs", ROW_GROUPS)
     down_piece = (down_weight * down_scale).T.astype(BF16)
     down_two = lax.ppermute(down_piece, PLANE, FROM_TWO)
 
@@ -71,30 +71,25 @@
         own = lax.dynamic_update_slice(own, block, (rows * ((x + k) % X), 0))
     other = lax.ppermute(own, "tp", OTHER_CORE)
 
-    up_next = lax.ppermute(up_own, PLANE, FROM_NEXT)
-    up_last = lax.ppermute(up_own, PLANE, FROM_LAST)
-    half = width // 2
-    up_two = jnp.concatenate(
-        [lax.ppermute(up_next[:half], PLANE, FROM_NEXT), lax.ppermute(up_last[half:], PLANE, FROM_LAST)],
-        0,
+    up = [
+        up_own,
+        lax.ppermute(up_own, PLANE, FROM_NEXT),
+        lax.ppermute(up_own, PLANE, FROM_TWO),
+        lax.ppermute(up_own, PLANE, FROM_LAST),
+    ]
+    up = lax.optimization_barrier(jnp.concatenate(up, 0))
+
+    down_own = spread(down_piece, "fs", ROW_GROUPS)
+    down_two, down_own = lax.optimization_barrier((down_two, down_own))
+    down_two = spread(down_two, "fs", ROW_GROUPS)
+    down_a = jnp.concatenate([down_own, down_two], 0)
+    down_b = jnp.concatenate(
+        [lax.ppermute(down_own, PLANE, FROM_NEXT), lax.ppermute(down_own, PLANE, FROM_LAST)], 0
     )
-
-    pieces, up_own = lax.optimization_barrier((jnp.stack([down_piece, down_two]), up_own))
-    copies = jnp.broadcast_to(pieces[None], (Y, *pieces.shape))
-    down_a = swapped(copies, "fs", ROW_GROUPS)
-    first = lax.ppermute(down_a[: Y // 2], PLANE, FROM_NEXT)
-    second = lax.ppermute(down_a[Y // 2 :], PLANE, FROM_LAST)
-    down_b = jnp.stack(
-        [jnp.concatenate([first[:, 0], second[:, 1]], 0), jnp.concatenate([first[:, 1], second[:, 0]], 0)]
-    )
-    down_b = down_b.reshape(2 * width, hidden_width)
-    down_a = down_a.transpose(1, 0, 2, 3).reshape(2 * width, hidden_width)
+    down_a, down_b = lax.optimization_barrier(down_a), lax.optimization_barrier(down_b)
 
     def hidden_of(t):
-        pre = 0.0
-        for k, block in enumerate([up_own, up_next, up_last, up_two]):
-            place = (0, 1, 3, 2)[k]
-            pre += jnp.dot(t[:, place * width : (place + 1) * width], block, preferred_element_type=F32)
+        pre = jnp.dot(t, up, preferred_element_type=F32)
         return jnp.square(jnp.maximum(pre * up_scale, 0.0)).astype(BF16)
 
     hidden_own, hidden_other = hidden_of(own), hidden_of(other)

time: 172 us -> 165 us (0.959)
  starting transfers between devices: 64.7 us -> 77.4 us
  waiting for transfers between devices: 69.7 us -> 57.4 us
  matrix products: 25.8 us -> 14 us
  other arithmetic: 4.94 us -> 7.56 us
    dot_general x8 -> x2, matrix products: 18.7 us -> 4.6 us  [hidden_of(): pre = jnp.dot(t, up, preferred_element_type=F32)]
    all_to_all x4 -> x5, starting transfers between devices: 20.6 us -> 29.1 us  [swapped(): lax.all_to_all(blocks, axis, 0, 0, axis_index_groups=groups, tiled=True)]
    ppermute x1, waiting for transfers between devices: 9.95 us -> 2.7 us  [body(): lax.ppermute(normed, 'tp', X_LAST)]
    ppermute x6 -> x5, waiting for transfers between devices: 9.53 us -> 2.34 us  [the longest x1 1.51 us: body(): lax.ppermute(down_own, PLANE, FROM_LAST)]
    ppermute x1, waiting for transfers between devices: 14.1 us -> 20.7 us  [body(): down_two = lax.ppermute(down_piece, PLANE, FROM_TWO)]
    ppermute x1, waiting for transfers between devices: 8.01 us -> 2.6 us  [body(): lax.ppermute(normed, 'tp', X_TWO)]
    ppermute x1, waiting for transfers between devices: 0.01 us -> 4.4 us  [body(): lax.ppermute(normed, 'tp', X_NEXT)]
    all_to_all x4 -> x5, waiting for transfers between devices: 28.1 us -> 24.7 us  [swapped(): lax.all_to_all(blocks, axis, 0, 0, axis_index_groups=groups, tiled=True)]
  transfers between devices with their start and end apart: 17 -> 17, of which waited for: 9 -> 9; matrix products, arithmetic and copies ran while one was open for 18% -> 14% of each run, Pallas kernels for 0% -> 0%
where the time goes in v1:
time: 165 us; the launch traced here: 164 us
  starting transfers between devices  77.4 us (47%)
  waiting for transfers between devices  57.4 us (35%)
  matrix products  14 us (8%)
  other arithmetic  7.56 us (5%)
  local copies, waits for them, and re-layouts  6.83 us (4%)
    all_to_all x5, starting transfers between devices, swapped(): lax.all_to_all(blocks, axis, 0, 0, axis_index_groups=groups, tiled=True)  29.1 us
    all_to_all x5, waiting for transfers between devices, swapped(): lax.all_to_all(blocks, axis, 0, 0, axis_index_groups=groups, tiled=True)  24.7 us
    ppermute x1, waiting for transfers between devices, body(): down_two = lax.ppermute(down_piece, PLANE, FROM_TWO)  20.7 us
    dot_general x4, matrix products, terms(): lax.dot_general(hidden, down, (((1,), (1,)), ((), ())), preferred_element...  9.39 us
    ppermute x2, starting transfers between devices, chunk(): arrived = lax.ppermute(terms(hidden_other).astype(BF16), 'tp', OTHER_CORE)  7.18 us
    ppermute x1, starting transfers between devices, body(): lax.ppermute(up_own, PLANE, FROM_NEXT)  6.13 us
    ppermute x1, starting transfers between devices, body(): lax.ppermute(up_own, PLANE, FROM_TWO)  5.81 us
    ppermute x1, starting transfers between devices, body(): lax.ppermute(down_own, PLANE, FROM_NEXT)  4.94 us
  transfers between devices with their start and end apart: 17, of which 9 were waited for; matrix products, arithmetic and copies ran while one was open for 14% of the time, Pallas kernels for 0%

profile of v1, /device:TPU:1, one launch (start us, length us, event | category | flops | bytes accessed | tf_op | source)
XLA Modules:
  0.0 163.7 jit_solution(109248709150038133)
XLA Ops:
  1.8 7.6 %all-to-all-start = ((bf16[8,48,768]{2,1,0:T(8,128)(2,1)}), bf16[8,48,768]{2,1,0:T(8,128)(2,1)S(1)}, u32[]{:S(2)}, u32[]{:S(2)}) async-start(bf16[8,48,768]{2,1,0:T(8,128)(2,1)} %broadcast_in_dim.9), calls=%async_computation | async-start | bytes 1179648 | tf_op jit(solution)/shard_map/all_to_all | solution.py:32
  13.6 4.4 %collective-permute-start = (bf16[128,1536]{1,0:T(8,128)(2,1)}, bf16[128,1536]{1,0:T(8,128)(2,1)S(1)}, u32[]{:S(2)}, u32[]{:S(2)}) collective-permute-start(bf16[128,1536]{1,0:T(8,128)(2,1)} %get-tuple-element.10), channel_id=1, source_target_pairs={{0,6},{1,7},{2,0},{3,1},{4,2},{5,3},{6,4},{7,5},{8,14},{9,15},{10,... | collective-permute-start | bytes 1179656 | tf_op jit(solution)/shard_map/ppermute | solution.py:65
  18.0 2.4 %collective-permute-start.1 = (bf16[128,1536]{1,0:T(8,128)(2,1)}, bf16[128,1536]{1,0:T(8,128)(2,1)S(1)}, u32[]{:S(2)}, u32[]{:S(2)}) collective-permute-start(bf16[128,1536]{1,0:T(8,128)(2,1)} %get-tuple-element.10), channel_id=1, source_target_pairs={{0,4},{1,5},{2,6},{3,7},{4,0},{5,1},{6,2},{7,3},{8,12},{9,13},{10,... | collective-permute-start | bytes 1179656 | tf_op jit(solution)/shard_map/ppermute | solution.py:66
  20.4 2.5 %collective-permute-start.2 = (bf16[128,1536]{1,0:T(8,128)(2,1)}, bf16[128,1536]{1,0:T(8,128)(2,1)S(1)}, u32[]{:S(2)}, u32[]{:S(2)}) collective-permute-start(bf16[128,1536]{1,0:T(8,128)(2,1)} %get-tuple-element.10), channel_id=1, source_target_pairs={{0,2},{1,3},{2,4},{3,5},{4,6},{5,7},{6,0},{7,1},{8,10},{9,11},{10,... | collective-permute-start | bytes 1179656 | tf_op jit(solution)/shard_map/ppermute | solution.py:67
  24.0 4.4 %collective-permute-done = bf16[128,1536]{1,0:T(8,128)(2,1)S(1)} collective-permute-done((bf16[128,1536]{1,0:T(8,128)(2,1)}, bf16[128,1536]{1,0:T(8,128)(2,1)S(1)}, u32[]{:S(2)}, u32[]{:S(2)}) %collective-permute-start) | collective-permute-done | bytes 393248 | tf_op jit(solution)/shard_map/ppermute | solution.py:65
  28.4 2.6 %collective-permute-done.1 = bf16[128,1536]{1,0:T(8,128)(2,1)S(1)} collective-permute-done((bf16[128,1536]{1,0:T(8,128)(2,1)}, bf16[128,1536]{1,0:T(8,128)(2,1)S(1)}, u32[]{:S(2)}, u32[]{:S(2)}) %collective-permute-start.1) | collective-permute-done | bytes 393248 | tf_op jit(solution)/shard_map/ppermute | solution.py:66
  32.0 6.4 %all-to-all-start.1 = ((bf16[8,48,768]{2,1,0:T(8,128)(2,1)}), bf16[8,48,768]{2,1,0:T(8,128)(2,1)S(1)}, u32[]{:S(2)}, u32[]{:S(2)}) async-start(bf16[8,48,768]{2,1,0:T(8,128)(2,1)} %broadcast_in_dim.10), calls=%async_computation.1 | async-start | bytes 1179648 | tf_op jit(solution)/shard_map/all_to_all | solution.py:32
  38.3 2.7 %collective-permute-done.2 = bf16[128,1536]{1,0:T(8,128)(2,1)S(1)} collective-permute-done((bf16[128,1536]{1,0:T(8,128)(2,1)}, bf16[128,1536]{1,0:T(8,128)(2,1)S(1)}, u32[]{:S(2)}, u32[]{:S(2)}) %collective-permute-start.2) | collective-permute-done | bytes 393248 | tf_op jit(solution)/shard_map/ppermute | solution.py:67
  41.1 4.8 %collective-permute-start.9 = (bf16[512,1536]{1,0:T(8,128)(2,1)S(1)}, bf16[512,1536]{1,0:T(8,128)(2,1)}, u32[]{:S(2)}, u32[]{:S(2)}) collective-permute-start(bf16[512,1536]{1,0:T(8,128)(2,1)S(1)} %constant_dynamic-update-slice_fusion), channel_id=1, source_target_pairs={{0,1},{1,0},{2,3},{3,2},{4,5},{5,4},{6,7},{7,6},{8,9},{9,8},{10,11... | collective-permute-start | bytes 4718600 | tf_op jit(solution)/shard_map/ppermute | solution.py:72
  45.9 4.0 %collective-permute-start.5 = (bf16[384,768]{1,0:T(8,128)(2,1)S(1)}, bf16[384,768]{1,0:T(8,128)(2,1)S(1)}, u32[]{:S(2)}, u32[]{:S(2)}) collective-permute-start(bf16[384,768]{1,0:T(8,128)(2,1)S(1)} %bitcast.20), channel_id=1, source_target_pairs={{0,64},{8,72},{16,80},{24,88},{32,96},{40,104},{48,112},{56,120},{... | collective-permute-start | bytes 1769480 | tf_op jit(solution)/shard_map/ppermute | solution.py:78
  49.9 5.8 %collective-permute-start.4 = (bf16[384,768]{1,0:T(8,128)(2,1)S(1)}, bf16[384,768]{1,0:T(8,128)(2,1)}, u32[]{:S(2)}, u32[]{:S(2)}) collective-permute-start(bf16[384,768]{1,0:T(8,128)(2,1)S(1)} %bitcast.21), channel_id=1, source_target_pairs={{0,128},{8,136},{16,144},{24,152},{32,160},{40,168},{48,176},{56,1... | collective-permute-start | bytes 1769480 | tf_op jit(solution)/shard_map/ppermute | solution.py:77
  55.7 6.1 %collective-permute-start.3 = (bf16[384,768]{1,0:T(8,128)(2,1)S(1)}, bf16[384,768]{1,0:T(8,128)(2,1)}, u32[]{:S(2)}, u32[]{:S(2)}) collective-permute-start(bf16[384,768]{1,0:T(8,128)(2,1)S(1)} %bitcast.22), channel_id=1, source_target_pairs={{0,448},{8,456},{16,464},{24,472},{32,480},{40,488},{48,496},{56,5... | collective-permute-start | bytes 1769480 | tf_op jit(solution)/shard_map/ppermute | solution.py:76
  61.9 2.8 %collective-permute-start.6 = (bf16[48,768]{1,0:T(8,128)(2,1)}, bf16[48,768]{1,0:T(8,128)(2,1)S(1)}, u32[]{:S(2)}, u32[]{:S(2)}) collective-permute-start(bf16[48,768]{1,0:T(8,128)(2,1)} %copy-done.12), channel_id=1, source_target_pairs={{0,128},{8,136},{16,144},{24,152},{32,160},{40,168},{48,176},{56,1... | collective-permute-start | bytes 221192 | tf_op jit(solution)/shard_map/ppermute | solution.py:56
  64.7 20.7 %collective-permute-done.6 = bf16[48,768]{1,0:T(8,128)(2,1)S(1)} collective-permute-done((bf16[48,768]{1,0:T(8,128)(2,1)}, bf16[48,768]{1,0:T(8,128)(2,1)S(1)}, u32[]{:S(2)}, u32[]{:S(2)}) %collective-permute-start.6) | collective-permute-done | bytes 73760 | tf_op jit(solution)/shard_map/ppermute | solution.py:56
  85.4 3.2 %collective-permute-start.8 = (bf16[384,768]{1,0:T(8,128)(2,1)S(1)}, bf16[384,768]{1,0:T(8,128)(2,1)}, u32[]{:S(2)}, u32[]{:S(2)}) collective-permute-start(bf16[384,768]{1,0:T(8,128)(2,1)S(1)} %bitcast.24), channel_id=1, source_target_pairs={{0,64},{8,72},{16,80},{24,88},{32,96},{40,104},{48,112},{56,120},{... | collective-permute-start | bytes 1769480 | tf_op jit(solution)/shard_map/ppermute | solution.py:87
  88.7 4.9 %collective-permute-start.7 = (bf16[384,768]{1,0:T(8,128)(2,1)S(1)}, bf16[384,768]{1,0:T(8,128)(2,1)}, u32[]{:S(2)}, u32[]{:S(2)}) collective-permute-start(bf16[384,768]{1,0:T(8,128)(2,1)S(1)} %bitcast.25), channel_id=1, source_target_pairs={{0,448},{8,456},{16,464},{24,472},{32,480},{40,488},{48,496},{56,5... | collective-permute-start | bytes 1769480 | tf_op jit(solution)/shard_map/ppermute | solution.py:87
  94.5 6.9 %all-to-all-start.3 = ((bf16[8,48,768]{2,1,0:T(8,128)(2,1)}), bf16[8,48,768]{2,1,0:T(8,128)(2,1)S(1)}, u32[]{:S(2)}, u32[]{:S(2)}) async-start(bf16[8,48,768]{2,1,0:T(8,128)(2,1)} %broadcast_in_dim.11), calls=%async_computation.3 | async-start | bytes 1179648 | tf_op jit(solution)/shard_map/all_to_all | solution.py:32
  101.5 1.6 pad_maximum_fusion
  103.1 1.5 collective-permute-done.8
  106.7 3.2 %multiply_convert_fusion = bf16[512,768]{1,0:T(8,128)(2,1)S(1)} fusion(bf16[512,1536]{1,0:T(8,128)(2,1)} %collective-permute-done.9, bf16[1536,768]{1,0:T(8,128)(2,1)S(1)} %pad_maximum_fusion, f32[768]{0:T(1024)S(1)} %reduce.2), kind=kOutput, calls=%fused_computation.3 | convolution fusion | flops 1209532416 | bytes 4721664 | tf_op jit(solution)/shard_map/dot_general | solution.py:92
  110.0 1.7 %convolution_convert_fusion.1 = bf16[512,768]{1,0:T(8,128)(2,1)} fusion(bf16[512,768]{1,0:T(8,128)(2,1)S(1)} %multiply_convert_fusion, bf16[768,768]{1,0:T(8,128)(2,1)S(1)} %pad_maximum_fusion.1), kind=kOutput, calls=%fused_computation.6 | convolution fusion | flops 604372992 | bytes 2752512 | tf_op jit(solution)/shard_map/dot_general | solution.py:99
  111.7 3.6 %collective-permute-start.10 = (bf16[512,768]{1,0:T(8,128)(2,1)}, bf16[512,768]{1,0:T(8,128)(2,1)}, u32[]{:S(2)}, u32[]{:S(2)}) collective-permute-start(bf16[512,768]{1,0:T(8,128)(2,1)} %convolution_convert_fusion.1), channel_id=1, source_target_pairs={{0,1},{1,0},{2,3},{3,2},{4,5},{5,4},{6,7},{7,6},{8,9},{9,8},{10,11... | collective-permute-start | bytes 2359304 | tf_op jit(solution)/shard_map/ppermute | solution.py:101
  115.3 4.4 %all-to-all-done.3 = bf16[8,48,768]{2,1,0:T(8,128)(2,1)S(1)} async-done(((bf16[8,48,768]{2,1,0:T(8,128)(2,1)}), bf16[8,48,768]{2,1,0:T(8,128)(2,1)S(1)}, u32[]{:S(2)}, u32[]{:S(2)}) %all-to-all-start.3) | async-done | bytes 589856 | tf_op jit(solution)/shard_map/all_to_all | solution.py:32
  121.3 1.7 %convolution_convert_fusion = bf16[512,768]{1,0:T(8,128)(2,1)} fusion(bf16[512,768]{1,0:T(8,128)(2,1)S(1)} %copy-done.18, bf16[768,768]{1,0:T(8,128)(2,1)S(1)} %pad_maximum_fusion.2), kind=kOutput, calls=%fused_computation.5 | convolution fusion | flops 604372992 | bytes 2752512 | tf_op jit(solution)/shard_map/dot_general | solution.py:99
  122.9 3.6 %collective-permute-start.11 = (bf16[512,768]{1,0:T(8,128)(2,1)}, bf16[512,768]{1,0:T(8,128)(2,1)S(1)}, u32[]{:S(2)}, u32[]{:S(2)}) collective-permute-start(bf16[512,768]{1,0:T(8,128)(2,1)} %convolution_convert_fusion), channel_id=1, source_target_pairs={{0,1},{1,0},{2,3},{3,2},{4,5},{5,4},{6,7},{7,6},{8,9},{9,8},{10,11... | collective-permute-start | bytes 2359304 | tf_op jit(solution)/shard_map/ppermute | solution.py:101
  126.5 1.4 multiply_convert_fusion.1
  127.9 3.1 %add_convert_fusion.1 = bf16[512,768]{1,0:T(8,128)(2,1)} fusion(bf16[512,768]{1,0:T(8,128)(2,1)} %collective-permute-done.10, bf16[512,768]{1,0:T(8,128)(2,1)S(1)} %multiply_convert_fusion.1, bf16[768,768]{1,0:T(8,128)(2,1)S(1)} %copy-done.4), kind=kOutput, calls=%fused_computation.2 | convolution fusion | flops 605159424 | bytes 3538944 | tf_op jit(solution)/shard_map/dot_general | solution.py:99
  131.1 4.7 %all-to-all-start.2 = ((bf16[4,128,768]{2,1,0:T(8,128)(2,1)}), bf16[4,128,768]{2,1,0:T(8,128)(2,1)S(1)}, u32[]{:S(2)}, u32[]{:S(2)}) async-start(bf16[4,128,768]{2,1,0:T(8,128)(2,1)} %bitcast.4), calls=%async_computation.2 | async-start | bytes 1572864 | tf_op jit(solution)/shard_map/all_to_all | solution.py:32
  135.8 2.9 %add_convert_fusion = bf16[512,768]{1,0:T(8,128)(2,1)} fusion(bf16[512,768]{1,0:T(8,128)(2,1)S(1)} %collective-permute-done.11, bf16[512,768]{1,0:T(8,128)(2,1)} %copy-done.16, bf16[768,768]{1,0:T(8,128)(2,1)S(1)} %copy-done.6), kind=kOutput, calls=%fused_computation.1 | convolution fusion | flops 605159424 | bytes 3538944 | tf_op jit(solution)/shard_map/dot_general | solution.py:99
  138.6 9.2 %all-to-all-done.2 = bf16[4,128,768]{2,1,0:T(8,128)(2,1)S(1)} async-done(((bf16[4,128,768]{2,1,0:T(8,128)(2,1)}), bf16[4,128,768]{2,1,0:T(8,128)(2,1)S(1)}, u32[]{:S(2)}, u32[]{:S(2)}) %all-to-all-start.2) | async-done | bytes 786464 | tf_op jit(solution)/shard_map/all_to_all | solution.py:32
  147.9 3.5 %all-to-all-start.4 = ((bf16[4,128,768]{2,1,0:T(8,128)(2,1)}), bf16[4,128,768]{2,1,0:T(8,128)(2,1)S(1)}, u32[]{:S(2)}, u32[]{:S(2)}) async-start(bf16[4,128,768]{2,1,0:T(8,128)(2,1)} %bitcast.6), calls=%async_computation.4 | async-start | bytes 1572864 | tf_op jit(solution)/shard_map/all_to_all | solution.py:32
  151.5 11.0 %all-to-all-done.4 = bf16[4,128,768]{2,1,0:T(8,128)(2,1)S(1)} async-done(((bf16[4,128,768]{2,1,0:T(8,128)(2,1)}), bf16[4,128,768]{2,1,0:T(8,128)(2,1)S(1)}, u32[]{:S(2)}, u32[]{:S(2)}) %all-to-all-start.4) | async-done | bytes 786464 | tf_op jit(solution)/shard_map/all_to_all | solution.py:32
  (71 shorter events, 13.7 us)
Async XLA Ops:
  0.0 9.5 %copy-start = (bf16[128,1536]{1,0:T(8,128)(2,1)S(1)}, bf16[128,1536]{1,0:T(8,128)(2,1)}, u32[]{:S(2)}) copy-start(bf16[128,1536]{1,0:T(8,128)(2,1)} %param.6) | copy-start | bytes 1179652
  0.0 9.6 %copy-start.13 = (f32[1536]{0:T(1024)S(1)}, f32[1536]{0:T(1024)}, u32[]{:S(2)}) copy-start(f32[1536]{0:T(1024)} %param.7) | copy-start | bytes 18436
  1.8 29.3 %all-to-all-start = ((bf16[8,48,768]{2,1,0:T(8,128)(2,1)}), bf16[8,48,768]{2,1,0:T(8,128)(2,1)S(1)}, u32[]{:S(2)}, u32[]{:S(2)}) async-start(bf16[8,48,768]{2,1,0:T(8,128)(2,1)} %broadcast_in_dim.9), calls=%async_computation | async-start | bytes 1179648 | tf_op jit(solution)/shard_map/all_to_all | solution.py:32
  11.4 1.1 copy-start.11
  12.5 10.5 %copy-start.15 = (f32[1,48]{1,0:T(1,128)S(1)}, f32[1,48]{1,0:T(1,128)}, u32[]{:S(2)}) copy-start(f32[1,48]{1,0:T(1,128)} %param.11) | copy-start | bytes 580
  13.6 14.8 %collective-permute-start = (bf16[128,1536]{1,0:T(8,128)(2,1)}, bf16[128,1536]{1,0:T(8,128)(2,1)S(1)}, u32[]{:S(2)}, u32[]{:S(2)}) collective-permute-start(bf16[128,1536]{1,0:T(8,128)(2,1)} %get-tuple-element.10), channel_id=1, source_target_pairs={{0,6},{1,7},{2,0},{3,1},{4,2},{5,3},{6,4},{7,5},{8,14},{9,15},{10,... | collective-permute-start | bytes 1179656 | tf_op jit(solution)/shard_map/ppermute | solution.py:65
  18.0 13.1 %collective-permute-start.1 = (bf16[128,1536]{1,0:T(8,128)(2,1)}, bf16[128,1536]{1,0:T(8,128)(2,1)S(1)}, u32[]{:S(2)}, u32[]{:S(2)}) collective-permute-start(bf16[128,1536]{1,0:T(8,128)(2,1)} %get-tuple-element.10), channel_id=1, source_target_pairs={{0,4},{1,5},{2,6},{3,7},{4,0},{5,1},{6,2},{7,3},{8,12},{9,13},{10,... | collective-permute-start | bytes 1179656 | tf_op jit(solution)/shard_map/ppermute | solution.py:66
  20.4 20.6 %collective-permute-start.2 = (bf16[128,1536]{1,0:T(8,128)(2,1)}, bf16[128,1536]{1,0:T(8,128)(2,1)S(1)}, u32[]{:S(2)}, u32[]{:S(2)}) collective-permute-start(bf16[128,1536]{1,0:T(8,128)(2,1)} %get-tuple-element.10), channel_id=1, source_target_pairs={{0,2},{1,3},{2,4},{3,5},{4,6},{5,7},{6,0},{7,1},{8,10},{9,11},{10,... | collective-permute-start | bytes 1179656 | tf_op jit(solution)/shard_map/ppermute | solution.py:67
  24.0 8.0 %copy-start.12 = (bf16[48,768]{1,0:T(8,128)(2,1)}, bf16[48,768]{1,0:T(8,128)(2,1)S(1)}, u32[]{:S(2)}) copy-start(bf16[48,768]{1,0:T(8,128)(2,1)S(1)} %fusion.3) | copy-start | bytes 221188
  28.4 65.2 %copy-start.14 = (f32[1,768]{1,0:T(1,128)S(1)}, f32[1,768]{1,0:T(1,128)}, u32[]{:S(2)}) copy-start(f32[1,768]{1,0:T(1,128)} %param.9) | copy-start | bytes 9220
  32.0 53.4 %all-to-all-start.1 = ((bf16[8,48,768]{2,1,0:T(8,128)(2,1)}), bf16[8,48,768]{2,1,0:T(8,128)(2,1)S(1)}, u32[]{:S(2)}, u32[]{:S(2)}) async-start(bf16[8,48,768]{2,1,0:T(8,128)(2,1)} %broadcast_in_dim.10), calls=%async_computation.1 | async-start | bytes 1179648 | tf_op jit(solution)/shard_map/all_to_all | solution.py:32
  41.1 65.7 %collective-permute-start.9 = (bf16[512,1536]{1,0:T(8,128)(2,1)S(1)}, bf16[512,1536]{1,0:T(8,128)(2,1)}, u32[]{:S(2)}, u32[]{:S(2)}) collective-permute-start(bf16[512,1536]{1,0:T(8,128)(2,1)S(1)} %constant_dynamic-update-slice_fusion), channel_id=1, source_target_pairs={{0,1},{1,0},{2,3},{3,2},{4,5},{5,4},{6,7},{7,6},{8,9},{9,8},{10,11... | collective-permute-start | bytes 4718600 | tf_op jit(solution)/shard_map/ppermute | solution.py:72
  45.9 42.7 %collective-permute-start.5 = (bf16[384,768]{1,0:T(8,128)(2,1)S(1)}, bf16[384,768]{1,0:T(8,128)(2,1)S(1)}, u32[]{:S(2)}, u32[]{:S(2)}) collective-permute-start(bf16[384,768]{1,0:T(8,128)(2,1)S(1)} %bitcast.20), channel_id=1, source_target_pairs={{0,64},{8,72},{16,80},{24,88},{32,96},{40,104},{48,112},{56,120},{... | collective-permute-start | bytes 1769480 | tf_op jit(solution)/shard_map/ppermute | solution.py:78
  49.9 51.5 %collective-permute-start.4 = (bf16[384,768]{1,0:T(8,128)(2,1)S(1)}, bf16[384,768]{1,0:T(8,128)(2,1)}, u32[]{:S(2)}, u32[]{:S(2)}) collective-permute-start(bf16[384,768]{1,0:T(8,128)(2,1)S(1)} %bitcast.21), channel_id=1, source_target_pairs={{0,128},{8,136},{16,144},{24,152},{32,160},{40,168},{48,176},{56,1... | collective-permute-start | bytes 1769480 | tf_op jit(solution)/shard_map/ppermute | solution.py:77
  55.7 45.7 %collective-permute-start.3 = (bf16[384,768]{1,0:T(8,128)(2,1)S(1)}, bf16[384,768]{1,0:T(8,128)(2,1)}, u32[]{:S(2)}, u32[]{:S(2)}) collective-permute-start(bf16[384,768]{1,0:T(8,128)(2,1)S(1)} %bitcast.22), channel_id=1, source_target_pairs={{0,448},{8,456},{16,464},{24,472},{32,480},{40,488},{48,496},{56,5... | collective-permute-start | bytes 1769480 | tf_op jit(solution)/shard_map/ppermute | solution.py:76
  61.9 23.5 %collective-permute-start.6 = (bf16[48,768]{1,0:T(8,128)(2,1)}, bf16[48,768]{1,0:T(8,128)(2,1)S(1)}, u32[]{:S(2)}, u32[]{:S(2)}) collective-permute-start(bf16[48,768]{1,0:T(8,128)(2,1)} %copy-done.12), channel_id=1, source_target_pairs={{0,128},{8,136},{16,144},{24,152},{32,160},{40,168},{48,176},{56,1... | collective-permute-start | bytes 221192 | tf_op jit(solution)/shard_map/ppermute | solution.py:56
  85.4 19.2 %collective-permute-start.8 = (bf16[384,768]{1,0:T(8,128)(2,1)S(1)}, bf16[384,768]{1,0:T(8,128)(2,1)}, u32[]{:S(2)}, u32[]{:S(2)}) collective-permute-start(bf16[384,768]{1,0:T(8,128)(2,1)S(1)} %bitcast.24), channel_id=1, source_target_pairs={{0,64},{8,72},{16,80},{24,88},{32,96},{40,104},{48,112},{56,120},{... | collective-permute-start | bytes 1769480 | tf_op jit(solution)/shard_map/ppermute | solution.py:87
  88.6 5.9 %copy-start.9 = (bf16[384,768]{1,0:T(8,128)(2,1)}, bf16[384,768]{1,0:T(8,128)(2,1)S(1)}, u32[]{:S(2)}) copy-start(bf16[384,768]{1,0:T(8,128)(2,1)S(1)} %collective-permute-done.5) | copy-start | bytes 1769476
  88.7 16.7 %collective-permute-start.7 = (bf16[384,768]{1,0:T(8,128)(2,1)S(1)}, bf16[384,768]{1,0:T(8,128)(2,1)}, u32[]{:S(2)}, u32[]{:S(2)}) collective-permute-start(bf16[384,768]{1,0:T(8,128)(2,1)S(1)} %bitcast.25), channel_id=1, source_target_pairs={{0,448},{8,456},{16,464},{24,472},{32,480},{40,488},{48,496},{56,5... | collective-permute-start | bytes 1769480 | tf_op jit(solution)/shard_map/ppermute | solution.py:87
  94.5 25.2 %all-to-all-start.3 = ((bf16[8,48,768]{2,1,0:T(8,128)(2,1)}), bf16[8,48,768]{2,1,0:T(8,128)(2,1)S(1)}, u32[]{:S(2)}, u32[]{:S(2)}) async-start(bf16[8,48,768]{2,1,0:T(8,128)(2,1)} %broadcast_in_dim.11), calls=%async_computation.3 | async-start | bytes 1179648 | tf_op jit(solution)/shard_map/all_to_all | solution.py:32
  103.1 6.9 %copy-start.1 = (bf16[1536,768]{1,0:T(8,128)(2,1)}, bf16[1536,768]{1,0:T(8,128)(2,1)S(1)}, u32[]{:S(2)}) copy-start(bf16[1536,768]{1,0:T(8,128)(2,1)S(1)} %pad_maximum_fusion) | copy-start | bytes 7077892
  106.7 3.3 %copy-start.3 = (bf16[768,768]{1,0:T(8,128)(2,1)}, bf16[768,768]{1,0:T(8,128)(2,1)S(1)}, u32[]{:S(2)}) copy-start(bf16[768,768]{1,0:T(8,128)(2,1)S(1)} %pad_maximum_fusion.1) | copy-start | bytes 3538948
  110.0 1.7 %copy-start.17 = (bf16[512,768]{1,0:T(8,128)(2,1)}, bf16[512,768]{1,0:T(8,128)(2,1)S(1)}, u32[]{:S(2)}) copy-start(bf16[512,768]{1,0:T(8,128)(2,1)S(1)} %multiply_convert_fusion) | copy-start | bytes 2359300
  111.7 16.2 %collective-permute-start.10 = (bf16[512,768]{1,0:T(8,128)(2,1)}, bf16[512,768]{1,0:T(8,128)(2,1)}, u32[]{:S(2)}, u32[]{:S(2)}) collective-permute-start(bf16[512,768]{1,0:T(8,128)(2,1)} %convolution_convert_fusion.1), channel_id=1, source_target_pairs={{0,1},{1,0},{2,3},{3,2},{4,5},{5,4},{6,7},{7,6},{8,9},{9,8},{10,11... | collective-permute-start | bytes 2359304 | tf_op jit(solution)/shard_map/ppermute | solution.py:101
  119.8 1.5 copy-start.18
  121.3 5.3 %copy-start.2 = (bf16[1536,768]{1,0:T(8,128)(2,1)S(1)}, bf16[1536,768]{1,0:T(8,128)(2,1)}, u32[]{:S(2)}) copy-start(bf16[1536,768]{1,0:T(8,128)(2,1)} %copy-done.1) | copy-start | bytes 7077892
  122.9 5.0 %copy-start.4 = (bf16[768,768]{1,0:T(8,128)(2,1)S(1)}, bf16[768,768]{1,0:T(8,128)(2,1)}, u32[]{:S(2)}) copy-start(bf16[768,768]{1,0:T(8,128)(2,1)} %copy-done.3) | copy-start | bytes 3538948
  122.9 12.8 %collective-permute-start.11 = (bf16[512,768]{1,0:T(8,128)(2,1)}, bf16[512,768]{1,0:T(8,128)(2,1)S(1)}, u32[]{:S(2)}, u32[]{:S(2)}) collective-permute-start(bf16[512,768]{1,0:T(8,128)(2,1)} %convolution_convert_fusion), channel_id=1, source_target_pairs={{0,1},{1,0},{2,3},{3,2},{4,5},{5,4},{6,7},{7,6},{8,9},{9,8},{10,11... | collective-permute-start | bytes 2359304 | tf_op jit(solution)/shard_map/ppermute | solution.py:101
  127.9 3.2 %copy-start.16 = (bf16[512,768]{1,0:T(8,128)(2,1)}, bf16[512,768]{1,0:T(8,128)(2,1)S(1)}, u32[]{:S(2)}) copy-start(bf16[512,768]{1,0:T(8,128)(2,1)S(1)} %multiply_convert_fusion.1) | copy-start | bytes 2359300
  131.1 4.7 %copy-start.6 = (bf16[768,768]{1,0:T(8,128)(2,1)S(1)}, bf16[768,768]{1,0:T(8,128)(2,1)}, u32[]{:S(2)}) copy-start(bf16[768,768]{1,0:T(8,128)(2,1)} %copy-done.5) | copy-start | bytes 3538948
  131.1 16.8 %all-to-all-start.2 = ((bf16[4,128,768]{2,1,0:T(8,128)(2,1)}), bf16[4,128,768]{2,1,0:T(8,128)(2,1)S(1)}, u32[]{:S(2)}, u32[]{:S(2)}) async-start(bf16[4,128,768]{2,1,0:T(8,128)(2,1)} %bitcast.4), calls=%async_computation.2 | async-start | bytes 1572864 | tf_op jit(solution)/shard_map/all_to_all | solution.py:32
  147.9 14.7 %all-to-all-start.4 = ((bf16[4,128,768]{2,1,0:T(8,128)(2,1)}), bf16[4,128,768]{2,1,0:T(8,128)(2,1)S(1)}, u32[]{:S(2)}, u32[]{:S(2)}) async-start(bf16[4,128,768]{2,1,0:T(8,128)(2,1)} %bitcast.6), calls=%async_computation.4 | async-start | bytes 1572864 | tf_op jit(solution)/shard_map/all_to_all | solution.py:32
  (4 other events, 4.0 us)

commit v2 on v1

--- a/solution.py
+++ b/solution.py
@@ -1,6 +1,10 @@
+import functools
+
 import jax
 import jax.numpy as jnp
 from jax import lax
+from jax.experimental import pallas as pl
+from jax.experimental.pallas import tpu as pltpu
 from jax.sharding import PartitionSpec as P
 
 
@@ -45,6 +49,86 @@
     return out
 
 
+def by_place_kernel(x_ref, *refs):
+    *blocks, out = refs
+    rows = blocks[0].shape[0]
+    for k, block in enumerate(blocks):
+        out[pl.ds(pl.multiple_of((x_ref[0] + k) % X * rows, rows), rows), :] = block[...]
+
+
+def by_place(x, blocks):
+    rows, columns = blocks[0].shape
+    return pl.pallas_call(
+        by_place_kernel,
+        out_shape=jax.ShapeDtypeStruct((X * rows, columns), blocks[0].dtype),
+        in_specs=[pl.BlockSpec(memory_space=pltpu.SMEM)] + [pl.BlockSpec(memory_space=pltpu.VMEM)] * X,
+        out_specs=pl.BlockSpec(memory_space=pltpu.VMEM),
+        cost_estimate=pl.CostEstimate(flops=1 << 28, bytes_accessed=4 * X * rows * columns, transcendentals=0),
+        name="by_place",
+    )(x[None], *blocks)
+
+
+def from_place_kernel(x_ref, a, *outs):
+    rows = outs[0].shape[0]
+    for k, out in enumerate(outs):
+        out[...] = a[pl.ds(pl.multiple_of((x_ref[0] + k) % X * rows, rows), rows), :]
+
+
+def from_place(x, a):
+    shape = (a.shape[0] // X, a.shape[1])
+    return pl.pallas_call(
+        from_place_kernel,
+        out_shape=[jax.ShapeDtypeStruct(shape, a.dtype)] * X,
+        in_specs=[pl.BlockSpec(memory_space=pltpu.SMEM), pl.BlockSpec(memory_space=pltpu.VMEM)],
+        out_specs=[pl.BlockSpec(memory_space=pltpu.VMEM)] * X,
+        cost_estimate=pl.CostEstimate(flops=1 << 28, bytes_accessed=4 * a.size, transcendentals=0),
+        name="from_place",
+    )(x[None], a)
+
+
+TILE = 256
+
+
+def hidden_kernel(half, own, other, u0, u1, u2, u3, scale, out):
+    def write(rows):
+        width = u0.shape[0]
+        pre = jnp.dot(rows[:, :width], u0[...], preferred_element_type=F32)
+        for k, block in enumerate((u1, u2, u3), 1):
+            pre += jnp.dot(rows[:, k * width : (k + 1) * width], block[...], preferred_element_type=F32)
+        out[...] = jnp.square(jnp.maximum(pre * scale[...], 0.0)).astype(out.dtype)
+
+    @pl.when(pl.program_id(0) < half)
+    def _():
+        write(own)
+
+    @pl.when(pl.program_id(0) >= half)
+    def _():
+        write(other)
+
+
+def hidden_of(own, other, up, scale):
+    rows, d = own.shape
+    width, columns = up[0].shape
+    half = rows // TILE
+    whole = pl.BlockSpec((width, columns), lambda i: (0, 0))
+    return pl.pallas_call(
+        functools.partial(hidden_kernel, half),
+        grid=(2 * half,),
+        out_shape=jax.ShapeDtypeStruct((2 * rows, columns), BF16),
+        in_specs=[
+            pl.BlockSpec((TILE, d), lambda i: (jnp.minimum(i, half - 1), 0)),
+            pl.BlockSpec((TILE, d), lambda i: (jnp.maximum(i - half, 0), 0)),
+            *([whole] * ZLO),
+            pl.BlockSpec((1, columns), lambda i: (0, 0)),
+        ],
+        out_specs=pl.BlockSpec((TILE, columns), lambda i: (i, 0)),
+        cost_estimate=pl.CostEstimate(
+            flops=4 * rows * d * columns, bytes_accessed=4 * rows * d + 2 * d * columns + 4 * rows * columns, transcendentals=0
+        ),
+        name="hidden",
+    )(own, other, *up, scale)
+
+
 def body(tokens, norm_gain, up_weight, up_scale, down_weight, down_scale):
     z = lax.axis_index("fs") // Y
     x = lax.axis_index("tp") // 2
@@ -53,8 +137,6 @@
 
     up_own = spread(up_weight.astype(BF16), "fs", ROW_GROUPS)
     down_piece = (down_weight * down_scale).T.astype(BF16)
-    down_two = lax.ppermute(down_piece, PLANE, FROM_TWO)
-
     values = tokens.astype(F32)
     normed = (
         values * lax.rsqrt(jnp.mean(values * values, axis=-1, keepdims=True) + 1e-06) * norm_gain
@@ -66,9 +148,7 @@
         lax.ppermute(normed, "tp", X_TWO),
         lax.ppermute(normed, "tp", X_LAST),
     ]
-    own = jnp.zeros((X * rows, d), BF16)
-    for k, block in enumerate(near):
-        own = lax.dynamic_update_slice(own, block, (rows * ((x + k) % X), 0))
+    own = by_place(x, near)
     other = lax.ppermute(own, "tp", OTHER_CORE)
 
     up = [
@@ -77,37 +157,34 @@
         lax.ppermute(up_own, PLANE, FROM_TWO),
         lax.ppermute(up_own, PLANE, FROM_LAST),
     ]
-    up = lax.optimization_barrier(jnp.concatenate(up, 0))
-
+    down_piece, _ = lax.optimization_barrier((down_piece, up_own))
     down_own = spread(down_piece, "fs", ROW_GROUPS)
-    down_two, down_own = lax.optimization_barrier((down_two, down_own))
-    down_two = spread(down_two, "fs", ROW_GROUPS)
-    down_a = jnp.concatenate([down_own, down_two], 0)
-    down_b = jnp.concatenate(
-        [lax.ppermute(down_own, PLANE, FROM_NEXT), lax.ppermute(down_own, PLANE, FROM_LAST)], 0
-    )
-    down_a, down_b = lax.optimization_barrier(down_a), lax.optimization_barrier(down_b)
-
-    def hidden_of(t):
-        pre = jnp.dot(t, up, preferred_element_type=F32)
-        return jnp.square(jnp.maximum(pre * up_scale, 0.0)).astype(BF16)
-
-    hidden_own, hidden_other = hidden_of(own), hidden_of(other)
-
-    def chunk(down):
+    down_b = jnp.concatenate([lax.ppermute(down_own, PLANE, FROM_NEXT), lax.ppermute(down_own, PLANE, FROM_LAST)], 0)
+    down_b = lax.optimization_barrier(down_b)
+    down_c = lax.ppermute(down_own, PLANE, FROM_TWO)
+
+    hidden = hidden_of(own, other, up, up_scale)
+    hidden_own, hidden_other = hidden[: X * rows], hidden[X * rows :]
+
+    def pair_of(down):
         def terms(hidden):
             return lax.dot_general(hidden, down, (((1,), (1,)), ((), ())), preferred_element_type=F32)
 
         arrived = lax.ppermute(terms(hidden_other).astype(BF16), "tp", OTHER_CORE)
-        pair = (terms(hidden_own) + arrived.astype(F32)).astype(BF16)
+        return (terms(hidden_own) + arrived.astype(F32)).astype(BF16)
+
+    def exchanged(pair):
         arrived = swapped(pair.reshape(X, rows, -1), "tp", X_GROUPS)
         return arrived.astype(F32).sum(axis=0).astype(BF16)
 
-    out_a = chunk(down_a)
-    out_b = chunk(down_b)
-    summed = jnp.concatenate(
-        [out_a[:, :width], out_b[:, :width], out_a[:, width:], out_b[:, width:]], 1
-    )
+    out_a = exchanged(pair_of(down_own))
+    out_b = exchanged(pair_of(down_b))
+    mine, for_next, for_two, for_last = from_place(x, pair_of(down_c))
+    out_c = mine.astype(F32)
+    out_c += lax.ppermute(for_next, "tp", X_LAST).astype(F32)
+    out_c += lax.ppermute(for_two, "tp", X_TWO).astype(F32)
+    out_c += lax.ppermute(for_last, "tp", X_NEXT).astype(F32)
+    summed = jnp.concatenate([out_a, out_b[:, :width], out_c.astype(BF16), out_b[:, width:]], 1)
     return rolled(summed, (ZLO - z) % ZLO, width)
 
 

time: 165 us -> 163 us (0.988)
  the two profiles are of different devices: /device:TPU:1 before, /device:TPU:8 now
where the time goes in v2:
time: 163 us; the launch traced here: 162 us
  starting transfers between devices  83.5 us (51%)
  waiting for transfers between devices  49.2 us (30%)
  Pallas kernels  11.5 us (7%)
  matrix products  10.3 us (6%)
  other arithmetic  3.89 us (2%)
  local copies, waits for them, and re-layouts  2.71 us (2%)
    all_to_all x4, starting transfers between devices, swapped(): lax.all_to_all(blocks, axis, 0, 0, axis_index_groups=groups, tiled=True)  23.4 us
    ppermute x1, starting transfers between devices, body(): lax.ppermute(down_own, PLANE, FROM_NEXT)  10.9 us
    ppermute x1, starting transfers between devices, body(): lax.ppermute(up_own, PLANE, FROM_NEXT)  10.9 us
    ppermute x1, waiting for transfers between devices, body(): lax.ppermute(normed, 'tp', X_NEXT)  10.7 us
    dot_general x6, matrix products, terms(): lax.dot_general(hidden, down, (((1,), (1,)), ((), ())), preferred_element...  10.3 us
    ppermute x1, waiting for transfers between devices, body(): lax.ppermute(up_own, PLANE, FROM_NEXT)  8.23 us
    all_to_all x4, waiting for transfers between devices, swapped(): lax.all_to_all(blocks, axis, 0, 0, axis_index_groups=groups, tiled=True)  7.43 us
    ppermute x1, waiting for transfers between devices, body(): down_c = lax.ppermute(down_own, PLANE, FROM_TWO)  7.25 us
  transfers between devices with their start and end apart: 20, of which 10 were waited for; matrix products, arithmetic and copies ran while one was open for 8% of the time, Pallas kernels for 7%

profile of v2, /device:TPU:8, one launch (start us, length us, event | category | flops | bytes accessed | tf_op | source)
XLA Modules:
  0.0 161.6 jit_solution(14103666862039093641)
XLA Ops:
  1.8 9.2 %all-to-all-start = ((bf16[8,48,768]{2,1,0:T(8,128)(2,1)}), bf16[8,48,768]{2,1,0:T(8,128)(2,1)S(1)}, u32[]{:S(2)}, u32[]{:S(2)}) async-start(bf16[8,48,768]{2,1,0:T(8,128)(2,1)} %broadcast_in_dim.7), calls=%async_computation | async-start | bytes 1179648 | tf_op jit(solution)/shard_map/all_to_all | solution.py:36
  11.9 3.0 %collective-permute-start = (bf16[128,1536]{1,0:T(8,128)(2,1)S(1)}, bf16[128,1536]{1,0:T(8,128)(2,1)S(1)}, u32[]{:S(2)}, u32[]{:S(2)}) collective-permute-start(bf16[128,1536]{1,0:T(8,128)(2,1)S(1)} %maximum_select_fusion.refs_0_), channel_id=1, source_target_pairs={{0,6},{1,7},{2,0},{3,1},{4,2},{5,3},{6,4},{7,5},{8,14},{9,15},{10,... | collective-permute-start | bytes 1179656 | tf_op jit(solution)/shard_map/ppermute | solution.py:147
  14.9 2.7 %collective-permute-start.1 = (bf16[128,1536]{1,0:T(8,128)(2,1)S(1)}, bf16[128,1536]{1,0:T(8,128)(2,1)S(1)}, u32[]{:S(2)}, u32[]{:S(2)}) collective-permute-start(bf16[128,1536]{1,0:T(8,128)(2,1)S(1)} %maximum_select_fusion.refs_0_), channel_id=1, source_target_pairs={{0,4},{1,5},{2,6},{3,7},{4,0},{5,1},{6,2},{7,3},{8,12},{9,13},{10,... | collective-permute-start | bytes 1179656 | tf_op jit(solution)/shard_map/ppermute | solution.py:148
  17.6 2.8 %collective-permute-start.2 = (bf16[128,1536]{1,0:T(8,128)(2,1)S(1)}, bf16[128,1536]{1,0:T(8,128)(2,1)S(1)}, u32[]{:S(2)}, u32[]{:S(2)}) collective-permute-start(bf16[128,1536]{1,0:T(8,128)(2,1)S(1)} %maximum_select_fusion.refs_0_), channel_id=1, source_target_pairs={{0,2},{1,3},{2,4},{3,5},{4,6},{5,7},{6,0},{7,1},{8,10},{9,11},{10,... | collective-permute-start | bytes 1179656 | tf_op jit(solution)/shard_map/ppermute | solution.py:149
  20.4 10.7 %collective-permute-done.refs_1_ = bf16[128,1536]{1,0:T(8,128)(2,1)S(1)} collective-permute-done((bf16[128,1536]{1,0:T(8,128)(2,1)S(1)}, bf16[128,1536]{1,0:T(8,128)(2,1)S(1)}, u32[]{:S(2)}, u32[]{:S(2)}) %collective-permute-start) | collective-permute-done | bytes 393248 | tf_op jit(solution)/shard_map/ppermute | solution.py:147
  31.2 5.6 %collective-permute-done.2.refs_3_ = bf16[128,1536]{1,0:T(8,128)(2,1)S(1)} collective-permute-done((bf16[128,1536]{1,0:T(8,128)(2,1)S(1)}, bf16[128,1536]{1,0:T(8,128)(2,1)S(1)}, u32[]{:S(2)}, u32[]{:S(2)}) %collective-permute-start.2) | collective-permute-done | bytes 393248 | tf_op jit(solution)/shard_map/ppermute | solution.py:149
  37.5 2.6 %by_place.1.own = bf16[512,1536]{1,0:T(8,128)(2,1)} custom-call(s32[1]{0:T(128)} %bitcast.x_ref, bf16[128,1536]{1,0:T(8,128)(2,1)} %copy-done.1, bf16[128,1536]{1,0:T(8,128)(2,1)} %copy-done.3, bf16[128,1536]{1,0:T(8,128)(2,1)} %copy-done.4, bf16[128,1536]{1,0:T(8,128)(2,1)} %copy-done.5), custom_call_target="tpu_custom_call" | custom-call | flops 268435456 | bytes 3145728 | tf_op jit(solution)/shard_map/by_place/pallas_call | solution.py:61
  40.2 1.9 %collective-permute-start.3 = (bf16[512,1536]{1,0:T(8,128)(2,1)}, bf16[512,1536]{1,0:T(8,128)(2,1)}, u32[]{:S(2)}, u32[]{:S(2)}) collective-permute-start(bf16[512,1536]{1,0:T(8,128)(2,1)} %by_place.1.own), channel_id=1, source_target_pairs={{0,1},{1,0},{2,3},{3,2},{4,5},{5,4},{6,7},{7,6},{8,9},{9,8},{10,11... | collective-permute-start | bytes 4718600 | tf_op jit(solution)/shard_map/ppermute | solution.py:152
  43.1 7.2 %all-to-all-start.1 = ((bf16[8,48,768]{2,1,0:T(8,128)(2,1)}), bf16[8,48,768]{2,1,0:T(8,128)(2,1)S(1)}, u32[]{:S(2)}, u32[]{:S(2)}) async-start(bf16[8,48,768]{2,1,0:T(8,128)(2,1)} %broadcast_in_dim.8), calls=%async_computation.1 | async-start | bytes 1179648 | tf_op jit(solution)/shard_map/all_to_all | solution.py:36
  50.4 10.9 %collective-permute-start.4 = (bf16[384,768]{1,0:T(8,128)(2,1)S(1)}, bf16[384,768]{1,0:T(8,128)(2,1)S(1)}, u32[]{:S(2)}, u32[]{:S(2)}) collective-permute-start(bf16[384,768]{1,0:T(8,128)(2,1)S(1)} %bitcast.14), channel_id=1, source_target_pairs={{0,448},{8,456},{16,464},{24,472},{32,480},{40,488},{48,496},{56,5... | collective-permute-start | bytes 1769480 | tf_op jit(solution)/shard_map/ppermute | solution.py:156
  61.3 1.9 %collective-permute-start.5 = (bf16[384,768]{1,0:T(8,128)(2,1)S(1)}, bf16[384,768]{1,0:T(8,128)(2,1)S(1)}, u32[]{:S(2)}, u32[]{:S(2)}) collective-permute-start(bf16[384,768]{1,0:T(8,128)(2,1)S(1)} %bitcast.15), channel_id=1, source_target_pairs={{0,128},{8,136},{16,144},{24,152},{32,160},{40,168},{48,176},{56,1... | collective-permute-start | bytes 1769480 | tf_op jit(solution)/shard_map/ppermute | solution.py:157
  63.2 3.9 %collective-permute-start.6 = (bf16[384,768]{1,0:T(8,128)(2,1)S(1)}, bf16[384,768]{1,0:T(8,128)(2,1)}, u32[]{:S(2)}, u32[]{:S(2)}) collective-permute-start(bf16[384,768]{1,0:T(8,128)(2,1)S(1)} %bitcast.16), channel_id=1, source_target_pairs={{0,64},{8,72},{16,80},{24,88},{32,96},{40,104},{48,112},{56,120},{... | collective-permute-start | bytes 1769480 | tf_op jit(solution)/shard_map/ppermute | solution.py:158
  68.5 10.9 %collective-permute-start.7 = (bf16[384,768]{1,0:T(8,128)(2,1)S(1)}, bf16[384,768]{1,0:T(8,128)(2,1)S(1)}, u32[]{:S(2)}, u32[]{:S(2)}) collective-permute-start(bf16[384,768]{1,0:T(8,128)(2,1)S(1)} %bitcast.18), channel_id=1, source_target_pairs={{0,448},{8,456},{16,464},{24,472},{32,480},{40,488},{48,496},{56,5... | collective-permute-start | bytes 1769480 | tf_op jit(solution)/shard_map/ppermute | solution.py:162
  79.4 8.2 %collective-permute-done.4.u1 = bf16[384,768]{1,0:T(8,128)(2,1)S(1)} collective-permute-done((bf16[384,768]{1,0:T(8,128)(2,1)S(1)}, bf16[384,768]{1,0:T(8,128)(2,1)S(1)}, u32[]{:S(2)}, u32[]{:S(2)}) %collective-permute-start.4) | collective-permute-done | bytes 589856 | tf_op jit(solution)/shard_map/ppermute | solution.py:156
  87.6 1.9 %collective-permute-start.8 = (bf16[384,768]{1,0:T(8,128)(2,1)S(1)}, bf16[384,768]{1,0:T(8,128)(2,1)S(1)}, u32[]{:S(2)}, u32[]{:S(2)}) collective-permute-start(bf16[384,768]{1,0:T(8,128)(2,1)S(1)} %bitcast.19), channel_id=1, source_target_pairs={{0,64},{8,72},{16,80},{24,88},{32,96},{40,104},{48,112},{56,120},{... | collective-permute-start | bytes 1769480 | tf_op jit(solution)/shard_map/ppermute | solution.py:162
  89.6 3.5 %collective-permute-done.6.u3 = bf16[384,768]{1,0:T(8,128)(2,1)} collective-permute-done((bf16[384,768]{1,0:T(8,128)(2,1)S(1)}, bf16[384,768]{1,0:T(8,128)(2,1)}, u32[]{:S(2)}, u32[]{:S(2)}) %collective-permute-start.6) | collective-permute-done | bytes 589856 | tf_op jit(solution)/shard_map/ppermute | solution.py:158
  93.0 7.1 %hidden.1 = bf16[1024,768]{1,0:T(8,128)(2,1)} custom-call(bf16[512,1536]{1,0:T(8,128)(2,1)} %by_place.1.own, bf16[512,1536]{1,0:T(8,128)(2,1)} %collective-permute-done.3.other, bf16[384,768]{1,0:T(8,128)(2,1)} %bitcast.17, bf16[384,768]{1,0:T(8,128)(2,1)} %copy-done.11, bf16[384,768]{1,0:T(8,128)(2,1)} %copy-done.12, ...), custom_call_target="tpu_custom_call" | custom-call | flops 2415919104 | bytes 7077888 | tf_op jit(solution)/shard_map/hidden/pallas_call | solution.py:114
  100.2 2.0 %collective-permute-start.11 = (bf16[384,768]{1,0:T(8,128)(2,1)S(1)}, bf16[384,768]{1,0:T(8,128)(2,1)S(1)}, u32[]{:S(2)}, u32[]{:S(2)}) collective-permute-start(bf16[384,768]{1,0:T(8,128)(2,1)S(1)} %bitcast.20), channel_id=1, source_target_pairs={{0,128},{8,136},{16,144},{24,152},{32,160},{40,168},{48,176},{56,1... | collective-permute-start | bytes 1769480 | tf_op jit(solution)/shard_map/ppermute | solution.py:164
  102.2 3.2 %collective-permute-done.8 = bf16[384,768]{1,0:T(8,128)(2,1)S(1)} collective-permute-done((bf16[384,768]{1,0:T(8,128)(2,1)S(1)}, bf16[384,768]{1,0:T(8,128)(2,1)S(1)}, u32[]{:S(2)}, u32[]{:S(2)}) %collective-permute-start.8) | collective-permute-done | bytes 589856 | tf_op jit(solution)/shard_map/ppermute | solution.py:162
  107.3 1.9 %collective-permute-start.9 = (bf16[512,768]{1,0:T(8,128)(2,1)}, bf16[512,768]{1,0:T(8,128)(2,1)S(1)}, u32[]{:S(2)}, u32[]{:S(2)}) collective-permute-start(bf16[512,768]{1,0:T(8,128)(2,1)} %convolution_convert_fusion), channel_id=1, source_target_pairs={{0,1},{1,0},{2,3},{3,2},{4,5},{5,4},{6,7},{7,6},{8,9},{9,8},{10,11... | collective-permute-start | bytes 2359304 | tf_op jit(solution)/shard_map/ppermute | solution.py:173
  109.8 2.4 %collective-permute-start.10 = (bf16[512,384]{1,0:T(8,128)(2,1)S(1)}, bf16[512,384]{1,0:T(8,128)(2,1)S(1)}, u32[]{:S(2)}, u32[]{:S(2)}) collective-permute-start(bf16[512,384]{1,0:T(8,128)(2,1)S(1)} %convolution_convert_fusion.2), channel_id=1, source_target_pairs={{0,1},{1,0},{2,3},{3,2},{4,5},{5,4},{6,7},{7,6},{8,9},{9,8},{10,11... | collective-permute-start | bytes 1179656 | tf_op jit(solution)/shard_map/ppermute | solution.py:173
  112.2 7.2 %collective-permute-done.11 = bf16[384,768]{1,0:T(8,128)(2,1)S(1)} collective-permute-done((bf16[384,768]{1,0:T(8,128)(2,1)S(1)}, bf16[384,768]{1,0:T(8,128)(2,1)S(1)}, u32[]{:S(2)}, u32[]{:S(2)}) %collective-permute-start.11) | collective-permute-done | bytes 589856 | tf_op jit(solution)/shard_map/ppermute | solution.py:164
  120.8 1.9 %collective-permute-start.12 = (bf16[512,384]{1,0:T(8,128)(2,1)}, bf16[512,384]{1,0:T(8,128)(2,1)S(1)}, u32[]{:S(2)}, u32[]{:S(2)}) collective-permute-start(bf16[512,384]{1,0:T(8,128)(2,1)} %convolution_convert_fusion.1), channel_id=1, source_target_pairs={{0,1},{1,0},{2,3},{3,2},{4,5},{5,4},{6,7},{7,6},{8,9},{9,8},{10,11... | collective-permute-start | bytes 1179656 | tf_op jit(solution)/shard_map/ppermute | solution.py:173
  124.1 3.5 %all-to-all-start.3 = ((bf16[4,128,384]{2,1,0:T(8,128)(2,1)}), bf16[4,128,384]{2,1,0:T(8,128)(2,1)S(1)}, u32[]{:S(2)}, u32[]{:S(2)}) async-start(bf16[4,128,384]{2,1,0:T(8,128)(2,1)} %bitcast.6), calls=%async_computation.3 | async-start | bytes 786432 | tf_op jit(solution)/shard_map/all_to_all | solution.py:36
  127.6 2.9 %add_convert_fusion = bf16[512,768]{1,0:T(8,128)(2,1)} fusion(bf16[512,768]{1,0:T(8,128)(2,1)S(1)} %collective-permute-done.9, bf16[768,768]{1,0:T(8,128)(2,1)S(1)} %pad_maximum_fusion, bf16[1024,768]{1,0:T(8,128)(2,1)} %hidden.1), kind=kOutput, calls=%fused_computation | convolution fusion | flops 605159424 | bytes 3538944 | tf_op jit(solution)/shard_map/dot_general | solution.py:171
  130.4 6.1 %all-to-all-done.3 = bf16[4,128,384]{2,1,0:T(8,128)(2,1)S(1)} async-done(((bf16[4,128,384]{2,1,0:T(8,128)(2,1)}), bf16[4,128,384]{2,1,0:T(8,128)(2,1)S(1)}, u32[]{:S(2)}, u32[]{:S(2)}) %all-to-all-start.3) | async-done | bytes 393248 | tf_op jit(solution)/shard_map/all_to_all | solution.py:36
  136.5 3.5 %all-to-all-start.2 = ((bf16[4,128,768]{2,1,0:T(8,128)(2,1)}), bf16[4,128,768]{2,1,0:T(8,128)(2,1)S(1)}, u32[]{:S(2)}, u32[]{:S(2)}) async-start(bf16[4,128,768]{2,1,0:T(8,128)(2,1)} %bitcast.5), calls=%async_computation.2 | async-start | bytes 1572864 | tf_op jit(solution)/shard_map/all_to_all | solution.py:36
  140.1 2.5 %fusion.1.a = bf16[512,384]{1,0:T(8,128)(2,1)} fusion(bf16[384,768]{1,0:T(8,128)(2,1)S(1)} %copy-done.10, bf16[512,384]{1,0:T(8,128)(2,1)S(1)} %collective-permute-done.12, bf16[1024,768]{1,0:T(8,128)(2,1)} %hidden.1), kind=kOutput, calls=%fused_computation.5 | convolution fusion | flops 302579712 | bytes 2162688 | tf_op jit(solution)/shard_map/dot_general | solution.py:171
  144.3 3.9 %collective-permute-start.13 = (bf16[128,384]{1,0:T(8,128)(2,1)}, bf16[128,384]{1,0:T(8,128)(2,1)S(1)}, u32[]{:S(2)}, u32[]{:S(2)}) collective-permute-start(bf16[128,384]{1,0:T(8,128)(2,1)} %get-tuple-element.12), channel_id=1, source_target_pairs={{0,2},{1,3},{2,4},{3,5},{4,6},{5,7},{6,0},{7,1},{8,10},{9,11},{10,... | collective-permute-start | bytes 294920 | tf_op jit(solution)/shard_map/ppermute | solution.py:184
  148.2 4.6 %collective-permute-start.14 = (bf16[128,384]{1,0:T(8,128)(2,1)}, bf16[128,384]{1,0:T(8,128)(2,1)S(1)}, u32[]{:S(2)}, u32[]{:S(2)}) collective-permute-start(bf16[128,384]{1,0:T(8,128)(2,1)} %get-tuple-element.13), channel_id=1, source_target_pairs={{0,4},{1,5},{2,6},{3,7},{4,0},{5,1},{6,2},{7,3},{8,12},{9,13},{10,... | collective-permute-start | bytes 294920 | tf_op jit(solution)/shard_map/ppermute | solution.py:185
  152.8 3.4 %collective-permute-start.15 = (bf16[128,384]{1,0:T(8,128)(2,1)}, bf16[128,384]{1,0:T(8,128)(2,1)S(1)}, u32[]{:S(2)}, u32[]{:S(2)}) collective-permute-start(bf16[128,384]{1,0:T(8,128)(2,1)} %get-tuple-element.14), channel_id=1, source_target_pairs={{0,6},{1,7},{2,0},{3,1},{4,2},{5,3},{6,4},{7,5},{8,14},{9,15},{10,... | collective-permute-start | bytes 294920 | tf_op jit(solution)/shard_map/ppermute | solution.py:186
  156.6 2.9 %collective-permute-done.15 = bf16[128,384]{1,0:T(8,128)(2,1)S(1)} collective-permute-done((bf16[128,384]{1,0:T(8,128)(2,1)}, bf16[128,384]{1,0:T(8,128)(2,1)S(1)}, u32[]{:S(2)}, u32[]{:S(2)}) %collective-permute-start.15) | collective-permute-done | bytes 98336 | tf_op jit(solution)/shard_map/ppermute | solution.py:186
  (62 shorter events, 15.0 us)
Async XLA Ops:
  0.0 11.1 %copy-start = (bf16[128,1536]{1,0:T(8,128)(2,1)S(1)}, bf16[128,1536]{1,0:T(8,128)(2,1)}, u32[]{:S(2)}) copy-start(bf16[128,1536]{1,0:T(8,128)(2,1)} %param.6) | copy-start | bytes 1179652
  0.0 11.2 %copy-start.7 = (f32[1536]{0:T(1024)S(1)}, f32[1536]{0:T(1024)}, u32[]{:S(2)}) copy-start(f32[1536]{0:T(1024)} %param.7) | copy-start | bytes 18436
  1.8 40.4 %all-to-all-start = ((bf16[8,48,768]{2,1,0:T(8,128)(2,1)}), bf16[8,48,768]{2,1,0:T(8,128)(2,1)S(1)}, u32[]{:S(2)}, u32[]{:S(2)}) async-start(bf16[8,48,768]{2,1,0:T(8,128)(2,1)} %broadcast_in_dim.7), calls=%async_computation | async-start | bytes 1179648 | tf_op jit(solution)/shard_map/all_to_all | solution.py:36
  11.9 24.8 %copy-start.1 = (bf16[128,1536]{1,0:T(8,128)(2,1)}, bf16[128,1536]{1,0:T(8,128)(2,1)S(1)}, u32[]{:S(2)}) copy-start(bf16[128,1536]{1,0:T(8,128)(2,1)S(1)} %maximum_select_fusion.refs_0_) | copy-start | bytes 1179652
  11.9 19.2 %collective-permute-start = (bf16[128,1536]{1,0:T(8,128)(2,1)S(1)}, bf16[128,1536]{1,0:T(8,128)(2,1)S(1)}, u32[]{:S(2)}, u32[]{:S(2)}) collective-permute-start(bf16[128,1536]{1,0:T(8,128)(2,1)S(1)} %maximum_select_fusion.refs_0_), channel_id=1, source_target_pairs={{0,6},{1,7},{2,0},{3,1},{4,2},{5,3},{6,4},{7,5},{8,14},{9,15},{10,... | collective-permute-start | bytes 1179656 | tf_op jit(solution)/shard_map/ppermute | solution.py:147
  14.9 16.3 %collective-permute-start.1 = (bf16[128,1536]{1,0:T(8,128)(2,1)S(1)}, bf16[128,1536]{1,0:T(8,128)(2,1)S(1)}, u32[]{:S(2)}, u32[]{:S(2)}) collective-permute-start(bf16[128,1536]{1,0:T(8,128)(2,1)S(1)} %maximum_select_fusion.refs_0_), channel_id=1, source_target_pairs={{0,4},{1,5},{2,6},{3,7},{4,0},{5,1},{6,2},{7,3},{8,12},{9,13},{10,... | collective-permute-start | bytes 1179656 | tf_op jit(solution)/shard_map/ppermute | solution.py:148
  17.6 19.1 %collective-permute-start.2 = (bf16[128,1536]{1,0:T(8,128)(2,1)S(1)}, bf16[128,1536]{1,0:T(8,128)(2,1)S(1)}, u32[]{:S(2)}, u32[]{:S(2)}) collective-permute-start(bf16[128,1536]{1,0:T(8,128)(2,1)S(1)} %maximum_select_fusion.refs_0_), channel_id=1, source_target_pairs={{0,2},{1,3},{2,4},{3,5},{4,6},{5,7},{6,0},{7,1},{8,10},{9,11},{10,... | collective-permute-start | bytes 1179656 | tf_op jit(solution)/shard_map/ppermute | solution.py:149
  31.2 5.6 %copy-start.3 = (bf16[128,1536]{1,0:T(8,128)(2,1)}, bf16[128,1536]{1,0:T(8,128)(2,1)S(1)}, u32[]{:S(2)}) copy-start(bf16[128,1536]{1,0:T(8,128)(2,1)S(1)} %collective-permute-done.refs_1_) | copy-start | bytes 1179652
  31.2 5.6 %copy-start.4 = (bf16[128,1536]{1,0:T(8,128)(2,1)}, bf16[128,1536]{1,0:T(8,128)(2,1)S(1)}, u32[]{:S(2)}) copy-start(bf16[128,1536]{1,0:T(8,128)(2,1)S(1)} %collective-permute-done.1.refs_2_) | copy-start | bytes 1179652
  37.5 4.6 %copy-start.6 = (f32[768,48]{0,1:T(8,128)S(1)}, f32[768,48]{0,1:T(8,128)}, u32[]{:S(2)}) copy-start(f32[768,48]{0,1:T(8,128)} %param.10) | copy-start | bytes 442372
  37.5 4.6 %copy-start.8 = (f32[1,48]{1,0:T(1,128)S(1)}, f32[1,48]{1,0:T(1,128)}, u32[]{:S(2)}) copy-start(f32[1,48]{1,0:T(1,128)} %param.11) | copy-start | bytes 580
  40.2 52.9 %collective-permute-start.3 = (bf16[512,1536]{1,0:T(8,128)(2,1)}, bf16[512,1536]{1,0:T(8,128)(2,1)}, u32[]{:S(2)}, u32[]{:S(2)}) collective-permute-start(bf16[512,1536]{1,0:T(8,128)(2,1)} %by_place.1.own), channel_id=1, source_target_pairs={{0,1},{1,0},{2,3},{3,2},{4,5},{5,4},{6,7},{7,6},{8,9},{9,8},{10,11... | collective-permute-start | bytes 4718600 | tf_op jit(solution)/shard_map/ppermute | solution.py:152
  42.2 50.8 %copy-start.2 = (bf16[8,48,768]{2,1,0:T(8,128)(2,1)}, bf16[8,48,768]{2,1,0:T(8,128)(2,1)S(1)}, u32[]{:S(2)}) copy-start(bf16[8,48,768]{2,1,0:T(8,128)(2,1)S(1)} %all-to-all-done) | copy-start | bytes 1769476
  43.1 25.3 %all-to-all-start.1 = ((bf16[8,48,768]{2,1,0:T(8,128)(2,1)}), bf16[8,48,768]{2,1,0:T(8,128)(2,1)S(1)}, u32[]{:S(2)}, u32[]{:S(2)}) async-start(bf16[8,48,768]{2,1,0:T(8,128)(2,1)} %broadcast_in_dim.8), calls=%async_computation.1 | async-start | bytes 1179648 | tf_op jit(solution)/shard_map/all_to_all | solution.py:36
  50.4 37.3 %collective-permute-start.4 = (bf16[384,768]{1,0:T(8,128)(2,1)S(1)}, bf16[384,768]{1,0:T(8,128)(2,1)S(1)}, u32[]{:S(2)}, u32[]{:S(2)}) collective-permute-start(bf16[384,768]{1,0:T(8,128)(2,1)S(1)} %bitcast.14), channel_id=1, source_target_pairs={{0,448},{8,456},{16,464},{24,472},{32,480},{40,488},{48,496},{56,5... | collective-permute-start | bytes 1769480 | tf_op jit(solution)/shard_map/ppermute | solution.py:156
  61.3 28.3 %collective-permute-start.5 = (bf16[384,768]{1,0:T(8,128)(2,1)S(1)}, bf16[384,768]{1,0:T(8,128)(2,1)S(1)}, u32[]{:S(2)}, u32[]{:S(2)}) collective-permute-start(bf16[384,768]{1,0:T(8,128)(2,1)S(1)} %bitcast.15), channel_id=1, source_target_pairs={{0,128},{8,136},{16,144},{24,152},{32,160},{40,168},{48,176},{56,1... | collective-permute-start | bytes 1769480 | tf_op jit(solution)/shard_map/ppermute | solution.py:157
  63.2 29.8 %collective-permute-start.6 = (bf16[384,768]{1,0:T(8,128)(2,1)S(1)}, bf16[384,768]{1,0:T(8,128)(2,1)}, u32[]{:S(2)}, u32[]{:S(2)}) collective-permute-start(bf16[384,768]{1,0:T(8,128)(2,1)S(1)} %bitcast.16), channel_id=1, source_target_pairs={{0,64},{8,72},{16,80},{24,88},{32,96},{40,104},{48,112},{56,120},{... | collective-permute-start | bytes 1769480 | tf_op jit(solution)/shard_map/ppermute | solution.py:158
  68.5 33.8 %collective-permute-start.7 = (bf16[384,768]{1,0:T(8,128)(2,1)S(1)}, bf16[384,768]{1,0:T(8,128)(2,1)S(1)}, u32[]{:S(2)}, u32[]{:S(2)}) collective-permute-start(bf16[384,768]{1,0:T(8,128)(2,1)S(1)} %bitcast.18), channel_id=1, source_target_pairs={{0,448},{8,456},{16,464},{24,472},{32,480},{40,488},{48,496},{56,5... | collective-permute-start | bytes 1769480 | tf_op jit(solution)/shard_map/ppermute | solution.py:162
  87.6 5.4 %copy-start.11 = (bf16[384,768]{1,0:T(8,128)(2,1)}, bf16[384,768]{1,0:T(8,128)(2,1)S(1)}, u32[]{:S(2)}) copy-start(bf16[384,768]{1,0:T(8,128)(2,1)S(1)} %collective-permute-done.4.u1) | copy-start | bytes 1769476
  87.6 17.8 %collective-permute-start.8 = (bf16[384,768]{1,0:T(8,128)(2,1)S(1)}, bf16[384,768]{1,0:T(8,128)(2,1)S(1)}, u32[]{:S(2)}, u32[]{:S(2)}) collective-permute-start(bf16[384,768]{1,0:T(8,128)(2,1)S(1)} %bitcast.19), channel_id=1, source_target_pairs={{0,64},{8,72},{16,80},{24,88},{32,96},{40,104},{48,112},{56,120},{... | collective-permute-start | bytes 1769480 | tf_op jit(solution)/shard_map/ppermute | solution.py:162
  100.2 5.4 %copy-start.13 = (bf16[1024,768]{1,0:T(8,128)(2,1)S(1)}, bf16[1024,768]{1,0:T(8,128)(2,1)}, u32[]{:S(2)}) copy-start(bf16[1024,768]{1,0:T(8,128)(2,1)} %hidden.1) | copy-start | bytes 4718596
  100.2 19.3 %collective-permute-start.11 = (bf16[384,768]{1,0:T(8,128)(2,1)S(1)}, bf16[384,768]{1,0:T(8,128)(2,1)S(1)}, u32[]{:S(2)}, u32[]{:S(2)}) collective-permute-start(bf16[384,768]{1,0:T(8,128)(2,1)S(1)} %bitcast.20), channel_id=1, source_target_pairs={{0,128},{8,136},{16,144},{24,152},{32,160},{40,168},{48,176},{56,1... | collective-permute-start | bytes 1769480 | tf_op jit(solution)/shard_map/ppermute | solution.py:164
  107.3 20.3 %collective-permute-start.9 = (bf16[512,768]{1,0:T(8,128)(2,1)}, bf16[512,768]{1,0:T(8,128)(2,1)S(1)}, u32[]{:S(2)}, u32[]{:S(2)}) collective-permute-start(bf16[512,768]{1,0:T(8,128)(2,1)} %convolution_convert_fusion), channel_id=1, source_target_pairs={{0,1},{1,0},{2,3},{3,2},{4,5},{5,4},{6,7},{7,6},{8,9},{9,8},{10,11... | collective-permute-start | bytes 2359304 | tf_op jit(solution)/shard_map/ppermute | solution.py:173
  109.8 12.9 %collective-permute-start.10 = (bf16[512,384]{1,0:T(8,128)(2,1)S(1)}, bf16[512,384]{1,0:T(8,128)(2,1)S(1)}, u32[]{:S(2)}, u32[]{:S(2)}) collective-permute-start(bf16[512,384]{1,0:T(8,128)(2,1)S(1)} %convolution_convert_fusion.2), channel_id=1, source_target_pairs={{0,1},{1,0},{2,3},{3,2},{4,5},{5,4},{6,7},{7,6},{8,9},{9,8},{10,11... | collective-permute-start | bytes 1179656 | tf_op jit(solution)/shard_map/ppermute | solution.py:173
  119.5 4.6 %copy-start.9 = (bf16[384,768]{1,0:T(8,128)(2,1)}, bf16[384,768]{1,0:T(8,128)(2,1)S(1)}, u32[]{:S(2)}) copy-start(bf16[384,768]{1,0:T(8,128)(2,1)S(1)} %collective-permute-done.11) | copy-start | bytes 1769476
  120.8 19.2 %collective-permute-start.12 = (bf16[512,384]{1,0:T(8,128)(2,1)}, bf16[512,384]{1,0:T(8,128)(2,1)S(1)}, u32[]{:S(2)}, u32[]{:S(2)}) collective-permute-start(bf16[512,384]{1,0:T(8,128)(2,1)} %convolution_convert_fusion.1), channel_id=1, source_target_pairs={{0,1},{1,0},{2,3},{3,2},{4,5},{5,4},{6,7},{7,6},{8,9},{9,8},{10,11... | collective-permute-start | bytes 1179656 | tf_op jit(solution)/shard_map/ppermute | solution.py:173
  124.1 12.5 %all-to-all-start.3 = ((bf16[4,128,384]{2,1,0:T(8,128)(2,1)}), bf16[4,128,384]{2,1,0:T(8,128)(2,1)S(1)}, u32[]{:S(2)}, u32[]{:S(2)}) async-start(bf16[4,128,384]{2,1,0:T(8,128)(2,1)} %bitcast.6), calls=%async_computation.3 | async-start | bytes 786432 | tf_op jit(solution)/shard_map/all_to_all | solution.py:36
  130.4 9.6 %copy-start.10 = (bf16[384,768]{1,0:T(8,128)(2,1)S(1)}, bf16[384,768]{1,0:T(8,128)(2,1)}, u32[]{:S(2)}) copy-start(bf16[384,768]{1,0:T(8,128)(2,1)} %copy-done.9) | copy-start | bytes 1769476
  136.5 23.9 %all-to-all-start.2 = ((bf16[4,128,768]{2,1,0:T(8,128)(2,1)}), bf16[4,128,768]{2,1,0:T(8,128)(2,1)S(1)}, u32[]{:S(2)}, u32[]{:S(2)}) async-start(bf16[4,128,768]{2,1,0:T(8,128)(2,1)} %bitcast.5), calls=%async_computation.2 | async-start | bytes 1572864 | tf_op jit(solution)/shard_map/all_to_all | solution.py:36
  144.3 11.9 %collective-permute-start.13 = (bf16[128,384]{1,0:T(8,128)(2,1)}, bf16[128,384]{1,0:T(8,128)(2,1)S(1)}, u32[]{:S(2)}, u32[]{:S(2)}) collective-permute-start(bf16[128,384]{1,0:T(8,128)(2,1)} %get-tuple-element.12), channel_id=1, source_target_pairs={{0,2},{1,3},{2,4},{3,5},{4,6},{5,7},{6,0},{7,1},{8,10},{9,11},{10,... | collective-permute-start | bytes 294920 | tf_op jit(solution)/shard_map/ppermute | solution.py:184
  148.2 8.4 %collective-permute-start.14 = (bf16[128,384]{1,0:T(8,128)(2,1)}, bf16[128,384]{1,0:T(8,128)(2,1)S(1)}, u32[]{:S(2)}, u32[]{:S(2)}) collective-permute-start(bf16[128,384]{1,0:T(8,128)(2,1)} %get-tuple-element.13), channel_id=1, source_target_pairs={{0,4},{1,5},{2,6},{3,7},{4,0},{5,1},{6,2},{7,3},{8,12},{9,13},{10,... | collective-permute-start | bytes 294920 | tf_op jit(solution)/shard_map/ppermute | solution.py:185
  152.8 6.7 %collective-permute-start.15 = (bf16[128,384]{1,0:T(8,128)(2,1)}, bf16[128,384]{1,0:T(8,128)(2,1)S(1)}, u32[]{:S(2)}, u32[]{:S(2)}) collective-permute-start(bf16[128,384]{1,0:T(8,128)(2,1)} %get-tuple-element.14), channel_id=1, source_target_pairs={{0,6},{1,7},{2,0},{3,1},{4,2},{5,3},{6,4},{7,5},{8,14},{9,15},{10,... | collective-permute-start | bytes 294920 | tf_op jit(solution)/shard_map/ppermute | solution.py:186
  (2 other events, 4.2 us)

commit v3 on v2

--- a/solution.py
+++ b/solution.py
@@ -64,64 +64,59 @@
         in_specs=[pl.BlockSpec(memory_space=pltpu.SMEM)] + [pl.BlockSpec(memory_space=pltpu.VMEM)] * X,
         out_specs=pl.BlockSpec(memory_space=pltpu.VMEM),
         cost_estimate=pl.CostEstimate(flops=1 << 28, bytes_accessed=4 * X * rows * columns, transcendentals=0),
+        compiler_params=pltpu.CompilerParams(vmem_limit_bytes=8 << 20),
         name="by_place",
     )(x[None], *blocks)
-
-
-def from_place_kernel(x_ref, a, *outs):
-    rows = outs[0].shape[0]
-    for k, out in enumerate(outs):
-        out[...] = a[pl.ds(pl.multiple_of((x_ref[0] + k) % X * rows, rows), rows), :]
-
-
-def from_place(x, a):
-    shape = (a.shape[0] // X, a.shape[1])
-    return pl.pallas_call(
-        from_place_kernel,
-        out_shape=[jax.ShapeDtypeStruct(shape, a.dtype)] * X,
-        in_specs=[pl.BlockSpec(memory_space=pltpu.SMEM), pl.BlockSpec(memory_space=pltpu.VMEM)],
-        out_specs=[pl.BlockSpec(memory_space=pltpu.VMEM)] * X,
-        cost_estimate=pl.CostEstimate(flops=1 << 28, bytes_accessed=4 * a.size, transcendentals=0),
-        name="from_place",
-    )(x[None], a)
 
 
 TILE = 256
 
 
-def hidden_kernel(half, own, other, u0, u1, u2, u3, scale, out):
+def hidden_kernel(half, own, other, u0, u1, u2, u3, scale, out, up, sems):
+    step = pl.program_id(0)
+
+    @pl.when(step == 0)
+    def _():
+        width = u0.shape[0]
+        copies = [
+            pltpu.make_async_copy(block, up.at[pl.ds(k * width, width)], sems.at[k])
+            for k, block in enumerate((u0, u1, u2, u3))
+        ]
+        for copy in copies:
+            copy.start()
+        for copy in copies:
+            copy.wait()
+
     def write(rows):
-        width = u0.shape[0]
-        pre = jnp.dot(rows[:, :width], u0[...], preferred_element_type=F32)
-        for k, block in enumerate((u1, u2, u3), 1):
-            pre += jnp.dot(rows[:, k * width : (k + 1) * width], block[...], preferred_element_type=F32)
+        pre = jnp.dot(rows[...], up[...], preferred_element_type=F32)
         out[...] = jnp.square(jnp.maximum(pre * scale[...], 0.0)).astype(out.dtype)
 
-    @pl.when(pl.program_id(0) < half)
+    @pl.when(step < half)
+    def _():
+        write(other)
+
+    @pl.when(step >= half)
     def _():
         write(own)
-
-    @pl.when(pl.program_id(0) >= half)
-    def _():
-        write(other)
 
 
 def hidden_of(own, other, up, scale):
     rows, d = own.shape
-    width, columns = up[0].shape
+    _, columns = up[0].shape
     half = rows // TILE
-    whole = pl.BlockSpec((width, columns), lambda i: (0, 0))
     return pl.pallas_call(
         functools.partial(hidden_kernel, half),
         grid=(2 * half,),
         out_shape=jax.ShapeDtypeStruct((2 * rows, columns), BF16),
         in_specs=[
+            pl.BlockSpec((TILE, d), lambda i: (jnp.maximum(i - half, 0), 0)),
             pl.BlockSpec((TILE, d), lambda i: (jnp.minimum(i, half - 1), 0)),
-            pl.BlockSpec((TILE, d), lambda i: (jnp.maximum(i - half, 0), 0)),
-            *([whole] * ZLO),
+            *([pl.BlockSpec(memory_space=pl.ANY)] * ZLO),
             pl.BlockSpec((1, columns), lambda i: (0, 0)),
         ],
         out_specs=pl.BlockSpec((TILE, columns), lambda i: (i, 0)),
+        scratch_shapes=[pltpu.VMEM((d, columns), BF16), pltpu.SemaphoreType.DMA((ZLO,))],
+        compiler_params=pltpu.CompilerParams(vmem_limit_bytes=16 << 20),
         cost_estimate=pl.CostEstimate(
             flops=4 * rows * d * columns, bytes_accessed=4 * rows * d + 2 * d * columns + 4 * rows * columns, transcendentals=0
         ),
@@ -137,6 +132,8 @@
 
     up_own = spread(up_weight.astype(BF16), "fs", ROW_GROUPS)
     down_piece = (down_weight * down_scale).T.astype(BF16)
+    down_two = lax.ppermute(down_piece, PLANE, FROM_TWO)
+
     values = tokens.astype(F32)
     normed = (
         values * lax.rsqrt(jnp.mean(values * values, axis=-1, keepdims=True) + 1e-06) * norm_gain
@@ -157,34 +154,30 @@
         lax.ppermute(up_own, PLANE, FROM_TWO),
         lax.ppermute(up_own, PLANE, FROM_LAST),
     ]
-    down_piece, _ = lax.optimization_barrier((down_piece, up_own))
     down_own = spread(down_piece, "fs", ROW_GROUPS)
+    down_two, down_own = lax.optimization_barrier((down_two, down_own))
+    down_two = spread(down_two, "fs", ROW_GROUPS)
+    down_a = jnp.concatenate([down_own, down_two], 0)
     down_b = jnp.concatenate([lax.ppermute(down_own, PLANE, FROM_NEXT), lax.ppermute(down_own, PLANE, FROM_LAST)], 0)
-    down_b = lax.optimization_barrier(down_b)
-    down_c = lax.ppermute(down_own, PLANE, FROM_TWO)
+    down_a, down_b = lax.optimization_barrier(down_a), lax.optimization_barrier(down_b)
 
     hidden = hidden_of(own, other, up, up_scale)
-    hidden_own, hidden_other = hidden[: X * rows], hidden[X * rows :]
+    hidden_other, hidden_own = hidden[: X * rows], hidden[X * rows :]
 
-    def pair_of(down):
+    def chunk(down):
         def terms(hidden):
             return lax.dot_general(hidden, down, (((1,), (1,)), ((), ())), preferred_element_type=F32)
 
         arrived = lax.ppermute(terms(hidden_other).astype(BF16), "tp", OTHER_CORE)
-        return (terms(hidden_own) + arrived.astype(F32)).astype(BF16)
-
-    def exchanged(pair):
+        pair = (terms(hidden_own) + arrived.astype(F32)).astype(BF16)
         arrived = swapped(pair.reshape(X, rows, -1), "tp", X_GROUPS)
         return arrived.astype(F32).sum(axis=0).astype(BF16)
 
-    out_a = exchanged(pair_of(down_own))
-    out_b = exchanged(pair_of(down_b))
-    mine, for_next, for_two, for_last = from_place(x, pair_of(down_c))
-    out_c = mine.astype(F32)
-    out_c += lax.ppermute(for_next, "tp", X_LAST).astype(F32)
-    out_c += lax.ppermute(for_two, "tp", X_TWO).astype(F32)
-    out_c += lax.ppermute(for_last, "tp", X_NEXT).astype(F32)
-    summed = jnp.concatenate([out_a, out_b[:, :width], out_c.astype(BF16), out_b[:, width:]], 1)
+    out_a = chunk(down_a)
+    out_b = chunk(down_b)
+    summed = jnp.concatenate(
+        [out_a[:, :width], out_b[:, :width], out_a[:, width:], out_b[:, width:]], 1
+    )
     return rolled(summed, (ZLO - z) % ZLO, width)
 
 

time: 163 us -> 154 us (0.945)
  starting transfers between devices: 83.5 us -> 65.9 us
  waiting for transfers between devices: 49.2 us -> 62.6 us
  Pallas kernels: 11.5 us -> 5.98 us
  matrix products: 10.3 us -> 8.04 us
  local copies, waits for them, and re-layouts: 2.71 us -> 4.82 us
  other arithmetic: 3.89 us -> 5.7 us
    all_to_all x4 -> x5, waiting for transfers between devices: 7.43 us -> 28 us  [swapped(): lax.all_to_all(blocks, axis, 0, 0, axis_index_groups=groups, tiled=True)]
    ppermute x1, waiting for transfers between devices: 10.7 us -> 0.01 us  [body(): lax.ppermute(normed, 'tp', X_NEXT)]
    ppermute x7 -> x3, starting transfers between devices: 20.1 us -> 10.4 us  [the longest x1 6.09 us: body(): down_two = lax.ppermute(down_piece, PLANE, FROM_TWO)]
    ppermute x1, starting transfers between devices: 10.9 us -> 5.13 us  [body(): lax.ppermute(up_own, PLANE, FROM_NEXT)]
    all_to_all x4 -> x5, starting transfers between devices: 23.4 us -> 29.1 us  [swapped(): lax.all_to_all(blocks, axis, 0, 0, axis_index_groups=groups, tiled=True)]
    ppermute x1, starting transfers between devices: 10.9 us -> 5.75 us  [body(): lax.ppermute(down_own, PLANE, FROM_NEXT)]
    ppermute x1, waiting for transfers between devices: 0.01 us -> 5 us  [body(): lax.ppermute(down_own, PLANE, FROM_NEXT)]
    ppermute x1, waiting for transfers between devices: 3.24 us -> 7.95 us  [body(): lax.ppermute(down_own, PLANE, FROM_LAST)]
  transfers between devices with their start and end apart: 20 -> 17, of which waited for: 10 -> 9; matrix products, arithmetic and copies ran while one was open for 8% -> 9% of each run, Pallas kernels for 7% -> 4%
where the time goes in v3:
time: 154 us; the launch traced here: 153 us
  starting transfers between devices  65.9 us (43%)
  waiting for transfers between devices  62.6 us (41%)
  matrix products  8.04 us (5%)
  Pallas kernels  5.98 us (4%)
  other arithmetic  5.7 us (4%)
  local copies, waits for them, and re-layouts  4.82 us (3%)
    all_to_all x5, starting transfers between devices, swapped(): lax.all_to_all(blocks, axis, 0, 0, axis_index_groups=groups, tiled=True)  29.1 us
    all_to_all x5, waiting for transfers between devices, swapped(): lax.all_to_all(blocks, axis, 0, 0, axis_index_groups=groups, tiled=True)  28 us
    dot_general x4, matrix products, terms(): lax.dot_general(hidden, down, (((1,), (1,)), ((), ())), preferred_element...  8.04 us
    ppermute x1, waiting for transfers between devices, body(): lax.ppermute(down_own, PLANE, FROM_LAST)  7.95 us
    ppermute x1, waiting for transfers between devices, body(): down_two = lax.ppermute(down_piece, PLANE, FROM_TWO)  7.76 us
    ppermute x1, starting transfers between devices, body(): down_two = lax.ppermute(down_piece, PLANE, FROM_TWO)  6.09 us
    pallas_call x1, Pallas kernels, hidden_of(): pl.pallas_call(functools.partial(hidden_kernel, half), grid=(2 * half,),...  5.87 us
    ppermute x1, starting transfers between devices, body(): lax.ppermute(down_own, PLANE, FROM_NEXT)  5.75 us
  transfers between devices with their start and end apart: 17, of which 9 were waited for; matrix products, arithmetic and copies ran while one was open for 9% of the time, Pallas kernels for 4%

profile of v3, /device:TPU:8, one launch (start us, length us, event | category | flops | bytes accessed | tf_op | source)
XLA Modules:
  0.0 153.4 jit_solution(907993113977525394)
XLA Ops:
  1.9 9.9 %all-to-all-start.1 = ((bf16[8,48,768]{2,1,0:T(8,128)(2,1)}), bf16[8,48,768]{2,1,0:T(8,128)(2,1)}, u32[]{:S(2)}, u32[]{:S(2)}) async-start(bf16[8,48,768]{2,1,0:T(8,128)(2,1)} %broadcast_in_dim.10), calls=%async_computation.1 | async-start | bytes 1179648 | tf_op jit(solution)/shard_map/all_to_all | solution.py:36
  12.6 2.3 %collective-permute-start = (bf16[128,1536]{1,0:T(8,128)(2,1)S(1)}, bf16[128,1536]{1,0:T(8,128)(2,1)S(1)}, u32[]{:S(2)}, u32[]{:S(2)}) collective-permute-start(bf16[128,1536]{1,0:T(8,128)(2,1)S(1)} %maximum_select_fusion.refs_0_), channel_id=1, source_target_pairs={{0,6},{1,7},{2,0},{3,1},{4,2},{5,3},{6,4},{7,5},{8,14},{9,15},{10,... | collective-permute-start | bytes 1179656 | tf_op jit(solution)/shard_map/ppermute | solution.py:144
  15.0 2.7 %collective-permute-start.1 = (bf16[128,1536]{1,0:T(8,128)(2,1)S(1)}, bf16[128,1536]{1,0:T(8,128)(2,1)S(1)}, u32[]{:S(2)}, u32[]{:S(2)}) collective-permute-start(bf16[128,1536]{1,0:T(8,128)(2,1)S(1)} %maximum_select_fusion.refs_0_), channel_id=1, source_target_pairs={{0,4},{1,5},{2,6},{3,7},{4,0},{5,1},{6,2},{7,3},{8,12},{9,13},{10,... | collective-permute-start | bytes 1179656 | tf_op jit(solution)/shard_map/ppermute | solution.py:145
  17.7 2.8 %collective-permute-start.2 = (bf16[128,1536]{1,0:T(8,128)(2,1)S(1)}, bf16[128,1536]{1,0:T(8,128)(2,1)S(1)}, u32[]{:S(2)}, u32[]{:S(2)}) collective-permute-start(bf16[128,1536]{1,0:T(8,128)(2,1)S(1)} %maximum_select_fusion.refs_0_), channel_id=1, source_target_pairs={{0,2},{1,3},{2,4},{3,5},{4,6},{5,7},{6,0},{7,1},{8,10},{9,11},{10,... | collective-permute-start | bytes 1179656 | tf_op jit(solution)/shard_map/ppermute | solution.py:146
  20.5 6.5 %all-to-all-done.1 = bf16[8,48,768]{2,1,0:T(8,128)(2,1)} async-done(((bf16[8,48,768]{2,1,0:T(8,128)(2,1)}), bf16[8,48,768]{2,1,0:T(8,128)(2,1)}, u32[]{:S(2)}, u32[]{:S(2)}) %all-to-all-start.1) | async-done | bytes 589856 | tf_op jit(solution)/shard_map/all_to_all | solution.py:36
  27.9 4.9 %all-to-all-start = ((bf16[8,48,768]{2,1,0:T(8,128)(2,1)}), bf16[8,48,768]{2,1,0:T(8,128)(2,1)S(1)}, u32[]{:S(2)}, u32[]{:S(2)}) async-start(bf16[8,48,768]{2,1,0:T(8,128)(2,1)} %broadcast_in_dim.9), calls=%async_computation | async-start | bytes 1179648 | tf_op jit(solution)/shard_map/all_to_all | solution.py:36
  32.8 4.0 %collective-permute-done.2.refs_3_ = bf16[128,1536]{1,0:T(8,128)(2,1)S(1)} collective-permute-done((bf16[128,1536]{1,0:T(8,128)(2,1)S(1)}, bf16[128,1536]{1,0:T(8,128)(2,1)S(1)}, u32[]{:S(2)}, u32[]{:S(2)}) %collective-permute-start.2) | collective-permute-done | bytes 393248 | tf_op jit(solution)/shard_map/ppermute | solution.py:146
  38.7 1.9 %collective-permute-start.3 = (bf16[512,1536]{1,0:T(8,128)(2,1)S(1)}, bf16[512,1536]{1,0:T(8,128)(2,1)}, u32[]{:S(2)}, u32[]{:S(2)}) collective-permute-start(bf16[512,1536]{1,0:T(8,128)(2,1)S(1)} %by_place.1.own), channel_id=1, source_target_pairs={{0,1},{1,0},{2,3},{3,2},{4,5},{5,4},{6,7},{7,6},{8,9},{9,8},{10,11... | collective-permute-start | bytes 4718600 | tf_op jit(solution)/shard_map/ppermute | solution.py:149
  40.6 6.1 %collective-permute-start.7 = (bf16[48,768]{1,0:T(8,128)(2,1)S(1)}, bf16[48,768]{1,0:T(8,128)(2,1)S(1)}, u32[]{:S(2)}, u32[]{:S(2)}) collective-permute-start(bf16[48,768]{1,0:T(8,128)(2,1)S(1)} %fusion.7), channel_id=1, source_target_pairs={{0,128},{8,136},{16,144},{24,152},{32,160},{40,168},{48,176},{56,1... | collective-permute-start | bytes 221192 | tf_op jit(solution)/shard_map/ppermute | solution.py:135
  46.7 7.8 %collective-permute-done.7 = bf16[48,768]{1,0:T(8,128)(2,1)S(1)} collective-permute-done((bf16[48,768]{1,0:T(8,128)(2,1)S(1)}, bf16[48,768]{1,0:T(8,128)(2,1)S(1)}, u32[]{:S(2)}, u32[]{:S(2)}) %collective-permute-start.7) | collective-permute-done | bytes 73760 | tf_op jit(solution)/shard_map/ppermute | solution.py:135
  54.5 5.8 %collective-permute-start.8 = (bf16[384,768]{1,0:T(8,128)(2,1)}, bf16[384,768]{1,0:T(8,128)(2,1)S(1)}, u32[]{:S(2)}, u32[]{:S(2)}) collective-permute-start(bf16[384,768]{1,0:T(8,128)(2,1)} %bitcast.4), channel_id=1, source_target_pairs={{0,448},{8,456},{16,464},{24,472},{32,480},{40,488},{48,496},{56,5... | collective-permute-start | bytes 1769480 | tf_op jit(solution)/shard_map/ppermute | solution.py:161
  60.2 1.9 %collective-permute-start.9 = (bf16[384,768]{1,0:T(8,128)(2,1)}, bf16[384,768]{1,0:T(8,128)(2,1)}, u32[]{:S(2)}, u32[]{:S(2)}) collective-permute-start(bf16[384,768]{1,0:T(8,128)(2,1)} %bitcast.4), channel_id=1, source_target_pairs={{0,64},{8,72},{16,80},{24,88},{32,96},{40,104},{48,112},{56,120},{... | collective-permute-start | bytes 1769480 | tf_op jit(solution)/shard_map/ppermute | solution.py:161
  62.2 5.1 %collective-permute-start.4 = (bf16[384,768]{1,0:T(8,128)(2,1)S(1)}, bf16[384,768]{1,0:T(8,128)(2,1)S(1)}, u32[]{:S(2)}, u32[]{:S(2)}) collective-permute-start(bf16[384,768]{1,0:T(8,128)(2,1)S(1)} %bitcast.13), channel_id=1, source_target_pairs={{0,448},{8,456},{16,464},{24,472},{32,480},{40,488},{48,496},{56,5... | collective-permute-start | bytes 1769480 | tf_op jit(solution)/shard_map/ppermute | solution.py:153
  67.3 1.9 %collective-permute-start.5 = (bf16[384,768]{1,0:T(8,128)(2,1)S(1)}, bf16[384,768]{1,0:T(8,128)(2,1)}, u32[]{:S(2)}, u32[]{:S(2)}) collective-permute-start(bf16[384,768]{1,0:T(8,128)(2,1)S(1)} %bitcast.14), channel_id=1, source_target_pairs={{0,128},{8,136},{16,144},{24,152},{32,160},{40,168},{48,176},{56,1... | collective-permute-start | bytes 1769480 | tf_op jit(solution)/shard_map/ppermute | solution.py:154
  69.2 5.0 %collective-permute-done.8 = bf16[384,768]{1,0:T(8,128)(2,1)S(1)} collective-permute-done((bf16[384,768]{1,0:T(8,128)(2,1)}, bf16[384,768]{1,0:T(8,128)(2,1)S(1)}, u32[]{:S(2)}, u32[]{:S(2)}) %collective-permute-start.8) | collective-permute-done | bytes 589856 | tf_op jit(solution)/shard_map/ppermute | solution.py:161
  74.2 1.9 %collective-permute-start.6 = (bf16[384,768]{1,0:T(8,128)(2,1)S(1)}, bf16[384,768]{1,0:T(8,128)(2,1)}, u32[]{:S(2)}, u32[]{:S(2)}) collective-permute-start(bf16[384,768]{1,0:T(8,128)(2,1)S(1)} %bitcast.15), channel_id=1, source_target_pairs={{0,64},{8,72},{16,80},{24,88},{32,96},{40,104},{48,112},{56,120},{... | collective-permute-start | bytes 1769480 | tf_op jit(solution)/shard_map/ppermute | solution.py:155
  77.0 7.3 %all-to-all-start.3 = ((bf16[8,48,768]{2,1,0:T(8,128)(2,1)}), bf16[8,48,768]{2,1,0:T(8,128)(2,1)}, u32[]{:S(2)}, u32[]{:S(2)}) async-start(bf16[8,48,768]{2,1,0:T(8,128)(2,1)} %broadcast_in_dim.11), calls=%async_computation.3 | async-start | bytes 1179648 | tf_op jit(solution)/shard_map/all_to_all | solution.py:36
  84.4 7.9 %collective-permute-done.9 = bf16[384,768]{1,0:T(8,128)(2,1)} collective-permute-done((bf16[384,768]{1,0:T(8,128)(2,1)}, bf16[384,768]{1,0:T(8,128)(2,1)}, u32[]{:S(2)}, u32[]{:S(2)}) %collective-permute-start.9) | collective-permute-done | bytes 589856 | tf_op jit(solution)/shard_map/ppermute | solution.py:161
  93.7 4.4 %collective-permute-done.4.u1 = bf16[384,768]{1,0:T(8,128)(2,1)S(1)} collective-permute-done((bf16[384,768]{1,0:T(8,128)(2,1)S(1)}, bf16[384,768]{1,0:T(8,128)(2,1)S(1)}, u32[]{:S(2)}, u32[]{:S(2)}) %collective-permute-start.4) | collective-permute-done | bytes 589856 | tf_op jit(solution)/shard_map/ppermute | solution.py:153
  98.1 5.4 %collective-permute-done.6.u3 = bf16[384,768]{1,0:T(8,128)(2,1)} collective-permute-done((bf16[384,768]{1,0:T(8,128)(2,1)S(1)}, bf16[384,768]{1,0:T(8,128)(2,1)}, u32[]{:S(2)}, u32[]{:S(2)}) %collective-permute-start.6) | collective-permute-done | bytes 589856 | tf_op jit(solution)/shard_map/ppermute | solution.py:155
  103.5 5.9 %hidden.1 = bf16[1024,768]{1,0:T(8,128)(2,1)S(1)} custom-call(bf16[512,1536]{1,0:T(8,128)(2,1)S(1)} %by_place.1.own, bf16[512,1536]{1,0:T(8,128)(2,1)} %collective-permute-done.3.other, bf16[384,768]{1,0:T(8,128)(2,1)S(1)} %bitcast.16, bf16[384,768]{1,0:T(8,128)(2,1)S(1)} %collective-permute-done.4.u1, bf16[384,768]{1,0:T(8,128)(2,1)} %collective-permute-done.5.u2, ...), custom_call_target="tpu_custom_call" | custom-call | flops 2415919104 | bytes 7077888 | tf_op jit(solution)/shard_map/hidden/pallas_call | solution.py:107
  109.4 1.7 %convolution_convert_fusion.1 = bf16[512,768]{1,0:T(8,128)(2,1)} fusion(bf16[768,768]{1,0:T(8,128)(2,1)S(1)} %pad_maximum_fusion, bf16[1024,768]{1,0:T(8,128)(2,1)S(1)} %hidden.1), kind=kOutput, calls=%fused_computation.3 | convolution fusion | flops 604372992 | bytes 2752512 | tf_op jit(solution)/shard_map/dot_general | solution.py:169
  111.1 1.9 %collective-permute-start.10 = (bf16[512,768]{1,0:T(8,128)(2,1)}, bf16[512,768]{1,0:T(8,128)(2,1)S(1)}, u32[]{:S(2)}, u32[]{:S(2)}) collective-permute-start(bf16[512,768]{1,0:T(8,128)(2,1)} %convolution_convert_fusion.1), channel_id=1, source_target_pairs={{0,1},{1,0},{2,3},{3,2},{4,5},{5,4},{6,7},{7,6},{8,9},{9,8},{10,11... | collective-permute-start | bytes 2359304 | tf_op jit(solution)/shard_map/ppermute | solution.py:171
  113.0 1.4 pad_maximum_fusion.1
  114.8 1.7 %convolution_convert_fusion = bf16[512,768]{1,0:T(8,128)(2,1)} fusion(bf16[768,768]{1,0:T(8,128)(2,1)S(1)} %pad_maximum_fusion.1, bf16[1024,768]{1,0:T(8,128)(2,1)S(1)} %copy-done.4), kind=kOutput, calls=%fused_computation.2 | convolution fusion | flops 604372992 | bytes 2752512 | tf_op jit(solution)/shard_map/dot_general | solution.py:169
  116.5 2.4 %collective-permute-start.11 = (bf16[512,768]{1,0:T(8,128)(2,1)}, bf16[512,768]{1,0:T(8,128)(2,1)}, u32[]{:S(2)}, u32[]{:S(2)}) collective-permute-start(bf16[512,768]{1,0:T(8,128)(2,1)} %convolution_convert_fusion), channel_id=1, source_target_pairs={{0,1},{1,0},{2,3},{3,2},{4,5},{5,4},{6,7},{7,6},{8,9},{9,8},{10,11... | collective-permute-start | bytes 2359304 | tf_op jit(solution)/shard_map/ppermute | solution.py:171
  119.0 1.7 %add_convert_fusion.1 = bf16[512,768]{1,0:T(8,128)(2,1)} fusion(bf16[512,768]{1,0:T(8,128)(2,1)S(1)} %collective-permute-done.10, bf16[768,768]{1,0:T(8,128)(2,1)S(1)} %copy-done.7, bf16[1024,768]{1,0:T(8,128)(2,1)S(1)} %copy-done.4), kind=kOutput, calls=%fused_computation.1 | convolution fusion | flops 605159424 | bytes 3538944 | tf_op jit(solution)/shard_map/dot_general | solution.py:169
  120.7 3.5 %all-to-all-start.2 = ((bf16[4,128,768]{2,1,0:T(8,128)(2,1)}), bf16[4,128,768]{2,1,0:T(8,128)(2,1)S(1)}, u32[]{:S(2)}, u32[]{:S(2)}) async-start(bf16[4,128,768]{2,1,0:T(8,128)(2,1)} %bitcast.18), calls=%async_computation.2 | async-start | bytes 1572864 | tf_op jit(solution)/shard_map/all_to_all | solution.py:36
  124.2 2.9 %add_convert_fusion = bf16[512,768]{1,0:T(8,128)(2,1)} fusion(bf16[512,768]{1,0:T(8,128)(2,1)} %collective-permute-done.11, bf16[768,768]{1,0:T(8,128)(2,1)S(1)} %pad_maximum_fusion.1, bf16[1024,768]{1,0:T(8,128)(2,1)S(1)} %copy-done.4), kind=kOutput, calls=%fused_computation | convolution fusion | flops 605159424 | bytes 3538944 | tf_op jit(solution)/shard_map/dot_general | solution.py:169
  127.1 9.8 %all-to-all-done.2 = bf16[4,128,768]{2,1,0:T(8,128)(2,1)S(1)} async-done(((bf16[4,128,768]{2,1,0:T(8,128)(2,1)}), bf16[4,128,768]{2,1,0:T(8,128)(2,1)S(1)}, u32[]{:S(2)}, u32[]{:S(2)}) %all-to-all-start.2) | async-done | bytes 786464 | tf_op jit(solution)/shard_map/all_to_all | solution.py:36
  136.9 3.5 %all-to-all-start.4 = ((bf16[4,128,768]{2,1,0:T(8,128)(2,1)}), bf16[4,128,768]{2,1,0:T(8,128)(2,1)S(1)}, u32[]{:S(2)}, u32[]{:S(2)}) async-start(bf16[4,128,768]{2,1,0:T(8,128)(2,1)} %bitcast.17), calls=%async_computation.4 | async-start | bytes 1572864 | tf_op jit(solution)/shard_map/all_to_all | solution.py:36
  140.6 11.7 %all-to-all-done.4 = bf16[4,128,768]{2,1,0:T(8,128)(2,1)S(1)} async-done(((bf16[4,128,768]{2,1,0:T(8,128)(2,1)}), bf16[4,128,768]{2,1,0:T(8,128)(2,1)S(1)}, u32[]{:S(2)}, u32[]{:S(2)}) %all-to-all-start.4) | async-done | bytes 786464 | tf_op jit(solution)/shard_map/all_to_all | solution.py:36
  (49 shorter events, 9.2 us)
Async XLA Ops:
  0.0 11.8 %copy-start.5 = (bf16[128,1536]{1,0:T(8,128)(2,1)S(1)}, bf16[128,1536]{1,0:T(8,128)(2,1)}, u32[]{:S(2)}) copy-start(bf16[128,1536]{1,0:T(8,128)(2,1)} %param.6) | copy-start | bytes 1179652
  0.0 12.0 %copy-start.10 = (f32[1536]{0:T(1024)S(1)}, f32[1536]{0:T(1024)}, u32[]{:S(2)}) copy-start(f32[1536]{0:T(1024)} %param.7) | copy-start | bytes 18436
  1.9 25.1 %all-to-all-start.1 = ((bf16[8,48,768]{2,1,0:T(8,128)(2,1)}), bf16[8,48,768]{2,1,0:T(8,128)(2,1)}, u32[]{:S(2)}, u32[]{:S(2)}) async-start(bf16[8,48,768]{2,1,0:T(8,128)(2,1)} %broadcast_in_dim.10), calls=%async_computation.1 | async-start | bytes 1179648 | tf_op jit(solution)/shard_map/all_to_all | solution.py:36
  12.2 8.3 %copy-start.9 = (f32[48,768]{1,0:T(8,128)S(1)}, f32[48,768]{1,0:T(8,128)}, u32[]{:S(2)}) copy-start(f32[48,768]{1,0:T(8,128)} %param.8) | copy-start | bytes 442372
  12.6 20.1 %collective-permute-start = (bf16[128,1536]{1,0:T(8,128)(2,1)S(1)}, bf16[128,1536]{1,0:T(8,128)(2,1)S(1)}, u32[]{:S(2)}, u32[]{:S(2)}) collective-permute-start(bf16[128,1536]{1,0:T(8,128)(2,1)S(1)} %maximum_select_fusion.refs_0_), channel_id=1, source_target_pairs={{0,6},{1,7},{2,0},{3,1},{4,2},{5,3},{6,4},{7,5},{8,14},{9,15},{10,... | collective-permute-start | bytes 1179656 | tf_op jit(solution)/shard_map/ppermute | solution.py:144
  15.0 17.8 %collective-permute-start.1 = (bf16[128,1536]{1,0:T(8,128)(2,1)S(1)}, bf16[128,1536]{1,0:T(8,128)(2,1)S(1)}, u32[]{:S(2)}, u32[]{:S(2)}) collective-permute-start(bf16[128,1536]{1,0:T(8,128)(2,1)S(1)} %maximum_select_fusion.refs_0_), channel_id=1, source_target_pairs={{0,4},{1,5},{2,6},{3,7},{4,0},{5,1},{6,2},{7,3},{8,12},{9,13},{10,... | collective-permute-start | bytes 1179656 | tf_op jit(solution)/shard_map/ppermute | solution.py:145
  17.7 19.1 %collective-permute-start.2 = (bf16[128,1536]{1,0:T(8,128)(2,1)S(1)}, bf16[128,1536]{1,0:T(8,128)(2,1)S(1)}, u32[]{:S(2)}, u32[]{:S(2)}) collective-permute-start(bf16[128,1536]{1,0:T(8,128)(2,1)S(1)} %maximum_select_fusion.refs_0_), channel_id=1, source_target_pairs={{0,2},{1,3},{2,4},{3,5},{4,6},{5,7},{6,0},{7,1},{8,10},{9,11},{10,... | collective-permute-start | bytes 1179656 | tf_op jit(solution)/shard_map/ppermute | solution.py:146
  27.9 34.3 %all-to-all-start = ((bf16[8,48,768]{2,1,0:T(8,128)(2,1)}), bf16[8,48,768]{2,1,0:T(8,128)(2,1)S(1)}, u32[]{:S(2)}, u32[]{:S(2)}) async-start(bf16[8,48,768]{2,1,0:T(8,128)(2,1)} %broadcast_in_dim.9), calls=%async_computation | async-start | bytes 1179648 | tf_op jit(solution)/shard_map/all_to_all | solution.py:36
  36.8 0.7 copy-start
  37.6 1.0 copy-start.1
  38.7 64.8 %collective-permute-start.3 = (bf16[512,1536]{1,0:T(8,128)(2,1)S(1)}, bf16[512,1536]{1,0:T(8,128)(2,1)}, u32[]{:S(2)}, u32[]{:S(2)}) collective-permute-start(bf16[512,1536]{1,0:T(8,128)(2,1)S(1)} %by_place.1.own), channel_id=1, source_target_pairs={{0,1},{1,0},{2,3},{3,2},{4,5},{5,4},{6,7},{7,6},{8,9},{9,8},{10,11... | collective-permute-start | bytes 4718600 | tf_op jit(solution)/shard_map/ppermute | solution.py:149
  40.6 13.9 %collective-permute-start.7 = (bf16[48,768]{1,0:T(8,128)(2,1)S(1)}, bf16[48,768]{1,0:T(8,128)(2,1)S(1)}, u32[]{:S(2)}, u32[]{:S(2)}) collective-permute-start(bf16[48,768]{1,0:T(8,128)(2,1)S(1)} %fusion.7), channel_id=1, source_target_pairs={{0,128},{8,136},{16,144},{24,152},{32,160},{40,168},{48,176},{56,1... | collective-permute-start | bytes 221192 | tf_op jit(solution)/shard_map/ppermute | solution.py:135
  54.5 19.8 %collective-permute-start.8 = (bf16[384,768]{1,0:T(8,128)(2,1)}, bf16[384,768]{1,0:T(8,128)(2,1)S(1)}, u32[]{:S(2)}, u32[]{:S(2)}) collective-permute-start(bf16[384,768]{1,0:T(8,128)(2,1)} %bitcast.4), channel_id=1, source_target_pairs={{0,448},{8,456},{16,464},{24,472},{32,480},{40,488},{48,496},{56,5... | collective-permute-start | bytes 1769480 | tf_op jit(solution)/shard_map/ppermute | solution.py:161
  60.2 32.1 %collective-permute-start.9 = (bf16[384,768]{1,0:T(8,128)(2,1)}, bf16[384,768]{1,0:T(8,128)(2,1)}, u32[]{:S(2)}, u32[]{:S(2)}) collective-permute-start(bf16[384,768]{1,0:T(8,128)(2,1)} %bitcast.4), channel_id=1, source_target_pairs={{0,64},{8,72},{16,80},{24,88},{32,96},{40,104},{48,112},{56,120},{... | collective-permute-start | bytes 1769480 | tf_op jit(solution)/shard_map/ppermute | solution.py:161
  62.2 35.9 %collective-permute-start.4 = (bf16[384,768]{1,0:T(8,128)(2,1)S(1)}, bf16[384,768]{1,0:T(8,128)(2,1)S(1)}, u32[]{:S(2)}, u32[]{:S(2)}) collective-permute-start(bf16[384,768]{1,0:T(8,128)(2,1)S(1)} %bitcast.13), channel_id=1, source_target_pairs={{0,448},{8,456},{16,464},{24,472},{32,480},{40,488},{48,496},{56,5... | collective-permute-start | bytes 1769480 | tf_op jit(solution)/shard_map/ppermute | solution.py:153
  67.3 30.8 %collective-permute-start.5 = (bf16[384,768]{1,0:T(8,128)(2,1)S(1)}, bf16[384,768]{1,0:T(8,128)(2,1)}, u32[]{:S(2)}, u32[]{:S(2)}) collective-permute-start(bf16[384,768]{1,0:T(8,128)(2,1)S(1)} %bitcast.14), channel_id=1, source_target_pairs={{0,128},{8,136},{16,144},{24,152},{32,160},{40,168},{48,176},{56,1... | collective-permute-start | bytes 1769480 | tf_op jit(solution)/shard_map/ppermute | solution.py:154
  74.2 1.9 %copy-start.8 = (bf16[384,768]{1,0:T(8,128)(2,1)}, bf16[384,768]{1,0:T(8,128)(2,1)S(1)}, u32[]{:S(2)}) copy-start(bf16[384,768]{1,0:T(8,128)(2,1)S(1)} %collective-permute-done.8) | copy-start | bytes 1769476
  74.2 29.3 %collective-permute-start.6 = (bf16[384,768]{1,0:T(8,128)(2,1)S(1)}, bf16[384,768]{1,0:T(8,128)(2,1)}, u32[]{:S(2)}, u32[]{:S(2)}) collective-permute-start(bf16[384,768]{1,0:T(8,128)(2,1)S(1)} %bitcast.15), channel_id=1, source_target_pairs={{0,64},{8,72},{16,80},{24,88},{32,96},{40,104},{48,112},{56,120},{... | collective-permute-start | bytes 1769480 | tf_op jit(solution)/shard_map/ppermute | solution.py:155
  77.0 26.5 %copy-start.2 = (f32[1,768]{1,0:T(1,128)S(1)}, f32[1,768]{1,0:T(1,128)}, u32[]{:S(2)}) copy-start(f32[1,768]{1,0:T(1,128)} %scale.1) | copy-start | bytes 9220
  77.0 36.0 %all-to-all-start.3 = ((bf16[8,48,768]{2,1,0:T(8,128)(2,1)}), bf16[8,48,768]{2,1,0:T(8,128)(2,1)}, u32[]{:S(2)}, u32[]{:S(2)}) async-start(bf16[8,48,768]{2,1,0:T(8,128)(2,1)} %broadcast_in_dim.11), calls=%async_computation.3 | async-start | bytes 1179648 | tf_op jit(solution)/shard_map/all_to_all | solution.py:36
  93.6 15.8 %copy-start.6 = (bf16[768,768]{1,0:T(8,128)(2,1)}, bf16[768,768]{1,0:T(8,128)(2,1)S(1)}, u32[]{:S(2)}) copy-start(bf16[768,768]{1,0:T(8,128)(2,1)S(1)} %pad_maximum_fusion) | copy-start | bytes 3538948
  109.4 1.7 %copy-start.3 = (bf16[1024,768]{1,0:T(8,128)(2,1)}, bf16[1024,768]{1,0:T(8,128)(2,1)S(1)}, u32[]{:S(2)}) copy-start(bf16[1024,768]{1,0:T(8,128)(2,1)S(1)} %hidden.1) | copy-start | bytes 4718596
  111.1 7.8 %collective-permute-start.10 = (bf16[512,768]{1,0:T(8,128)(2,1)}, bf16[512,768]{1,0:T(8,128)(2,1)S(1)}, u32[]{:S(2)}, u32[]{:S(2)}) collective-permute-start(bf16[512,768]{1,0:T(8,128)(2,1)} %convolution_convert_fusion.1), channel_id=1, source_target_pairs={{0,1},{1,0},{2,3},{3,2},{4,5},{5,4},{6,7},{7,6},{8,9},{9,8},{10,11... | collective-permute-start | bytes 2359304 | tf_op jit(solution)/shard_map/ppermute | solution.py:171
  113.0 1.8 %copy-start.4 = (bf16[1024,768]{1,0:T(8,128)(2,1)S(1)}, bf16[1024,768]{1,0:T(8,128)(2,1)}, u32[]{:S(2)}) copy-start(bf16[1024,768]{1,0:T(8,128)(2,1)} %copy-done.3) | copy-start | bytes 4718596
  114.8 4.2 %copy-start.7 = (bf16[768,768]{1,0:T(8,128)(2,1)S(1)}, bf16[768,768]{1,0:T(8,128)(2,1)}, u32[]{:S(2)}) copy-start(bf16[768,768]{1,0:T(8,128)(2,1)} %copy-done.6) | copy-start | bytes 3538948
  116.5 7.7 %collective-permute-start.11 = (bf16[512,768]{1,0:T(8,128)(2,1)}, bf16[512,768]{1,0:T(8,128)(2,1)}, u32[]{:S(2)}, u32[]{:S(2)}) collective-permute-start(bf16[512,768]{1,0:T(8,128)(2,1)} %convolution_convert_fusion), channel_id=1, source_target_pairs={{0,1},{1,0},{2,3},{3,2},{4,5},{5,4},{6,7},{7,6},{8,9},{9,8},{10,11... | collective-permute-start | bytes 2359304 | tf_op jit(solution)/shard_map/ppermute | solution.py:171
  120.7 16.2 %all-to-all-start.2 = ((bf16[4,128,768]{2,1,0:T(8,128)(2,1)}), bf16[4,128,768]{2,1,0:T(8,128)(2,1)S(1)}, u32[]{:S(2)}, u32[]{:S(2)}) async-start(bf16[4,128,768]{2,1,0:T(8,128)(2,1)} %bitcast.18), calls=%async_computation.2 | async-start | bytes 1572864 | tf_op jit(solution)/shard_map/all_to_all | solution.py:36
  136.9 15.3 %all-to-all-start.4 = ((bf16[4,128,768]{2,1,0:T(8,128)(2,1)}), bf16[4,128,768]{2,1,0:T(8,128)(2,1)S(1)}, u32[]{:S(2)}, u32[]{:S(2)}) async-start(bf16[4,128,768]{2,1,0:T(8,128)(2,1)} %bitcast.17), calls=%async_computation.4 | async-start | bytes 1572864 | tf_op jit(solution)/shard_map/all_to_all | solution.py:36

commit v4 on v3

v4 whole, which is shorter than its diff:
```python
import functools

import jax
import jax.numpy as jnp
from jax import lax
from jax.experimental import pallas as pl
from jax.experimental.pallas import tpu as pltpu
from jax.sharding import PartitionSpec as P


Z, ZLO, Y, X = 8, 4, 8, 4
ROW_GROUPS = [[z * Y + y for y in range(Y)] for z in range(ZLO)]
X_GROUPS = [[2 * x + c for x in range(X)] for c in range(2)]
OTHER_CORE = [(i, i ^ 1) for i in range(2 * X)]
PLANE = ("rep", "fs")
F32, BF16 = jnp.float32, jnp.bfloat16


def z_shift(by):
    return [(z * Y + y, (z + by(z)) % Z * Y + y) for z in range(Z) for y in range(Y)]


def x_shift(by):
    return [(2 * x + c, (x + by(x)) % X * 2 + c) for x in range(X) for c in range(2)]


FROM_NEXT = z_shift(lambda z: -1)
FROM_LAST = z_shift(lambda z: 1)
FROM_TWO = z_shift(lambda z: 2 if z % 2 == 0 else -2)
X_NEXT = x_shift(lambda x: -1)
X_LAST = x_shift(lambda x: 1)
X_TWO = x_shift(lambda x: 2)


def swapped(blocks, axis, groups):
    return lax.all_to_all(blocks, axis, 0, 0, axis_index_groups=groups, tiled=True)


def rolled(a, by, width):
    n = a.shape[1] // width
    out = a
    for k in range(1, n):
        out = jnp.where(by == k, jnp.concatenate([a[:, width * k :], a[:, : width * k]], 1), out)
    return out


VMEM = pl.BlockSpec(memory_space=pltpu.VMEM)
SMEM = pl.BlockSpec(memory_space=pltpu.SMEM)


def cost(flops, *arrays):
    return pl.CostEstimate(flops=flops, bytes_accessed=sum(a.size * a.dtype.itemsize for a in arrays), transcendentals=0)


def copies_kernel(*refs):
    *shards, out = refs
    for k, shard in enumerate(shards):
        block = shard[...].astype(out.dtype)
        for i in range(out.shape[0]):
            out[i, k] = block


def copies_of(shards):
    out = jax.ShapeDtypeStruct((Y, len(shards), *shards[0].shape), BF16)
    return pl.pallas_call(
        copies_kernel,
        out_shape=out,
        in_specs=[VMEM] * len(shards),
        out_specs=VMEM,
        compiler_params=pltpu.CompilerParams(vmem_limit_bytes=8 << 20),
        cost_estimate=cost(1 << 28, out, *shards),
        name="copies",
    )(*shards)


def split_kernel(blocks, own, both):
    rows = blocks.shape[2]
    width = own.shape[0]
    for y in range(blocks.shape[0]):
        own[y * rows : (y + 1) * rows] = both[y * rows : (y + 1) * rows] = blocks[y, 0]
        both[width + y * rows : width + (y + 1) * rows] = blocks[y, 1]


def split(blocks):
    count, _, rows, columns = blocks.shape
    own = jax.ShapeDtypeStruct((count * rows, columns), BF16)
    both = jax.ShapeDtypeStruct((2 * count * rows, columns), BF16)
    return pl.pallas_call(
        split_kernel,
        out_shape=[own, both],
        in_specs=[VMEM],
        out_specs=[VMEM] * 2,
        compiler_params=pltpu.CompilerParams(vmem_limit_bytes=8 << 20),
        cost_estimate=cost(1 << 28, own, both, blocks),
        name="split",
    )(blocks)


def by_place_kernel(x_ref, *refs):
    *blocks, out = refs
    rows = blocks[0].shape[0]
    for k, block in enumerate(blocks):
        out[pl.ds(pl.multiple_of((x_ref[0] + k) % X * rows, rows), rows), :] = block[...]


def by_place(x, blocks):
    rows, columns = blocks[0].shape
    return pl.pallas_call(
        by_place_kernel,
        out_shape=jax.ShapeDtypeStruct((X * rows, columns), blocks[0].dtype),
        in_specs=[SMEM] + [VMEM] * X,
        out_specs=VMEM,
        cost_estimate=cost(1 << 28, *blocks, *blocks),
        compiler_params=pltpu.CompilerParams(vmem_limit_bytes=8 << 20),
        name="by_place",
    )(x[None], *blocks)


TILE = 256


def hidden_kernel(half, other, own, u0, u1, u2, u3, scale, down_ref, hidden, terms, up, down, sems):
    step = pl.program_id(0)

    @pl.when(step == 0)
    def _():
        width = u0.shape[0]
        fetches = [
            pltpu.make_async_copy(block, up.at[pl.ds(k * width, width)], sems.at[k])
            for k, block in enumerate((u0, u1, u2, u3))
        ]
        fetches.append(pltpu.make_async_copy(down_ref, down, sems.at[len(fetches)]))
        for fetch in fetches:
            fetch.start()
        for fetch in fetches:
            fetch.wait()

    def hidden_of(rows):
        pre = jnp.dot(rows[...], up[...], preferred_element_type=F32)
        return jnp.square(jnp.maximum(pre * scale[...], 0.0)).astype(BF16)

    @pl.when(step < half)
    def _():
        tile = hidden_of(other)
        hidden[...] = tile
        terms[...] = lax.dot_general(
            tile, down[...], (((1,), (1,)), ((), ())), preferred_element_type=F32
        ).astype(BF16)

    @pl.when(step >= half)
    def _():
        hidden[...] = hidden_of(own)


def hidden_of(other, own, up, scale, down):
    rows, d = own.shape
    _, columns = up[0].shape
    half = rows // TILE
    hidden = jax.ShapeDtypeStruct((2 * rows, columns), BF16)
    terms = jax.ShapeDtypeStruct((rows, down.shape[0]), BF16)
    anywhere = pl.BlockSpec(memory_space=pl.ANY)
    return pl.pallas_call(
        functools.partial(hidden_kernel, half),
        grid=(2 * half,),
        out_shape=[hidden, terms],
        in_specs=[
            pl.BlockSpec((TILE, d), lambda i: (jnp.minimum(i, half - 1), 0)),
            pl.BlockSpec((TILE, d), lambda i: (jnp.maximum(i - half, 0), 0)),
            *([anywhere] * ZLO),
            pl.BlockSpec((1, columns), lambda i: (0, 0)),
            anywhere,
        ],
        out_specs=[
            pl.BlockSpec((TILE, columns), lambda i: (i, 0)),
            pl.BlockSpec((TILE, down.shape[0]), lambda i: (jnp.minimum(i, half - 1), 0)),
        ],
        scratch_shapes=[
            pltpu.VMEM((d, columns), BF16),
            pltpu.VMEM(down.shape, BF16),
            pltpu.SemaphoreType.DMA((ZLO + 1,)),
        ],
        compiler_params=pltpu.CompilerParams(vmem_limit_bytes=24 << 20),
        cost_estimate=cost(4 * rows * d * columns, own, other, *up, down, hidden, terms),
        name="hidden",
    )(other, own, *up, scale, down)


def body(tokens, norm_gain, up_weight, up_scale, down_weight, down_scale):
    z = lax.axis_index("fs") // Y
    x = lax.axis_index("tp") // 2
    rows, d = tokens.shape
    width = d // ZLO
    hidden_width = up_weight.shape[1]

    copies = copies_of([up_weight])
    up_own = swapped(copies[:, 0], "fs", ROW_GROUPS).reshape(width, hidden_width)
    down_piece = (down_weight * down_scale).T.astype(BF16)
    down_two = lax.ppermute(down_piece, PLANE, FROM_TWO)

    values = tokens.astype(F32)
    normed = (
        values * lax.rsqrt(jnp.mean(values * values, axis=-1, keepdims=True) + 1e-06) * norm_gain
    ).astype(BF16)
    normed = rolled(normed, z, width)
    near = [
        normed,
        lax.ppermute(normed, "tp", X_NEXT),
        lax.ppermute(normed, "tp", X_TWO),
        lax.ppermute(normed, "tp", X_LAST),
    ]
    own = by_place(x, near)
    other = lax.ppermute(own, "tp", OTHER_CORE)

    up = [
        up_own,
        lax.ppermute(up_own, PLANE, FROM_NEXT),
        lax.ppermute(up_own, PLANE, FROM_TWO),
        lax.ppermute(up_own, PLANE, FROM_LAST),
    ]
    copies = copies_of([down_piece, down_two])
    down_own, down_a = split(swapped(copies, "fs", ROW_GROUPS))
    down_b = jnp.concatenate(
        [lax.ppermute(down_own, PLANE, FROM_NEXT), lax.ppermute(down_own, PLANE, FROM_LAST)], 0
    )
    down_b = lax.optimization_barrier(down_b)

    hidden, for_other = hidden_of(other, own, up, up_scale, down_a)
    hidden_other, hidden_own = hidden[: X * rows], hidden[X * rows :]

    def terms(hidden, down):
        return lax.dot_general(hidden, down, (((1,), (1,)), ((), ())), preferred_element_type=F32)

    def chunk(down, for_other):
        arrived = lax.ppermute(for_other, "tp", OTHER_CORE)
        pair = (terms(hidden_own, down) + arrived.astype(F32)).astype(BF16)
        arrived = swapped(pair.reshape(X, rows, -1), "tp", X_GROUPS)
        return arrived.astype(F32).sum(axis=0).astype(BF16)

    out_a = chunk(down_a, for_other)
    out_b = chunk(down_b, terms(hidden_other, down_b).astype(BF16))
    summed = jnp.concatenate(
        [out_a[:, :width], out_b[:, :width], out_a[:, width:], out_b[:, width:]], 1
    )
    return rolled(summed, (ZLO - z) % ZLO, width)


def solution(mesh):
    return jax.shard_map(
        body,
        mesh=mesh,
        in_specs=(
            P(("rep", "fs", "tp"), None),
            P(),
            P("fs", "tp"),
            P(None, "tp"),
            P("tp", "fs"),
            P(None, "fs"),
        ),
        out_specs=P(("rep", "fs", "tp"), None),
        check_vma=False,
    )
```

time: 154 us -> 163 us (1.058)
  starting transfers between devices: 65.9 us -> 76.8 us
  Pallas kernels: 5.98 us -> 8.98 us
  other arithmetic: 5.7 us -> 2.98 us
  matrix products: 8.04 us -> 6.26 us
    ppermute x1, starting transfers between devices: 1.92 us -> 16.6 us  [body(): lax.ppermute(down_own, PLANE, FROM_LAST)]
    ppermute x1, waiting for transfers between devices: 0.01 us -> 11.2 us  [body(): lax.ppermute(normed, 'tp', X_NEXT)]
    all_to_all x5 -> x4, waiting for transfers between devices: 28 us -> 38.1 us  [swapped(): lax.all_to_all(blocks, axis, 0, 0, axis_index_groups=groups, tiled=True)]
    all_to_all x5 -> x4, starting transfers between devices: 29.1 us -> 19.6 us  [swapped(): lax.all_to_all(blocks, axis, 0, 0, axis_index_groups=groups, tiled=True)]
    ppermute x1, waiting for transfers between devices: 7.76 us -> 0.01 us  [body(): down_two = lax.ppermute(down_piece, PLANE, FROM_TWO)]
    ppermute x1, waiting for transfers between devices: 5 us -> 0.01 us  [body(): lax.ppermute(down_own, PLANE, FROM_NEXT)]
    ppermute x1, waiting for transfers between devices: 5.43 us -> 0.64 us  [body(): lax.ppermute(up_own, PLANE, FROM_LAST)]
    ppermute x1, waiting for transfers between devices: 7.95 us -> 3.72 us  [body(): lax.ppermute(down_own, PLANE, FROM_LAST)]
  transfers between devices with their start and end apart: 17 -> 16, of which waited for: 9 -> 8; matrix products, arithmetic and copies ran while one was open for 9% -> 4% of each run, Pallas kernels for 4% -> 6%
where the time goes in v4:
time: 163 us; the launch traced here: 162 us
  starting transfers between devices  76.8 us (47%)
  waiting for transfers between devices  62.3 us (38%)
  Pallas kernels  8.98 us (6%)
  matrix products  6.26 us (4%)
  local copies, waits for them, and re-layouts  4.56 us (3%)
  other arithmetic  2.98 us (2%)
    all_to_all x4, waiting for transfers between devices, swapped(): lax.all_to_all(blocks, axis, 0, 0, axis_index_groups=groups, tiled=True)  38.1 us
    all_to_all x4, starting transfers between devices, swapped(): lax.all_to_all(blocks, axis, 0, 0, axis_index_groups=groups, tiled=True)  19.6 us
    ppermute x1, starting transfers between devices, body(): lax.ppermute(down_own, PLANE, FROM_LAST)  16.6 us
    ppermute x1, waiting for transfers between devices, body(): lax.ppermute(normed, 'tp', X_NEXT)  11.2 us
    ppermute x1, starting transfers between devices, body(): lax.ppermute(up_own, PLANE, FROM_NEXT)  7.31 us
    pallas_call x1, Pallas kernels, hidden_of(): pl.pallas_call(functools.partial(hidden_kernel, half), grid=(2 * half,),...  6.76 us
    dot_general x3, matrix products, terms(): lax.dot_general(hidden, down, (((1,), (1,)), ((), ())), preferred_element...  6.26 us
    ppermute x1, starting transfers between devices, body(): down_two = lax.ppermute(down_piece, PLANE, FROM_TWO)  6.09 us
  transfers between devices with their start and end apart: 16, of which 8 were waited for; matrix products, arithmetic and copies ran while one was open for 4% of the time, Pallas kernels for 6%

profile of v4, /device:TPU:8, one launch (start us, length us, event | category | flops | bytes accessed | tf_op | source)
XLA Modules:
  0.0 162.2 jit_solution(12849051981915140814)
XLA Ops:
  0.0 1.0 fusion.6.refs_0_
  1.0 6.1 %collective-permute-start.7 = (bf16[48,768]{1,0:T(8,128)(2,1)S(1)}, bf16[48,768]{1,0:T(8,128)(2,1)S(1)}, u32[]{:S(2)}, u32[]{:S(2)}) collective-permute-start(bf16[48,768]{1,0:T(8,128)(2,1)S(1)} %fusion.6.refs_0_), channel_id=1, source_target_pairs={{0,128},{8,136},{16,144},{24,152},{32,160},{40,168},{48,176},{56,1... | collective-permute-start | bytes 221192 | tf_op jit(solution)/shard_map/ppermute | solution.py:198
  8.9 7.5 %all-to-all-start = ((bf16[8,48,768]{2,1,0:T(8,128)(2,1)}), bf16[8,48,768]{2,1,0:T(8,128)(2,1)}, u32[]{:S(2)}, u32[]{:S(2)}) async-start(bf16[8,48,768]{2,1,0:T(8,128)(2,1)} %bitcast.1), calls=%async_computation | async-start | bytes 1179648 | tf_op jit(solution)/shard_map/all_to_all | solution.py:36
  17.0 1.1 copies.3
  18.1 15.7 %all-to-all-done = bf16[8,48,768]{2,1,0:T(8,128)(2,1)} async-done(((bf16[8,48,768]{2,1,0:T(8,128)(2,1)}), bf16[8,48,768]{2,1,0:T(8,128)(2,1)}, u32[]{:S(2)}, u32[]{:S(2)}) %all-to-all-start) | async-done | bytes 589856 | tf_op jit(solution)/shard_map/all_to_all | solution.py:36
  33.7 4.9 %all-to-all-start.1 = ((bf16[8,2,48,768]{3,2,1,0:T(8,128)(2,1)}), bf16[8,2,48,768]{3,2,1,0:T(8,128)(2,1)S(1)}, u32[]{:S(2)}, u32[]{:S(2)}) async-start(bf16[8,2,48,768]{3,2,1,0:T(8,128)(2,1)} %copies.3), calls=%async_computation.1 | async-start | bytes 2359296 | tf_op jit(solution)/shard_map/all_to_all | solution.py:36
  39.0 4.7 %collective-permute-start = (bf16[128,1536]{1,0:T(8,128)(2,1)S(1)}, bf16[128,1536]{1,0:T(8,128)(2,1)S(1)}, u32[]{:S(2)}, u32[]{:S(2)}) collective-permute-start(bf16[128,1536]{1,0:T(8,128)(2,1)S(1)} %maximum_select_fusion.refs_0_), channel_id=1, source_target_pairs={{0,6},{1,7},{2,0},{3,1},{4,2},{5,3},{6,4},{7,5},{8,14},{9,15},{10,... | collective-permute-start | bytes 1179656 | tf_op jit(solution)/shard_map/ppermute | solution.py:207
  43.7 2.7 %collective-permute-start.1 = (bf16[128,1536]{1,0:T(8,128)(2,1)S(1)}, bf16[128,1536]{1,0:T(8,128)(2,1)S(1)}, u32[]{:S(2)}, u32[]{:S(2)}) collective-permute-start(bf16[128,1536]{1,0:T(8,128)(2,1)S(1)} %maximum_select_fusion.refs_0_), channel_id=1, source_target_pairs={{0,4},{1,5},{2,6},{3,7},{4,0},{5,1},{6,2},{7,3},{8,12},{9,13},{10,... | collective-permute-start | bytes 1179656 | tf_op jit(solution)/shard_map/ppermute | solution.py:208
  46.4 2.8 %collective-permute-start.2 = (bf16[128,1536]{1,0:T(8,128)(2,1)S(1)}, bf16[128,1536]{1,0:T(8,128)(2,1)S(1)}, u32[]{:S(2)}, u32[]{:S(2)}) collective-permute-start(bf16[128,1536]{1,0:T(8,128)(2,1)S(1)} %maximum_select_fusion.refs_0_), channel_id=1, source_target_pairs={{0,2},{1,3},{2,4},{3,5},{4,6},{5,7},{6,0},{7,1},{8,10},{9,11},{10,... | collective-permute-start | bytes 1179656 | tf_op jit(solution)/shard_map/ppermute | solution.py:209
  49.2 11.2 %collective-permute-done.refs_1_ = bf16[128,1536]{1,0:T(8,128)(2,1)S(1)} collective-permute-done((bf16[128,1536]{1,0:T(8,128)(2,1)S(1)}, bf16[128,1536]{1,0:T(8,128)(2,1)S(1)}, u32[]{:S(2)}, u32[]{:S(2)}) %collective-permute-start) | collective-permute-done | bytes 393248 | tf_op jit(solution)/shard_map/ppermute | solution.py:207
  61.1 4.8 %collective-permute-done.2.refs_3_ = bf16[128,1536]{1,0:T(8,128)(2,1)S(1)} collective-permute-done((bf16[128,1536]{1,0:T(8,128)(2,1)S(1)}, bf16[128,1536]{1,0:T(8,128)(2,1)S(1)}, u32[]{:S(2)}, u32[]{:S(2)}) %collective-permute-start.2) | collective-permute-done | bytes 393248 | tf_op jit(solution)/shard_map/ppermute | solution.py:209
  66.7 1.0 copy-done.1
  67.7 1.0 copy-done.3
  68.8 1.9 %collective-permute-start.3 = (bf16[512,1536]{1,0:T(8,128)(2,1)S(1)}, bf16[512,1536]{1,0:T(8,128)(2,1)}, u32[]{:S(2)}, u32[]{:S(2)}) collective-permute-start(bf16[512,1536]{1,0:T(8,128)(2,1)S(1)} %by_place.1.own), channel_id=1, source_target_pairs={{0,1},{1,0},{2,3},{3,2},{4,5},{5,4},{6,7},{7,6},{8,9},{9,8},{10,11... | collective-permute-start | bytes 4718600 | tf_op jit(solution)/shard_map/ppermute | solution.py:212
  70.8 7.3 %collective-permute-start.4 = (bf16[384,768]{1,0:T(8,128)(2,1)}, bf16[384,768]{1,0:T(8,128)(2,1)S(1)}, u32[]{:S(2)}, u32[]{:S(2)}) collective-permute-start(bf16[384,768]{1,0:T(8,128)(2,1)} %bitcast.2.u0), channel_id=1, source_target_pairs={{0,448},{8,456},{16,464},{24,472},{32,480},{40,488},{48,496},{56,5... | collective-permute-start | bytes 1769480 | tf_op jit(solution)/shard_map/ppermute | solution.py:216
  78.1 4.3 %collective-permute-start.5 = (bf16[384,768]{1,0:T(8,128)(2,1)}, bf16[384,768]{1,0:T(8,128)(2,1)}, u32[]{:S(2)}, u32[]{:S(2)}) collective-permute-start(bf16[384,768]{1,0:T(8,128)(2,1)} %bitcast.2.u0), channel_id=1, source_target_pairs={{0,128},{8,136},{16,144},{24,152},{32,160},{40,168},{48,176},{56,1... | collective-permute-start | bytes 1769480 | tf_op jit(solution)/shard_map/ppermute | solution.py:217
  82.4 1.9 %collective-permute-start.6 = (bf16[384,768]{1,0:T(8,128)(2,1)}, bf16[384,768]{1,0:T(8,128)(2,1)}, u32[]{:S(2)}, u32[]{:S(2)}) collective-permute-start(bf16[384,768]{1,0:T(8,128)(2,1)} %bitcast.2.u0), channel_id=1, source_target_pairs={{0,64},{8,72},{16,80},{24,88},{32,96},{40,104},{48,112},{56,120},{... | collective-permute-start | bytes 1769480 | tf_op jit(solution)/shard_map/ppermute | solution.py:218
  84.4 5.1 %collective-permute-start.8 = (bf16[384,768]{1,0:T(8,128)(2,1)S(1)}, bf16[384,768]{1,0:T(8,128)(2,1)S(1)}, u32[]{:S(2)}, u32[]{:S(2)}) collective-permute-start(bf16[384,768]{1,0:T(8,128)(2,1)S(1)} %get-tuple-element.11), channel_id=1, source_target_pairs={{0,448},{8,456},{16,464},{24,472},{32,480},{40,488},{48,496},{56,5... | collective-permute-start | bytes 1769480 | tf_op jit(solution)/shard_map/ppermute | solution.py:223
  89.6 3.8 %collective-permute-done.4.u1 = bf16[384,768]{1,0:T(8,128)(2,1)S(1)} collective-permute-done((bf16[384,768]{1,0:T(8,128)(2,1)}, bf16[384,768]{1,0:T(8,128)(2,1)S(1)}, u32[]{:S(2)}, u32[]{:S(2)}) %collective-permute-start.4) | collective-permute-done | bytes 589856 | tf_op jit(solution)/shard_map/ppermute | solution.py:216
  93.4 16.6 %collective-permute-start.9 = (bf16[384,768]{1,0:T(8,128)(2,1)S(1)}, bf16[384,768]{1,0:T(8,128)(2,1)S(1)}, u32[]{:S(2)}, u32[]{:S(2)}) collective-permute-start(bf16[384,768]{1,0:T(8,128)(2,1)S(1)} %get-tuple-element.11), channel_id=1, source_target_pairs={{0,64},{8,72},{16,80},{24,88},{32,96},{40,104},{48,112},{56,120},{... | collective-permute-start | bytes 1769480 | tf_op jit(solution)/shard_map/ppermute | solution.py:223
  110.6 6.8 %hidden.1 = (bf16[1024,768]{1,0:T(8,128)(2,1)S(1)}, bf16[512,768]{1,0:T(8,128)(2,1)S(1)}) custom-call(bf16[512,1536]{1,0:T(8,128)(2,1)} %collective-permute-done.3.other, bf16[512,1536]{1,0:T(8,128)(2,1)S(1)} %by_place.1.own, bf16[384,768]{1,0:T(8,128)(2,1)} %bitcast.2.u0, bf16[384,768]{1,0:T(8,128)(2,1)S(1)} %collective-permute-done.4.u1, ...), custom_call_target="tpu_custom_call" | custom-call | flops 2415919104 | bytes 9043968 | tf_op jit(solution)/shard_map/hidden/pallas_call | solution.py:162
  117.4 1.9 %collective-permute-start.11 = (bf16[512,768]{1,0:T(8,128)(2,1)S(1)}, bf16[512,768]{1,0:T(8,128)(2,1)S(1)}, u32[]{:S(2)}, u32[]{:S(2)}) collective-permute-start(bf16[512,768]{1,0:T(8,128)(2,1)S(1)} %get-tuple-element.12), channel_id=1, source_target_pairs={{0,1},{1,0},{2,3},{3,2},{4,5},{5,4},{6,7},{7,6},{8,9},{9,8},{10,11... | collective-permute-start | bytes 2359304 | tf_op jit(solution)/shard_map/ppermute | solution.py:234
  119.3 3.7 %collective-permute-done.9 = bf16[384,768]{1,0:T(8,128)(2,1)S(1)} collective-permute-done((bf16[384,768]{1,0:T(8,128)(2,1)S(1)}, bf16[384,768]{1,0:T(8,128)(2,1)S(1)}, u32[]{:S(2)}, u32[]{:S(2)}) %collective-permute-start.9) | collective-permute-done | bytes 589856 | tf_op jit(solution)/shard_map/ppermute | solution.py:223
  123.1 1.7 %convolution_convert_fusion = bf16[512,768]{1,0:T(8,128)(2,1)} fusion(bf16[768,768]{1,0:T(8,128)(2,1)S(1)} %pad_maximum_fusion, bf16[1024,768]{1,0:T(8,128)(2,1)S(1)} %get-tuple-element.10), kind=kOutput, calls=%fused_computation.2 | convolution fusion | flops 604372992 | bytes 2752512 | tf_op jit(solution)/shard_map/dot_general | solution.py:231
  124.8 1.9 %collective-permute-start.10 = (bf16[512,768]{1,0:T(8,128)(2,1)}, bf16[512,768]{1,0:T(8,128)(2,1)}, u32[]{:S(2)}, u32[]{:S(2)}) collective-permute-start(bf16[512,768]{1,0:T(8,128)(2,1)} %convolution_convert_fusion), channel_id=1, source_target_pairs={{0,1},{1,0},{2,3},{3,2},{4,5},{5,4},{6,7},{7,6},{8,9},{9,8},{10,11... | collective-permute-start | bytes 2359304 | tf_op jit(solution)/shard_map/ppermute | solution.py:234
  126.7 1.7 %add_convert_fusion = bf16[512,768]{1,0:T(8,128)(2,1)} fusion(bf16[512,768]{1,0:T(8,128)(2,1)S(1)} %collective-permute-done.11, bf16[768,768]{1,0:T(8,128)(2,1)S(1)} %get-tuple-element.9.down_ref, bf16[1024,768]{1,0:T(8,128)(2,1)S(1)} %get-tuple-element.10), kind=kOutput, calls=%fused_computation | convolution fusion | flops 605159424 | bytes 3538944 | tf_op jit(solution)/shard_map/dot_general | solution.py:231
  128.5 3.6 %all-to-all-start.3 = ((bf16[4,128,768]{2,1,0:T(8,128)(2,1)}), bf16[4,128,768]{2,1,0:T(8,128)(2,1)S(1)}, u32[]{:S(2)}, u32[]{:S(2)}) async-start(bf16[4,128,768]{2,1,0:T(8,128)(2,1)} %bitcast.12), calls=%async_computation.3 | async-start | bytes 1572864 | tf_op jit(solution)/shard_map/all_to_all | solution.py:36
  132.1 2.8 %add_convert_fusion.1 = bf16[512,768]{1,0:T(8,128)(2,1)} fusion(bf16[512,768]{1,0:T(8,128)(2,1)} %collective-permute-done.10, bf16[768,768]{1,0:T(8,128)(2,1)S(1)} %pad_maximum_fusion, bf16[1024,768]{1,0:T(8,128)(2,1)S(1)} %copy-done.7), kind=kOutput, calls=%fused_computation.1 | convolution fusion | flops 605159424 | bytes 3538944 | tf_op jit(solution)/shard_map/dot_general | solution.py:231
  135.0 10.3 %all-to-all-done.3 = bf16[4,128,768]{2,1,0:T(8,128)(2,1)S(1)} async-done(((bf16[4,128,768]{2,1,0:T(8,128)(2,1)}), bf16[4,128,768]{2,1,0:T(8,128)(2,1)S(1)}, u32[]{:S(2)}, u32[]{:S(2)}) %all-to-all-start.3) | async-done | bytes 786464 | tf_op jit(solution)/shard_map/all_to_all | solution.py:36
  145.3 3.5 %all-to-all-start.2 = ((bf16[4,128,768]{2,1,0:T(8,128)(2,1)}), bf16[4,128,768]{2,1,0:T(8,128)(2,1)S(1)}, u32[]{:S(2)}, u32[]{:S(2)}) async-start(bf16[4,128,768]{2,1,0:T(8,128)(2,1)} %bitcast.11), calls=%async_computation.2 | async-start | bytes 1572864 | tf_op jit(solution)/shard_map/all_to_all | solution.py:36
  149.0 12.2 %all-to-all-done.2 = bf16[4,128,768]{2,1,0:T(8,128)(2,1)S(1)} async-done(((bf16[4,128,768]{2,1,0:T(8,128)(2,1)}), bf16[4,128,768]{2,1,0:T(8,128)(2,1)S(1)}, u32[]{:S(2)}, u32[]{:S(2)}) %all-to-all-start.2) | async-done | bytes 786464 | tf_op jit(solution)/shard_map/all_to_all | solution.py:36
  161.3 1.0 maximum_select_fusion.3
  (42 shorter events, 5.3 us)
Async XLA Ops:
  0.0 16.6 %copy-start.9 = (f32[1536]{0:T(1024)S(1)}, f32[1536]{0:T(1024)}, u32[]{:S(2)}) copy-start(f32[1536]{0:T(1024)} %param.7) | copy-start | bytes 18436
  1.0 15.9 %collective-permute-start.7 = (bf16[48,768]{1,0:T(8,128)(2,1)S(1)}, bf16[48,768]{1,0:T(8,128)(2,1)S(1)}, u32[]{:S(2)}, u32[]{:S(2)}) collective-permute-start(bf16[48,768]{1,0:T(8,128)(2,1)S(1)} %fusion.6.refs_0_), channel_id=1, source_target_pairs={{0,128},{8,136},{16,144},{24,152},{32,160},{40,168},{48,176},{56,1... | collective-permute-start | bytes 221192 | tf_op jit(solution)/shard_map/ppermute | solution.py:198
  7.1 0.9 copy-start.4
  8.0 8.4 %copy-start.8 = (bf16[128,1536]{1,0:T(8,128)(2,1)S(1)}, bf16[128,1536]{1,0:T(8,128)(2,1)}, u32[]{:S(2)}) copy-start(bf16[128,1536]{1,0:T(8,128)(2,1)} %param.6) | copy-start | bytes 1179652
  8.9 24.8 %all-to-all-start = ((bf16[8,48,768]{2,1,0:T(8,128)(2,1)}), bf16[8,48,768]{2,1,0:T(8,128)(2,1)}, u32[]{:S(2)}, u32[]{:S(2)}) async-start(bf16[8,48,768]{2,1,0:T(8,128)(2,1)} %bitcast.1), calls=%async_computation | async-start | bytes 1179648 | tf_op jit(solution)/shard_map/all_to_all | solution.py:36
  33.7 50.6 %all-to-all-start.1 = ((bf16[8,2,48,768]{3,2,1,0:T(8,128)(2,1)}), bf16[8,2,48,768]{3,2,1,0:T(8,128)(2,1)S(1)}, u32[]{:S(2)}, u32[]{:S(2)}) async-start(bf16[8,2,48,768]{3,2,1,0:T(8,128)(2,1)} %copies.3), calls=%async_computation.1 | async-start | bytes 2359296 | tf_op jit(solution)/shard_map/all_to_all | solution.py:36
  39.0 21.4 %collective-permute-start = (bf16[128,1536]{1,0:T(8,128)(2,1)S(1)}, bf16[128,1536]{1,0:T(8,128)(2,1)S(1)}, u32[]{:S(2)}, u32[]{:S(2)}) collective-permute-start(bf16[128,1536]{1,0:T(8,128)(2,1)S(1)} %maximum_select_fusion.refs_0_), channel_id=1, source_target_pairs={{0,6},{1,7},{2,0},{3,1},{4,2},{5,3},{6,4},{7,5},{8,14},{9,15},{10,... | collective-permute-start | bytes 1179656 | tf_op jit(solution)/shard_map/ppermute | solution.py:207
  43.7 16.7 %collective-permute-start.1 = (bf16[128,1536]{1,0:T(8,128)(2,1)S(1)}, bf16[128,1536]{1,0:T(8,128)(2,1)S(1)}, u32[]{:S(2)}, u32[]{:S(2)}) collective-permute-start(bf16[128,1536]{1,0:T(8,128)(2,1)S(1)} %maximum_select_fusion.refs_0_), channel_id=1, source_target_pairs={{0,4},{1,5},{2,6},{3,7},{4,0},{5,1},{6,2},{7,3},{8,12},{9,13},{10,... | collective-permute-start | bytes 1179656 | tf_op jit(solution)/shard_map/ppermute | solution.py:208
  46.4 19.6 %collective-permute-start.2 = (bf16[128,1536]{1,0:T(8,128)(2,1)S(1)}, bf16[128,1536]{1,0:T(8,128)(2,1)S(1)}, u32[]{:S(2)}, u32[]{:S(2)}) collective-permute-start(bf16[128,1536]{1,0:T(8,128)(2,1)S(1)} %maximum_select_fusion.refs_0_), channel_id=1, source_target_pairs={{0,2},{1,3},{2,4},{3,5},{4,6},{5,7},{6,0},{7,1},{8,10},{9,11},{10,... | collective-permute-start | bytes 1179656 | tf_op jit(solution)/shard_map/ppermute | solution.py:209
  60.4 0.7 copy-start
  66.0 0.8 copy-start.2
  66.7 1.0 copy-start.1
  67.7 1.0 copy-start.3
  68.7 41.9 %copy-start.5 = (f32[1,768]{1,0:T(1,128)S(1)}, f32[1,768]{1,0:T(1,128)}, u32[]{:S(2)}) copy-start(f32[1,768]{1,0:T(1,128)} %scale.1) | copy-start | bytes 9220
  68.8 41.8 %collective-permute-start.3 = (bf16[512,1536]{1,0:T(8,128)(2,1)S(1)}, bf16[512,1536]{1,0:T(8,128)(2,1)}, u32[]{:S(2)}, u32[]{:S(2)}) collective-permute-start(bf16[512,1536]{1,0:T(8,128)(2,1)S(1)} %by_place.1.own), channel_id=1, source_target_pairs={{0,1},{1,0},{2,3},{3,2},{4,5},{5,4},{6,7},{7,6},{8,9},{9,8},{10,11... | collective-permute-start | bytes 4718600 | tf_op jit(solution)/shard_map/ppermute | solution.py:212
  70.8 22.6 %collective-permute-start.4 = (bf16[384,768]{1,0:T(8,128)(2,1)}, bf16[384,768]{1,0:T(8,128)(2,1)S(1)}, u32[]{:S(2)}, u32[]{:S(2)}) collective-permute-start(bf16[384,768]{1,0:T(8,128)(2,1)} %bitcast.2.u0), channel_id=1, source_target_pairs={{0,448},{8,456},{16,464},{24,472},{32,480},{40,488},{48,496},{56,5... | collective-permute-start | bytes 1769480 | tf_op jit(solution)/shard_map/ppermute | solution.py:216
  78.1 31.9 %collective-permute-start.5 = (bf16[384,768]{1,0:T(8,128)(2,1)}, bf16[384,768]{1,0:T(8,128)(2,1)}, u32[]{:S(2)}, u32[]{:S(2)}) collective-permute-start(bf16[384,768]{1,0:T(8,128)(2,1)} %bitcast.2.u0), channel_id=1, source_target_pairs={{0,128},{8,136},{16,144},{24,152},{32,160},{40,168},{48,176},{56,1... | collective-permute-start | bytes 1769480 | tf_op jit(solution)/shard_map/ppermute | solution.py:217
  82.4 28.2 %collective-permute-start.6 = (bf16[384,768]{1,0:T(8,128)(2,1)}, bf16[384,768]{1,0:T(8,128)(2,1)}, u32[]{:S(2)}, u32[]{:S(2)}) collective-permute-start(bf16[384,768]{1,0:T(8,128)(2,1)} %bitcast.2.u0), channel_id=1, source_target_pairs={{0,64},{8,72},{16,80},{24,88},{32,96},{40,104},{48,112},{56,120},{... | collective-permute-start | bytes 1769480 | tf_op jit(solution)/shard_map/ppermute | solution.py:218
  84.4 34.8 %collective-permute-start.8 = (bf16[384,768]{1,0:T(8,128)(2,1)S(1)}, bf16[384,768]{1,0:T(8,128)(2,1)S(1)}, u32[]{:S(2)}, u32[]{:S(2)}) collective-permute-start(bf16[384,768]{1,0:T(8,128)(2,1)S(1)} %get-tuple-element.11), channel_id=1, source_target_pairs={{0,448},{8,456},{16,464},{24,472},{32,480},{40,488},{48,496},{56,5... | collective-permute-start | bytes 1769480 | tf_op jit(solution)/shard_map/ppermute | solution.py:223
  93.4 29.6 %collective-permute-start.9 = (bf16[384,768]{1,0:T(8,128)(2,1)S(1)}, bf16[384,768]{1,0:T(8,128)(2,1)S(1)}, u32[]{:S(2)}, u32[]{:S(2)}) collective-permute-start(bf16[384,768]{1,0:T(8,128)(2,1)S(1)} %get-tuple-element.11), channel_id=1, source_target_pairs={{0,64},{8,72},{16,80},{24,88},{32,96},{40,104},{48,112},{56,120},{... | collective-permute-start | bytes 1769480 | tf_op jit(solution)/shard_map/ppermute | solution.py:223
  117.3 9.4 %copy-start.6 = (bf16[1024,768]{1,0:T(8,128)(2,1)}, bf16[1024,768]{1,0:T(8,128)(2,1)S(1)}, u32[]{:S(2)}) copy-start(bf16[1024,768]{1,0:T(8,128)(2,1)S(1)} %get-tuple-element.10) | copy-start | bytes 4718596
  117.4 9.4 %collective-permute-start.11 = (bf16[512,768]{1,0:T(8,128)(2,1)S(1)}, bf16[512,768]{1,0:T(8,128)(2,1)S(1)}, u32[]{:S(2)}, u32[]{:S(2)}) collective-permute-start(bf16[512,768]{1,0:T(8,128)(2,1)S(1)} %get-tuple-element.12), channel_id=1, source_target_pairs={{0,1},{1,0},{2,3},{3,2},{4,5},{5,4},{6,7},{7,6},{8,9},{9,8},{10,11... | collective-permute-start | bytes 2359304 | tf_op jit(solution)/shard_map/ppermute | solution.py:234
  124.8 7.3 %collective-permute-start.10 = (bf16[512,768]{1,0:T(8,128)(2,1)}, bf16[512,768]{1,0:T(8,128)(2,1)}, u32[]{:S(2)}, u32[]{:S(2)}) collective-permute-start(bf16[512,768]{1,0:T(8,128)(2,1)} %convolution_convert_fusion), channel_id=1, source_target_pairs={{0,1},{1,0},{2,3},{3,2},{4,5},{5,4},{6,7},{7,6},{8,9},{9,8},{10,11... | collective-permute-start | bytes 2359304 | tf_op jit(solution)/shard_map/ppermute | solution.py:234
  128.5 3.6 %copy-start.7 = (bf16[1024,768]{1,0:T(8,128)(2,1)S(1)}, bf16[1024,768]{1,0:T(8,128)(2,1)}, u32[]{:S(2)}) copy-start(bf16[1024,768]{1,0:T(8,128)(2,1)} %copy-done.6) | copy-start | bytes 4718596
  128.5 16.8 %all-to-all-start.3 = ((bf16[4,128,768]{2,1,0:T(8,128)(2,1)}), bf16[4,128,768]{2,1,0:T(8,128)(2,1)S(1)}, u32[]{:S(2)}, u32[]{:S(2)}) async-start(bf16[4,128,768]{2,1,0:T(8,128)(2,1)} %bitcast.12), calls=%async_computation.3 | async-start | bytes 1572864 | tf_op jit(solution)/shard_map/all_to_all | solution.py:36
  145.3 15.8 %all-to-all-start.2 = ((bf16[4,128,768]{2,1,0:T(8,128)(2,1)}), bf16[4,128,768]{2,1,0:T(8,128)(2,1)S(1)}, u32[]{:S(2)}, u32[]{:S(2)}) async-start(bf16[4,128,768]{2,1,0:T(8,128)(2,1)} %bitcast.11), calls=%async_computation.2 | async-start | bytes 1572864 | tf_op jit(solution)/shard_map/all_to_all | solution.py:36

commit v5 on v4

--- a/solution.py
+++ b/solution.py
@@ -45,6 +45,7 @@
 
 
 VMEM = pl.BlockSpec(memory_space=pltpu.VMEM)
+HBM = pl.BlockSpec(memory_space=pltpu.HBM)
 SMEM = pl.BlockSpec(memory_space=pltpu.SMEM)
 
 
@@ -97,10 +98,18 @@
 
 
 def by_place_kernel(x_ref, *refs):
-    *blocks, out = refs
+    *blocks, out, sems = refs
     rows = blocks[0].shape[0]
-    for k, block in enumerate(blocks):
-        out[pl.ds(pl.multiple_of((x_ref[0] + k) % X * rows, rows), rows), :] = block[...]
+    fetches = [
+        pltpu.make_async_copy(
+            block, out.at[pl.ds(pl.multiple_of((x_ref[0] + k) % X * rows, rows), rows)], sems.at[k]
+        )
+        for k, block in enumerate(blocks)
+    ]
+    for fetch in fetches:
+        fetch.start()
+    for fetch in fetches:
+        fetch.wait()
 
 
 def by_place(x, blocks):
@@ -108,10 +117,11 @@
     return pl.pallas_call(
         by_place_kernel,
         out_shape=jax.ShapeDtypeStruct((X * rows, columns), blocks[0].dtype),
-        in_specs=[SMEM] + [VMEM] * X,
+        in_specs=[SMEM] + [HBM] * X,
         out_specs=VMEM,
+        scratch_shapes=[pltpu.SemaphoreType.DMA((X,))],
         cost_estimate=cost(1 << 28, *blocks, *blocks),
-        compiler_params=pltpu.CompilerParams(vmem_limit_bytes=8 << 20),
+        compiler_params=pltpu.CompilerParams(vmem_limit_bytes=4 << 20),
         name="by_place",
     )(x[None], *blocks)
 
@@ -119,70 +129,105 @@
 TILE = 256
 
 
-def hidden_kernel(half, other, own, u0, u1, u2, u3, scale, down_ref, hidden, terms, up, down, sems):
-    step = pl.program_id(0)
-
-    @pl.when(step == 0)
+def fetched(sources, target, sems):
+    @pl.when(pl.program_id(0) == 0)
     def _():
-        width = u0.shape[0]
+        rows = sources[0].shape[0]
         fetches = [
-            pltpu.make_async_copy(block, up.at[pl.ds(k * width, width)], sems.at[k])
-            for k, block in enumerate((u0, u1, u2, u3))
+            pltpu.make_async_copy(source, target.at[pl.ds(k * rows, rows)], sems.at[k])
+            for k, source in enumerate(sources)
         ]
-        fetches.append(pltpu.make_async_copy(down_ref, down, sems.at[len(fetches)]))
         for fetch in fetches:
             fetch.start()
         for fetch in fetches:
             fetch.wait()
 
-    def hidden_of(rows):
-        pre = jnp.dot(rows[...], up[...], preferred_element_type=F32)
-        return jnp.square(jnp.maximum(pre * scale[...], 0.0)).astype(BF16)
-
-    @pl.when(step < half)
+
+def early_kernel(half, other, own, u0, u1, u3, early, up, sems):
+    fetched((u0, u1, u3), up, sems)
+    width, columns = u0.shape
+
+    def write(rows):
+        pre = jnp.dot(rows[:, : 2 * width], up[: 2 * width], preferred_element_type=F32)
+        pre += jnp.dot(rows[:, 3 * width :], up[2 * width :], preferred_element_type=F32)
+        early[:, :columns] = pre.astype(early.dtype)
+        early[:, columns:] = rows[:, 2 * width : 3 * width]
+
+    @pl.when(pl.program_id(0) < half)
     def _():
-        tile = hidden_of(other)
-        hidden[...] = tile
-        terms[...] = lax.dot_general(
-            tile, down[...], (((1,), (1,)), ((), ())), preferred_element_type=F32
-        ).astype(BF16)
-
-    @pl.when(step >= half)
+        write(other)
+
+    @pl.when(pl.program_id(0) >= half)
     def _():
-        hidden[...] = hidden_of(own)
-
-
-def hidden_of(other, own, up, scale, down):
+        write(own)
+
+
+def early_of(other, own, blocks):
     rows, d = own.shape
-    _, columns = up[0].shape
+    width, columns = blocks[0].shape
     half = rows // TILE
-    hidden = jax.ShapeDtypeStruct((2 * rows, columns), BF16)
-    terms = jax.ShapeDtypeStruct((rows, down.shape[0]), BF16)
-    anywhere = pl.BlockSpec(memory_space=pl.ANY)
-    return pl.pallas_call(
-        functools.partial(hidden_kernel, half),
+    shape = (2 * rows, columns + width)
+    return pl.pallas_call(
+        functools.partial(early_kernel, half),
         grid=(2 * half,),
-        out_shape=[hidden, terms],
+        out_shape=pltpu.HBM(shape, BF16),
         in_specs=[
             pl.BlockSpec((TILE, d), lambda i: (jnp.minimum(i, half - 1), 0)),
             pl.BlockSpec((TILE, d), lambda i: (jnp.maximum(i - half, 0), 0)),
-            *([anywhere] * ZLO),
-            pl.BlockSpec((1, columns), lambda i: (0, 0)),
-            anywhere,
+            *([HBM] * len(blocks)),
         ],
-        out_specs=[
-            pl.BlockSpec((TILE, columns), lambda i: (i, 0)),
-            pl.BlockSpec((TILE, down.shape[0]), lambda i: (jnp.minimum(i, half - 1), 0)),
+        out_specs=pl.BlockSpec((TILE, shape[1]), lambda i: (i, 0)),
+        scratch_shapes=[
+            pltpu.VMEM((len(blocks) * width, columns), BF16),
+            pltpu.SemaphoreType.DMA((len(blocks),)),
         ],
+        compiler_params=pltpu.CompilerParams(vmem_limit_bytes=16 << 20),
+        cost_estimate=cost(4 * rows * 3 * width * columns, own, other, *blocks),
+        name="early",
+    )(other, own, *blocks)
+
+
+def late_kernel(early, u2, scale, hidden, tiles, up, sems):
+    step, steps = pl.program_id(0), early.shape[0] // TILE
+    columns = hidden.shape[1]
+
+    def fetch(i):
+        rows = pl.ds(i * TILE if isinstance(i, int) else pl.multiple_of(i * TILE, TILE), TILE)
+        return pltpu.make_async_copy(early.at[rows], tiles.at[rows], sems.at[i])
+
+    @pl.when(step == 0)
+    def _():
+        block = pltpu.make_async_copy(u2, up, sems.at[steps])
+        block.start()
+        for i in range(steps):
+            fetch(i).start()
+        block.wait()
+
+    fetch(step).wait()
+    tile = tiles.at[pl.ds(pl.multiple_of(step * TILE, TILE), TILE)]
+    pre = jnp.dot(tile[:, columns:], up[...], preferred_element_type=F32) + tile[:, :columns].astype(F32)
+    hidden[...] = jnp.square(jnp.maximum(pre * scale[...], 0.0)).astype(BF16)
+
+
+def late_of(early, block, scale):
+    width, columns = block.shape
+    steps = early.shape[0] // TILE
+    out = jax.ShapeDtypeStruct((early.shape[0], columns), BF16)
+    return pl.pallas_call(
+        late_kernel,
+        grid=(steps,),
+        out_shape=out,
+        in_specs=[HBM, HBM, pl.BlockSpec((1, columns), lambda i: (0, 0))],
+        out_specs=pl.BlockSpec((TILE, columns), lambda i: (i, 0)),
         scratch_shapes=[
-            pltpu.VMEM((d, columns), BF16),
-            pltpu.VMEM(down.shape, BF16),
-            pltpu.SemaphoreType.DMA((ZLO + 1,)),
+            pltpu.VMEM(early.shape, BF16),
+            pltpu.VMEM((width, columns), BF16),
+            pltpu.SemaphoreType.DMA((steps + 1,)),
         ],
-        compiler_params=pltpu.CompilerParams(vmem_limit_bytes=24 << 20),
-        cost_estimate=cost(4 * rows * d * columns, own, other, *up, down, hidden, terms),
-        name="hidden",
-    )(other, own, *up, scale, down)
+        compiler_params=pltpu.CompilerParams(vmem_limit_bytes=12 << 20),
+        cost_estimate=cost(2 * early.shape[0] * width * columns, early, block, out),
+        name="late",
+    )(early, block, scale)
 
 
 def body(tokens, norm_gain, up_weight, up_scale, down_weight, down_scale):
@@ -211,12 +256,10 @@
     own = by_place(x, near)
     other = lax.ppermute(own, "tp", OTHER_CORE)
 
-    up = [
-        up_own,
-        lax.ppermute(up_own, PLANE, FROM_NEXT),
-        lax.ppermute(up_own, PLANE, FROM_TWO),
-        lax.ppermute(up_own, PLANE, FROM_LAST),
-    ]
+    up_next = lax.ppermute(up_own, PLANE, FROM_NEXT)
+    up_last = lax.ppermute(up_own, PLANE, FROM_LAST)
+    up_two = lax.ppermute(up_own, PLANE, FROM_TWO)
+
     copies = copies_of([down_piece, down_two])
     down_own, down_a = split(swapped(copies, "fs", ROW_GROUPS))
     down_b = jnp.concatenate(
@@ -224,7 +267,8 @@
     )
     down_b = lax.optimization_barrier(down_b)
 
-    hidden, for_other = hidden_of(other, own, up, up_scale, down_a)
+    early = early_of(other, own, (up_own, up_next, up_last))
+    hidden = late_of(early, up_two, up_scale)
     hidden_other, hidden_own = hidden[: X * rows], hidden[X * rows :]
 
     def terms(hidden, down):
@@ -236,7 +280,7 @@
         arrived = swapped(pair.reshape(X, rows, -1), "tp", X_GROUPS)
         return arrived.astype(F32).sum(axis=0).astype(BF16)
 
-    out_a = chunk(down_a, for_other)
+    out_a = chunk(down_a, terms(hidden_other, down_a).astype(BF16))
     out_b = chunk(down_b, terms(hidden_other, down_b).astype(BF16))
     summed = jnp.concatenate(
         [out_a[:, :width], out_b[:, :width], out_a[:, width:], out_b[:, width:]], 1

time: 163 us -> 163 us (level)
  starting transfers between devices: 76.8 us -> 63.8 us
  local copies, waits for them, and re-layouts: 4.56 us -> 11.1 us
  Pallas kernels: 8.98 us -> 11.8 us
  waiting for transfers between devices: 62.3 us -> 64.7 us
    ppermute x3, waiting for transfers between devices: 4.43 us -> 20.2 us  [the longest x1 17.2 us: body(): up_next = lax.ppermute(up_own, PLANE, FROM_NEXT)]
    ppermute x1, starting transfers between devices: 16.6 us -> 1.91 us  [body(): lax.ppermute(down_own, PLANE, FROM_LAST)]
    all_to_all x4, waiting for transfers between devices: 38.1 us -> 24.5 us  [swapped(): lax.all_to_all(blocks, axis, 0, 0, axis_index_groups=groups, tiled=True)]
    ppermute x1, waiting for transfers between devices: 0.01 us -> 5.36 us  [body(): down_two = lax.ppermute(down_piece, PLANE, FROM_TWO)]
    unnamed x20 -> x32, local copies, waits for them, and re-layouts: 4.42 us -> 9.56 us
    ppermute x1, waiting for transfers between devices: 3.72 us -> 0.01 us  [body(): lax.ppermute(down_own, PLANE, FROM_LAST)]
    pallas_call x1 -> x2, Pallas kernels: 6.76 us -> 8.92 us  [the longest x1 6.25 us: early_of(): pl.pallas_call(functools.partial(early_kernel, half), grid=(2 * half,), o...]
    ppermute x1, starting transfers between devices: 6.09 us -> 4.4 us  [body(): down_two = lax.ppermute(down_piece, PLANE, FROM_TWO)]
  transfers between devices with their start and end apart: 16 -> 16, of which waited for: 8 -> 8; matrix products, arithmetic and copies ran while one was open for 4% -> 6% of each run, Pallas kernels for 6% -> 7%
where the time goes in v5:
time: 163 us; the launch traced here: 162 us
  waiting for transfers between devices  64.7 us (40%)
  starting transfers between devices  63.8 us (39%)
  Pallas kernels  11.8 us (7%)
  local copies, waits for them, and re-layouts  11.1 us (7%)
  matrix products  7.11 us (4%)
  other arithmetic  3.02 us (2%)
    all_to_all x4, waiting for transfers between devices, swapped(): lax.all_to_all(blocks, axis, 0, 0, axis_index_groups=groups, tiled=True)  24.5 us
    all_to_all x4, starting transfers between devices, swapped(): lax.all_to_all(blocks, axis, 0, 0, axis_index_groups=groups, tiled=True)  21.1 us
    ppermute x1, waiting for transfers between devices, body(): up_next = lax.ppermute(up_own, PLANE, FROM_NEXT)  17.2 us
    ppermute x1, starting transfers between devices, body(): up_next = lax.ppermute(up_own, PLANE, FROM_NEXT)  10.9 us
    ppermute x1, waiting for transfers between devices, body(): lax.ppermute(normed, 'tp', X_NEXT)  10.4 us
    unnamed x32, local copies, waits for them, and re-layouts  9.56 us
    dot_general x4, matrix products, terms(): lax.dot_general(hidden, down, (((1,), (1,)), ((), ())), preferred_element...  7.11 us
    pallas_call x1, Pallas kernels, early_of(): pl.pallas_call(functools.partial(early_kernel, half), grid=(2 * half,), o...  6.25 us
  transfers between devices with their start and end apart: 16, of which 8 were waited for; matrix products, arithmetic and copies ran while one was open for 6% of the time, Pallas kernels for 7%

profile of v5, /device:TPU:8, one launch (start us, length us, event | category | flops | bytes accessed | tf_op | source)
XLA Modules:
  0.0 161.8 jit_solution(14207784928731417923)
XLA Ops:
  1.8 9.2 %all-to-all-start = ((bf16[8,48,768]{2,1,0:T(8,128)(2,1)}), bf16[8,48,768]{2,1,0:T(8,128)(2,1)S(1)}, u32[]{:S(2)}, u32[]{:S(2)}) async-start(bf16[8,48,768]{2,1,0:T(8,128)(2,1)} %bitcast.1), calls=%async_computation | async-start | bytes 1179648 | tf_op jit(solution)/shard_map/all_to_all | solution.py:36
  11.1 4.4 %collective-permute-start.7 = (bf16[48,768]{1,0:T(8,128)(2,1)S(1)}, bf16[48,768]{1,0:T(8,128)(2,1)S(1)}, u32[]{:S(2)}, u32[]{:S(2)}) collective-permute-start(bf16[48,768]{1,0:T(8,128)(2,1)S(1)} %fusion.7.refs_0_), channel_id=1, source_target_pairs={{0,128},{8,136},{16,144},{24,152},{32,160},{40,168},{48,176},{56,1... | collective-permute-start | bytes 221192 | tf_op jit(solution)/shard_map/ppermute | solution.py:243
  17.3 5.4 %collective-permute-done.7.refs_1_ = bf16[48,768]{1,0:T(8,128)(2,1)S(1)} collective-permute-done((bf16[48,768]{1,0:T(8,128)(2,1)S(1)}, bf16[48,768]{1,0:T(8,128)(2,1)S(1)}, u32[]{:S(2)}, u32[]{:S(2)}) %collective-permute-start.7) | collective-permute-done | bytes 73760 | tf_op jit(solution)/shard_map/ppermute | solution.py:243
  22.7 1.1 copies.3
  23.8 3.0 %all-to-all-done = bf16[8,48,768]{2,1,0:T(8,128)(2,1)S(1)} async-done(((bf16[8,48,768]{2,1,0:T(8,128)(2,1)}), bf16[8,48,768]{2,1,0:T(8,128)(2,1)S(1)}, u32[]{:S(2)}, u32[]{:S(2)}) %all-to-all-start) | async-done | bytes 589856 | tf_op jit(solution)/shard_map/all_to_all | solution.py:36
  26.8 4.9 %all-to-all-start.1 = ((bf16[8,2,48,768]{3,2,1,0:T(8,128)(2,1)}), bf16[8,2,48,768]{3,2,1,0:T(8,128)(2,1)S(1)}, u32[]{:S(2)}, u32[]{:S(2)}) async-start(bf16[8,2,48,768]{3,2,1,0:T(8,128)(2,1)} %copies.3), calls=%async_computation.1 | async-start | bytes 2359296 | tf_op jit(solution)/shard_map/all_to_all | solution.py:36
  31.7 1.3 maximum_select_fusion.refs_0_
  33.0 4.7 %collective-permute-start = (bf16[128,1536]{1,0:T(8,128)(2,1)S(1)}, bf16[128,1536]{1,0:T(8,128)(2,1)S(1)}, u32[]{:S(2)}, u32[]{:S(2)}) collective-permute-start(bf16[128,1536]{1,0:T(8,128)(2,1)S(1)} %maximum_select_fusion.refs_0_), channel_id=1, source_target_pairs={{0,6},{1,7},{2,0},{3,1},{4,2},{5,3},{6,4},{7,5},{8,14},{9,15},{10,... | collective-permute-start | bytes 1179656 | tf_op jit(solution)/shard_map/ppermute | solution.py:252
  37.7 2.7 %collective-permute-start.1 = (bf16[128,1536]{1,0:T(8,128)(2,1)S(1)}, bf16[128,1536]{1,0:T(8,128)(2,1)S(1)}, u32[]{:S(2)}, u32[]{:S(2)}) collective-permute-start(bf16[128,1536]{1,0:T(8,128)(2,1)S(1)} %maximum_select_fusion.refs_0_), channel_id=1, source_target_pairs={{0,4},{1,5},{2,6},{3,7},{4,0},{5,1},{6,2},{7,3},{8,12},{9,13},{10,... | collective-permute-start | bytes 1179656 | tf_op jit(solution)/shard_map/ppermute | solution.py:253
  40.4 2.8 %collective-permute-start.2 = (bf16[128,1536]{1,0:T(8,128)(2,1)S(1)}, bf16[128,1536]{1,0:T(8,128)(2,1)S(1)}, u32[]{:S(2)}, u32[]{:S(2)}) collective-permute-start(bf16[128,1536]{1,0:T(8,128)(2,1)S(1)} %maximum_select_fusion.refs_0_), channel_id=1, source_target_pairs={{0,2},{1,3},{2,4},{3,5},{4,6},{5,7},{6,0},{7,1},{8,10},{9,11},{10,... | collective-permute-start | bytes 1179656 | tf_op jit(solution)/shard_map/ppermute | solution.py:254
  44.0 10.4 %collective-permute-done.refs_1_ = bf16[128,1536]{1,0:T(8,128)(2,1)S(1)} collective-permute-done((bf16[128,1536]{1,0:T(8,128)(2,1)S(1)}, bf16[128,1536]{1,0:T(8,128)(2,1)S(1)}, u32[]{:S(2)}, u32[]{:S(2)}) %collective-permute-start) | collective-permute-done | bytes 393248 | tf_op jit(solution)/shard_map/ppermute | solution.py:252
  55.9 4.1 %collective-permute-done.2.refs_3_ = bf16[128,1536]{1,0:T(8,128)(2,1)S(1)} collective-permute-done((bf16[128,1536]{1,0:T(8,128)(2,1)S(1)}, bf16[128,1536]{1,0:T(8,128)(2,1)S(1)}, u32[]{:S(2)}, u32[]{:S(2)}) %collective-permute-start.2) | collective-permute-done | bytes 393248 | tf_op jit(solution)/shard_map/ppermute | solution.py:254
  65.5 1.9 %collective-permute-start.3 = (bf16[512,1536]{1,0:T(8,128)(2,1)S(1)}, bf16[512,1536]{1,0:T(8,128)(2,1)}, u32[]{:S(2)}, u32[]{:S(2)}) collective-permute-start(bf16[512,1536]{1,0:T(8,128)(2,1)S(1)} %by_place.1.own), channel_id=1, source_target_pairs={{0,1},{1,0},{2,3},{3,2},{4,5},{5,4},{6,7},{7,6},{8,9},{9,8},{10,11... | collective-permute-start | bytes 4718600 | tf_op jit(solution)/shard_map/ppermute | solution.py:257
  67.5 10.9 %collective-permute-start.4 = (bf16[384,768]{1,0:T(8,128)(2,1)S(1)}, bf16[384,768]{1,0:T(8,128)(2,1)}, u32[]{:S(2)}, u32[]{:S(2)}) collective-permute-start(bf16[384,768]{1,0:T(8,128)(2,1)S(1)} %bitcast.12), channel_id=1, source_target_pairs={{0,448},{8,456},{16,464},{24,472},{32,480},{40,488},{48,496},{56,5... | collective-permute-start | bytes 1769480 | tf_op jit(solution)/shard_map/ppermute | solution.py:259
  78.4 1.9 %collective-permute-start.5 = (bf16[384,768]{1,0:T(8,128)(2,1)S(1)}, bf16[384,768]{1,0:T(8,128)(2,1)}, u32[]{:S(2)}, u32[]{:S(2)}) collective-permute-start(bf16[384,768]{1,0:T(8,128)(2,1)S(1)} %bitcast.13), channel_id=1, source_target_pairs={{0,64},{8,72},{16,80},{24,88},{32,96},{40,104},{48,112},{56,120},{... | collective-permute-start | bytes 1769480 | tf_op jit(solution)/shard_map/ppermute | solution.py:260
  80.4 1.9 %collective-permute-start.6 = (bf16[384,768]{1,0:T(8,128)(2,1)S(1)}, bf16[384,768]{1,0:T(8,128)(2,1)}, u32[]{:S(2)}, u32[]{:S(2)}) collective-permute-start(bf16[384,768]{1,0:T(8,128)(2,1)S(1)} %bitcast.14), channel_id=1, source_target_pairs={{0,128},{8,136},{16,144},{24,152},{32,160},{40,168},{48,176},{56,1... | collective-permute-start | bytes 1769480 | tf_op jit(solution)/shard_map/ppermute | solution.py:261
  82.4 5.1 %collective-permute-start.8 = (bf16[384,768]{1,0:T(8,128)(2,1)S(1)}, bf16[384,768]{1,0:T(8,128)(2,1)S(1)}, u32[]{:S(2)}, u32[]{:S(2)}) collective-permute-start(bf16[384,768]{1,0:T(8,128)(2,1)S(1)} %get-tuple-element.7), channel_id=1, source_target_pairs={{0,448},{8,456},{16,464},{24,472},{32,480},{40,488},{48,496},{56,5... | collective-permute-start | bytes 1769480 | tf_op jit(solution)/shard_map/ppermute | solution.py:266
  87.6 17.2 %collective-permute-done.4.u1 = bf16[384,768]{1,0:T(8,128)(2,1)} collective-permute-done((bf16[384,768]{1,0:T(8,128)(2,1)S(1)}, bf16[384,768]{1,0:T(8,128)(2,1)}, u32[]{:S(2)}, u32[]{:S(2)}) %collective-permute-start.4) | collective-permute-done | bytes 589856 | tf_op jit(solution)/shard_map/ppermute | solution.py:259
  104.8 1.9 %collective-permute-start.9 = (bf16[384,768]{1,0:T(8,128)(2,1)S(1)}, bf16[384,768]{1,0:T(8,128)(2,1)S(1)}, u32[]{:S(2)}, u32[]{:S(2)}) collective-permute-start(bf16[384,768]{1,0:T(8,128)(2,1)S(1)} %get-tuple-element.7), channel_id=1, source_target_pairs={{0,64},{8,72},{16,80},{24,88},{32,96},{40,104},{48,112},{56,120},{... | collective-permute-start | bytes 1769480 | tf_op jit(solution)/shard_map/ppermute | solution.py:266
  106.7 3.0 %collective-permute-done.5.u3 = bf16[384,768]{1,0:T(8,128)(2,1)} collective-permute-done((bf16[384,768]{1,0:T(8,128)(2,1)S(1)}, bf16[384,768]{1,0:T(8,128)(2,1)}, u32[]{:S(2)}, u32[]{:S(2)}) %collective-permute-start.5) | collective-permute-done | bytes 589856 | tf_op jit(solution)/shard_map/ppermute | solution.py:260
  109.7 6.3 %early.1 = bf16[1024,1152]{1,0:T(8,128)(2,1)} custom-call(bf16[512,1536]{1,0:T(8,128)(2,1)} %collective-permute-done.3.other, bf16[512,1536]{1,0:T(8,128)(2,1)S(1)} %by_place.1.own, bf16[384,768]{1,0:T(8,128)(2,1)S(1)} %bitcast.15, bf16[384,768]{1,0:T(8,128)(2,1)} %collective-permute-done.4.u1, bf16[384,768]{1,0:T(8,128)(2,1)} %collective-permute-done.5.u3), custom_call_target="tpu_custom_call" | custom-call | flops 1811939328 | bytes 4915200 | tf_op jit(solution)/shard_map/early/pallas_call | solution.py:170
  116.0 1.7 %copy-done = bf16[1024,1152]{1,0:T(8,128)(2,1)S(1)} copy-done((bf16[1024,1152]{1,0:T(8,128)(2,1)S(1)}, bf16[1024,1152]{1,0:T(8,128)(2,1)}, u32[]{:S(2)}) %copy-start) | copy-done | bytes 2359320
  117.7 2.7 %late.1 = bf16[1024,768]{1,0:T(8,128)(2,1)S(1)} custom-call(bf16[1024,1152]{1,0:T(8,128)(2,1)S(1)} %copy-done, bf16[384,768]{1,0:T(8,128)(2,1)} %collective-permute-done.6.u2, f32[1,768]{1,0:T(1,128)S(1)} %copy-done.9), custom_call_target="tpu_custom_call" | custom-call | flops 603979776 | bytes 4521984 | tf_op jit(solution)/shard_map/late/pallas_call | solution.py:216
  121.2 1.9 %collective-permute-start.11 = (bf16[512,768]{1,0:T(8,128)(2,1)S(1)}, bf16[512,768]{1,0:T(8,128)(2,1)S(1)}, u32[]{:S(2)}, u32[]{:S(2)}) collective-permute-start(bf16[512,768]{1,0:T(8,128)(2,1)S(1)} %convolution_convert_fusion), channel_id=1, source_target_pairs={{0,1},{1,0},{2,3},{3,2},{4,5},{5,4},{6,7},{7,6},{8,9},{9,8},{10,11... | collective-permute-start | bytes 2359304 | tf_op jit(solution)/shard_map/ppermute | solution.py:278
  123.2 1.7 %convolution_convert_fusion.1 = bf16[512,768]{1,0:T(8,128)(2,1)} fusion(bf16[768,768]{1,0:T(8,128)(2,1)S(1)} %pad_maximum_fusion, bf16[1024,768]{1,0:T(8,128)(2,1)S(1)} %late.1), kind=kOutput, calls=%fused_computation.3 | convolution fusion | flops 604372992 | bytes 2752512 | tf_op jit(solution)/shard_map/dot_general | solution.py:275
  124.9 2.4 %collective-permute-start.10 = (bf16[512,768]{1,0:T(8,128)(2,1)}, bf16[512,768]{1,0:T(8,128)(2,1)}, u32[]{:S(2)}, u32[]{:S(2)}) collective-permute-start(bf16[512,768]{1,0:T(8,128)(2,1)} %convolution_convert_fusion.1), channel_id=1, source_target_pairs={{0,1},{1,0},{2,3},{3,2},{4,5},{5,4},{6,7},{7,6},{8,9},{9,8},{10,11... | collective-permute-start | bytes 2359304 | tf_op jit(solution)/shard_map/ppermute | solution.py:278
  127.3 1.7 %add_convert_fusion = bf16[512,768]{1,0:T(8,128)(2,1)} fusion(bf16[512,768]{1,0:T(8,128)(2,1)S(1)} %collective-permute-done.11, bf16[768,768]{1,0:T(8,128)(2,1)S(1)} %get-tuple-element.8, bf16[1024,768]{1,0:T(8,128)(2,1)S(1)} %late.1), kind=kOutput, calls=%fused_computation | convolution fusion | flops 605159424 | bytes 3538944 | tf_op jit(solution)/shard_map/dot_general | solution.py:275
  129.1 3.5 %all-to-all-start.3 = ((bf16[4,128,768]{2,1,0:T(8,128)(2,1)}), bf16[4,128,768]{2,1,0:T(8,128)(2,1)S(1)}, u32[]{:S(2)}, u32[]{:S(2)}) async-start(bf16[4,128,768]{2,1,0:T(8,128)(2,1)} %bitcast.17), calls=%async_computation.3 | async-start | bytes 1572864 | tf_op jit(solution)/shard_map/all_to_all | solution.py:36
  132.6 2.9 %add_convert_fusion.1 = bf16[512,768]{1,0:T(8,128)(2,1)} fusion(bf16[512,768]{1,0:T(8,128)(2,1)} %collective-permute-done.10, bf16[768,768]{1,0:T(8,128)(2,1)S(1)} %pad_maximum_fusion, bf16[1024,768]{1,0:T(8,128)(2,1)S(1)} %late.1), kind=kOutput, calls=%fused_computation.1 | convolution fusion | flops 605159424 | bytes 3538944 | tf_op jit(solution)/shard_map/dot_general | solution.py:275
  135.4 9.9 %all-to-all-done.3 = bf16[4,128,768]{2,1,0:T(8,128)(2,1)S(1)} async-done(((bf16[4,128,768]{2,1,0:T(8,128)(2,1)}), bf16[4,128,768]{2,1,0:T(8,128)(2,1)S(1)}, u32[]{:S(2)}, u32[]{:S(2)}) %all-to-all-start.3) | async-done | bytes 786464 | tf_op jit(solution)/shard_map/all_to_all | solution.py:36
  145.3 3.5 %all-to-all-start.2 = ((bf16[4,128,768]{2,1,0:T(8,128)(2,1)}), bf16[4,128,768]{2,1,0:T(8,128)(2,1)S(1)}, u32[]{:S(2)}, u32[]{:S(2)}) async-start(bf16[4,128,768]{2,1,0:T(8,128)(2,1)} %bitcast.16), calls=%async_computation.2 | async-start | bytes 1572864 | tf_op jit(solution)/shard_map/all_to_all | solution.py:36
  149.0 11.7 %all-to-all-done.2 = bf16[4,128,768]{2,1,0:T(8,128)(2,1)S(1)} async-done(((bf16[4,128,768]{2,1,0:T(8,128)(2,1)}), bf16[4,128,768]{2,1,0:T(8,128)(2,1)S(1)}, u32[]{:S(2)}, u32[]{:S(2)}) %all-to-all-start.2) | async-done | bytes 786464 | tf_op jit(solution)/shard_map/all_to_all | solution.py:36
  (56 shorter events, 13.7 us)
Async XLA Ops:
  0.0 0.9 copy-start.10
  0.9 10.1 %copy-start.13 = (f32[768,48]{0,1:T(8,128)S(1)}, f32[768,48]{0,1:T(8,128)}, u32[]{:S(2)}) copy-start(f32[768,48]{0,1:T(8,128)} %param.10) | copy-start | bytes 442372
  0.9 10.1 %copy-start.15 = (f32[1,48]{1,0:T(1,128)S(1)}, f32[1,48]{1,0:T(1,128)}, u32[]{:S(2)}) copy-start(f32[1,48]{1,0:T(1,128)} %param.11) | copy-start | bytes 580
  0.9 14.6 %copy-start.11 = (bf16[128,1536]{1,0:T(8,128)(2,1)S(1)}, bf16[128,1536]{1,0:T(8,128)(2,1)}, u32[]{:S(2)}) copy-start(bf16[128,1536]{1,0:T(8,128)(2,1)} %param.6) | copy-start | bytes 1179652
  0.9 14.8 %copy-start.14 = (f32[1536]{0:T(1024)S(1)}, f32[1536]{0:T(1024)}, u32[]{:S(2)}) copy-start(f32[1536]{0:T(1024)} %param.7) | copy-start | bytes 18436
  1.8 25.0 %all-to-all-start = ((bf16[8,48,768]{2,1,0:T(8,128)(2,1)}), bf16[8,48,768]{2,1,0:T(8,128)(2,1)S(1)}, u32[]{:S(2)}, u32[]{:S(2)}) async-start(bf16[8,48,768]{2,1,0:T(8,128)(2,1)} %bitcast.1), calls=%async_computation | async-start | bytes 1179648 | tf_op jit(solution)/shard_map/all_to_all | solution.py:36
  11.1 11.6 %collective-permute-start.7 = (bf16[48,768]{1,0:T(8,128)(2,1)S(1)}, bf16[48,768]{1,0:T(8,128)(2,1)S(1)}, u32[]{:S(2)}, u32[]{:S(2)}) collective-permute-start(bf16[48,768]{1,0:T(8,128)(2,1)S(1)} %fusion.7.refs_0_), channel_id=1, source_target_pairs={{0,128},{8,136},{16,144},{24,152},{32,160},{40,168},{48,176},{56,1... | collective-permute-start | bytes 221192 | tf_op jit(solution)/shard_map/ppermute | solution.py:243
  17.3 14.4 %copy-start.12 = (bf16[128,384]{1,0:T(8,128)(2,1)S(1)}, bf16[128,384]{1,0:T(8,128)(2,1)}, u32[]{:S(2)}) copy-start(bf16[128,384]{1,0:T(8,128)(2,1)} %get-tuple-element.11) | copy-start | bytes 294916
  26.8 55.5 %all-to-all-start.1 = ((bf16[8,2,48,768]{3,2,1,0:T(8,128)(2,1)}), bf16[8,2,48,768]{3,2,1,0:T(8,128)(2,1)S(1)}, u32[]{:S(2)}, u32[]{:S(2)}) async-start(bf16[8,2,48,768]{3,2,1,0:T(8,128)(2,1)} %copies.3), calls=%async_computation.1 | async-start | bytes 2359296 | tf_op jit(solution)/shard_map/all_to_all | solution.py:36
  33.0 21.4 %collective-permute-start = (bf16[128,1536]{1,0:T(8,128)(2,1)S(1)}, bf16[128,1536]{1,0:T(8,128)(2,1)S(1)}, u32[]{:S(2)}, u32[]{:S(2)}) collective-permute-start(bf16[128,1536]{1,0:T(8,128)(2,1)S(1)} %maximum_select_fusion.refs_0_), channel_id=1, source_target_pairs={{0,6},{1,7},{2,0},{3,1},{4,2},{5,3},{6,4},{7,5},{8,14},{9,15},{10,... | collective-permute-start | bytes 1179656 | tf_op jit(solution)/shard_map/ppermute | solution.py:252
  37.7 17.4 %collective-permute-start.1 = (bf16[128,1536]{1,0:T(8,128)(2,1)S(1)}, bf16[128,1536]{1,0:T(8,128)(2,1)S(1)}, u32[]{:S(2)}, u32[]{:S(2)}) collective-permute-start(bf16[128,1536]{1,0:T(8,128)(2,1)S(1)} %maximum_select_fusion.refs_0_), channel_id=1, source_target_pairs={{0,4},{1,5},{2,6},{3,7},{4,0},{5,1},{6,2},{7,3},{8,12},{9,13},{10,... | collective-permute-start | bytes 1179656 | tf_op jit(solution)/shard_map/ppermute | solution.py:253
  40.4 19.6 %collective-permute-start.2 = (bf16[128,1536]{1,0:T(8,128)(2,1)S(1)}, bf16[128,1536]{1,0:T(8,128)(2,1)S(1)}, u32[]{:S(2)}, u32[]{:S(2)}) collective-permute-start(bf16[128,1536]{1,0:T(8,128)(2,1)S(1)} %maximum_select_fusion.refs_0_), channel_id=1, source_target_pairs={{0,2},{1,3},{2,4},{3,5},{4,6},{5,7},{6,0},{7,1},{8,10},{9,11},{10,... | collective-permute-start | bytes 1179656 | tf_op jit(solution)/shard_map/ppermute | solution.py:254
  43.2 0.7 copy-start.1
  54.4 0.7 copy-start.3
  55.1 0.8 copy-start.5
  60.0 0.8 copy-start.7
  60.8 1.0 copy-start.2
  61.8 1.0 copy-start.4
  62.7 1.0 copy-start.6
  63.7 1.0 copy-start.8
  65.5 44.2 %collective-permute-start.3 = (bf16[512,1536]{1,0:T(8,128)(2,1)S(1)}, bf16[512,1536]{1,0:T(8,128)(2,1)}, u32[]{:S(2)}, u32[]{:S(2)}) collective-permute-start(bf16[512,1536]{1,0:T(8,128)(2,1)S(1)} %by_place.1.own), channel_id=1, source_target_pairs={{0,1},{1,0},{2,3},{3,2},{4,5},{5,4},{6,7},{7,6},{8,9},{9,8},{10,11... | collective-permute-start | bytes 4718600 | tf_op jit(solution)/shard_map/ppermute | solution.py:257
  67.5 37.3 %collective-permute-start.4 = (bf16[384,768]{1,0:T(8,128)(2,1)S(1)}, bf16[384,768]{1,0:T(8,128)(2,1)}, u32[]{:S(2)}, u32[]{:S(2)}) collective-permute-start(bf16[384,768]{1,0:T(8,128)(2,1)S(1)} %bitcast.12), channel_id=1, source_target_pairs={{0,448},{8,456},{16,464},{24,472},{32,480},{40,488},{48,496},{56,5... | collective-permute-start | bytes 1769480 | tf_op jit(solution)/shard_map/ppermute | solution.py:259
  78.4 31.3 %collective-permute-start.5 = (bf16[384,768]{1,0:T(8,128)(2,1)S(1)}, bf16[384,768]{1,0:T(8,128)(2,1)}, u32[]{:S(2)}, u32[]{:S(2)}) collective-permute-start(bf16[384,768]{1,0:T(8,128)(2,1)S(1)} %bitcast.13), channel_id=1, source_target_pairs={{0,64},{8,72},{16,80},{24,88},{32,96},{40,104},{48,112},{56,120},{... | collective-permute-start | bytes 1769480 | tf_op jit(solution)/shard_map/ppermute | solution.py:260
  80.4 35.6 %collective-permute-start.6 = (bf16[384,768]{1,0:T(8,128)(2,1)S(1)}, bf16[384,768]{1,0:T(8,128)(2,1)}, u32[]{:S(2)}, u32[]{:S(2)}) collective-permute-start(bf16[384,768]{1,0:T(8,128)(2,1)S(1)} %bitcast.14), channel_id=1, source_target_pairs={{0,128},{8,136},{16,144},{24,152},{32,160},{40,168},{48,176},{56,1... | collective-permute-start | bytes 1769480 | tf_op jit(solution)/shard_map/ppermute | solution.py:261
  82.4 33.6 %copy-start.9 = (f32[1,768]{1,0:T(1,128)S(1)}, f32[1,768]{1,0:T(1,128)}, u32[]{:S(2)}) copy-start(f32[1,768]{1,0:T(1,128)} %scale.1) | copy-start | bytes 9220
  82.4 40.7 %collective-permute-start.8 = (bf16[384,768]{1,0:T(8,128)(2,1)S(1)}, bf16[384,768]{1,0:T(8,128)(2,1)S(1)}, u32[]{:S(2)}, u32[]{:S(2)}) collective-permute-start(bf16[384,768]{1,0:T(8,128)(2,1)S(1)} %get-tuple-element.7), channel_id=1, source_target_pairs={{0,448},{8,456},{16,464},{24,472},{32,480},{40,488},{48,496},{56,5... | collective-permute-start | bytes 1769480 | tf_op jit(solution)/shard_map/ppermute | solution.py:266
  104.8 18.3 %collective-permute-start.9 = (bf16[384,768]{1,0:T(8,128)(2,1)S(1)}, bf16[384,768]{1,0:T(8,128)(2,1)S(1)}, u32[]{:S(2)}, u32[]{:S(2)}) collective-permute-start(bf16[384,768]{1,0:T(8,128)(2,1)S(1)} %get-tuple-element.7), channel_id=1, source_target_pairs={{0,64},{8,72},{16,80},{24,88},{32,96},{40,104},{48,112},{56,120},{... | collective-permute-start | bytes 1769480 | tf_op jit(solution)/shard_map/ppermute | solution.py:266
  116.0 1.7 %copy-start = (bf16[1024,1152]{1,0:T(8,128)(2,1)S(1)}, bf16[1024,1152]{1,0:T(8,128)(2,1)}, u32[]{:S(2)}) copy-start(bf16[1024,1152]{1,0:T(8,128)(2,1)} %early.1) | copy-start | bytes 7077892
  121.2 6.2 %collective-permute-start.11 = (bf16[512,768]{1,0:T(8,128)(2,1)S(1)}, bf16[512,768]{1,0:T(8,128)(2,1)S(1)}, u32[]{:S(2)}, u32[]{:S(2)}) collective-permute-start(bf16[512,768]{1,0:T(8,128)(2,1)S(1)} %convolution_convert_fusion), channel_id=1, source_target_pairs={{0,1},{1,0},{2,3},{3,2},{4,5},{5,4},{6,7},{7,6},{8,9},{9,8},{10,11... | collective-permute-start | bytes 2359304 | tf_op jit(solution)/shard_map/ppermute | solution.py:278
  124.9 7.6 %collective-permute-start.10 = (bf16[512,768]{1,0:T(8,128)(2,1)}, bf16[512,768]{1,0:T(8,128)(2,1)}, u32[]{:S(2)}, u32[]{:S(2)}) collective-permute-start(bf16[512,768]{1,0:T(8,128)(2,1)} %convolution_convert_fusion.1), channel_id=1, source_target_pairs={{0,1},{1,0},{2,3},{3,2},{4,5},{5,4},{6,7},{7,6},{8,9},{9,8},{10,11... | collective-permute-start | bytes 2359304 | tf_op jit(solution)/shard_map/ppermute | solution.py:278
  129.1 16.2 %all-to-all-start.3 = ((bf16[4,128,768]{2,1,0:T(8,128)(2,1)}), bf16[4,128,768]{2,1,0:T(8,128)(2,1)S(1)}, u32[]{:S(2)}, u32[]{:S(2)}) async-start(bf16[4,128,768]{2,1,0:T(8,128)(2,1)} %bitcast.17), calls=%async_computation.3 | async-start | bytes 1572864 | tf_op jit(solution)/shard_map/all_to_all | solution.py:36
  145.3 15.4 %all-to-all-start.2 = ((bf16[4,128,768]{2,1,0:T(8,128)(2,1)}), bf16[4,128,768]{2,1,0:T(8,128)(2,1)S(1)}, u32[]{:S(2)}, u32[]{:S(2)}) async-start(bf16[4,128,768]{2,1,0:T(8,128)(2,1)} %bitcast.16), calls=%async_computation.2 | async-start | bytes 1572864 | tf_op jit(solution)/shard_map/all_to_all | solution.py:36

commit v6 on v5

--- a/solution.py
+++ b/solution.py
@@ -126,6 +126,24 @@
     )(x[None], *blocks)
 
 
+def half_kernel(first, a, out):
+    out[...] = a[first : first + out.shape[0]]
+
+
+def half_of(a, part):
+    rows = a.shape[0] // 2
+    out = jax.ShapeDtypeStruct((rows, a.shape[1]), a.dtype)
+    return pl.pallas_call(
+        functools.partial(half_kernel, part * rows),
+        out_shape=out,
+        in_specs=[VMEM],
+        out_specs=VMEM,
+        cost_estimate=cost(1 << 26, out, out),
+        compiler_params=pltpu.CompilerParams(vmem_limit_bytes=1 << 20),
+        name="half",
+    )(a)
+
+
 TILE = 256
 
 
@@ -170,7 +188,7 @@
     return pl.pallas_call(
         functools.partial(early_kernel, half),
         grid=(2 * half,),
-        out_shape=pltpu.HBM(shape, BF16),
+        out_shape=jax.ShapeDtypeStruct(shape, BF16),
         in_specs=[
             pl.BlockSpec((TILE, d), lambda i: (jnp.minimum(i, half - 1), 0)),
             pl.BlockSpec((TILE, d), lambda i: (jnp.maximum(i - half, 0), 0)),
@@ -187,7 +205,7 @@
     )(other, own, *blocks)
 
 
-def late_kernel(early, u2, scale, hidden, tiles, up, sems):
+def late_kernel(early, u2_top, u2_bottom, scale, hidden, tiles, up, sems):
     step, steps = pl.program_id(0), early.shape[0] // TILE
     columns = hidden.shape[1]
 
@@ -197,11 +215,17 @@
 
     @pl.when(step == 0)
     def _():
-        block = pltpu.make_async_copy(u2, up, sems.at[steps])
-        block.start()
+        rows = u2_top.shape[0]
+        blocks = [
+            pltpu.make_async_copy(block, up.at[pl.ds(k * rows, rows)], sems.at[steps + k])
+            for k, block in enumerate((u2_top, u2_bottom))
+        ]
+        for block in blocks:
+            block.start()
         for i in range(steps):
             fetch(i).start()
-        block.wait()
+        for block in blocks:
+            block.wait()
 
     fetch(step).wait()
     tile = tiles.at[pl.ds(pl.multiple_of(step * TILE, TILE), TILE)]
@@ -209,25 +233,25 @@
     hidden[...] = jnp.square(jnp.maximum(pre * scale[...], 0.0)).astype(BF16)
 
 
-def late_of(early, block, scale):
-    width, columns = block.shape
+def late_of(early, halves, scale):
+    width, columns = halves[0].shape
     steps = early.shape[0] // TILE
     out = jax.ShapeDtypeStruct((early.shape[0], columns), BF16)
     return pl.pallas_call(
         late_kernel,
         grid=(steps,),
         out_shape=out,
-        in_specs=[HBM, HBM, pl.BlockSpec((1, columns), lambda i: (0, 0))],
+        in_specs=[HBM, HBM, HBM, pl.BlockSpec((1, columns), lambda i: (0, 0))],
         out_specs=pl.BlockSpec((TILE, columns), lambda i: (i, 0)),
         scratch_shapes=[
             pltpu.VMEM(early.shape, BF16),
-            pltpu.VMEM((width, columns), BF16),
-            pltpu.SemaphoreType.DMA((steps + 1,)),
+            pltpu.VMEM((2 * width, columns), BF16),
+            pltpu.SemaphoreType.DMA((steps + 2,)),
         ],
         compiler_params=pltpu.CompilerParams(vmem_limit_bytes=12 << 20),
-        cost_estimate=cost(2 * early.shape[0] * width * columns, early, block, out),
+        cost_estimate=cost(4 * early.shape[0] * width * columns, early, *halves, out),
         name="late",
-    )(early, block, scale)
+    )(early, *halves, scale)
 
 
 def body(tokens, norm_gain, up_weight, up_scale, down_weight, down_scale):
@@ -258,7 +282,10 @@
 
     up_next = lax.ppermute(up_own, PLANE, FROM_NEXT)
     up_last = lax.ppermute(up_own, PLANE, FROM_LAST)
-    up_two = lax.ppermute(up_own, PLANE, FROM_TWO)
+    up_two = (
+        lax.ppermute(half_of(up_next, 0), PLANE, FROM_NEXT),
+        lax.ppermute(half_of(up_last, 1), PLANE, FROM_LAST),
+    )
 
     copies = copies_of([down_piece, down_two])
     down_own, down_a = split(swapped(copies, "fs", ROW_GROUPS))

time: 163 us -> 163 us (level)
  starting transfers between devices: 63.8 us -> 69 us
  waiting for transfers between devices: 64.7 us -> 61.8 us
    ppermute x1, waiting for transfers between devices: 17.2 us -> 11.3 us  [body(): up_next = lax.ppermute(up_own, PLANE, FROM_NEXT)]
    ppermute x1 -> x2, starting transfers between devices: 1.92 us -> 7.5 us  [the longest x1 5.59 us: body(): lax.ppermute(half_of(up_next, 0), PLANE, FROM_NEXT)]
    ppermute x1, waiting for transfers between devices: 0.01 us -> 5.13 us  [body(): lax.ppermute(down_own, PLANE, FROM_LAST)]
    ppermute x1, waiting for transfers between devices: 3.05 us -> 0.01 us  [body(): up_last = lax.ppermute(up_own, PLANE, FROM_LAST)]
    pallas_call x1, Pallas kernels: 6.25 us -> 4.29 us  [early_of(): pl.pallas_call(functools.partial(early_kernel, half), grid=(2 * half,), o...]
    unnamed x32 -> x38, local copies, waits for them, and re-layouts: 9.56 us -> 8.03 us
  transfers between devices with their start and end apart: 16 -> 17, of which waited for: 8 -> 8; matrix products, arithmetic and copies ran while one was open for 6% -> 6% of each run, Pallas kernels for 7% -> 7%
where the time goes in v6:
time: 163 us; the launch traced here: 162 us
  starting transfers between devices  69 us (42%)
  waiting for transfers between devices  61.8 us (38%)
  Pallas kernels  11.4 us (7%)
  local copies, waits for them, and re-layouts  9.52 us (6%)
  matrix products  7.04 us (4%)
  other arithmetic  3.02 us (2%)
    all_to_all x4, waiting for transfers between devices, swapped(): lax.all_to_all(blocks, axis, 0, 0, axis_index_groups=groups, tiled=True)  25.5 us
    all_to_all x4, starting transfers between devices, swapped(): lax.all_to_all(blocks, axis, 0, 0, axis_index_groups=groups, tiled=True)  21.1 us
    ppermute x1, waiting for transfers between devices, body(): up_next = lax.ppermute(up_own, PLANE, FROM_NEXT)  11.3 us
    ppermute x1, starting transfers between devices, body(): up_next = lax.ppermute(up_own, PLANE, FROM_NEXT)  10.9 us
    ppermute x1, waiting for transfers between devices, body(): lax.ppermute(normed, 'tp', X_NEXT)  10.4 us
    unnamed x38, local copies, waits for them, and re-layouts  8.03 us
    dot_general x4, matrix products, terms(): lax.dot_general(hidden, down, (((1,), (1,)), ((), ())), preferred_element...  7.04 us
    ppermute x1, starting transfers between devices, body(): lax.ppermute(half_of(up_next, 0), PLANE, FROM_NEXT)  5.59 us
  transfers between devices with their start and end apart: 17, of which 8 were waited for; matrix products, arithmetic and copies ran while one was open for 6% of the time, Pallas kernels for 7%

profile of v6, /device:TPU:8, one launch (start us, length us, event | category | flops | bytes accessed | tf_op | source)
XLA Modules:
  0.0 162.2 jit_solution(11449357582587591194)
XLA Ops:
  1.8 9.2 %all-to-all-start = ((bf16[8,48,768]{2,1,0:T(8,128)(2,1)}), bf16[8,48,768]{2,1,0:T(8,128)(2,1)S(1)}, u32[]{:S(2)}, u32[]{:S(2)}) async-start(bf16[8,48,768]{2,1,0:T(8,128)(2,1)} %bitcast.1), calls=%async_computation | async-start | bytes 1179648 | tf_op jit(solution)/shard_map/all_to_all | solution.py:36
  11.1 4.4 %collective-permute-start.8 = (bf16[48,768]{1,0:T(8,128)(2,1)S(1)}, bf16[48,768]{1,0:T(8,128)(2,1)S(1)}, u32[]{:S(2)}, u32[]{:S(2)}) collective-permute-start(bf16[48,768]{1,0:T(8,128)(2,1)S(1)} %fusion.7.refs_0_), channel_id=1, source_target_pairs={{0,128},{8,136},{16,144},{24,152},{32,160},{40,168},{48,176},{56,1... | collective-permute-start | bytes 221192 | tf_op jit(solution)/shard_map/ppermute | solution.py:267
  17.3 5.4 %collective-permute-done.8.refs_1_ = bf16[48,768]{1,0:T(8,128)(2,1)S(1)} collective-permute-done((bf16[48,768]{1,0:T(8,128)(2,1)S(1)}, bf16[48,768]{1,0:T(8,128)(2,1)S(1)}, u32[]{:S(2)}, u32[]{:S(2)}) %collective-permute-start.8) | collective-permute-done | bytes 73760 | tf_op jit(solution)/shard_map/ppermute | solution.py:267
  22.7 1.1 copies.3
  23.8 3.0 %all-to-all-done = bf16[8,48,768]{2,1,0:T(8,128)(2,1)S(1)} async-done(((bf16[8,48,768]{2,1,0:T(8,128)(2,1)}), bf16[8,48,768]{2,1,0:T(8,128)(2,1)S(1)}, u32[]{:S(2)}, u32[]{:S(2)}) %all-to-all-start) | async-done | bytes 589856 | tf_op jit(solution)/shard_map/all_to_all | solution.py:36
  26.8 4.9 %all-to-all-start.1 = ((bf16[8,2,48,768]{3,2,1,0:T(8,128)(2,1)}), bf16[8,2,48,768]{3,2,1,0:T(8,128)(2,1)S(1)}, u32[]{:S(2)}, u32[]{:S(2)}) async-start(bf16[8,2,48,768]{3,2,1,0:T(8,128)(2,1)} %copies.3), calls=%async_computation.1 | async-start | bytes 2359296 | tf_op jit(solution)/shard_map/all_to_all | solution.py:36
  31.7 1.3 maximum_select_fusion.refs_0_
  33.0 4.7 %collective-permute-start = (bf16[128,1536]{1,0:T(8,128)(2,1)S(1)}, bf16[128,1536]{1,0:T(8,128)(2,1)S(1)}, u32[]{:S(2)}, u32[]{:S(2)}) collective-permute-start(bf16[128,1536]{1,0:T(8,128)(2,1)S(1)} %maximum_select_fusion.refs_0_), channel_id=1, source_target_pairs={{0,6},{1,7},{2,0},{3,1},{4,2},{5,3},{6,4},{7,5},{8,14},{9,15},{10,... | collective-permute-start | bytes 1179656 | tf_op jit(solution)/shard_map/ppermute | solution.py:276
  37.7 2.7 %collective-permute-start.1 = (bf16[128,1536]{1,0:T(8,128)(2,1)S(1)}, bf16[128,1536]{1,0:T(8,128)(2,1)S(1)}, u32[]{:S(2)}, u32[]{:S(2)}) collective-permute-start(bf16[128,1536]{1,0:T(8,128)(2,1)S(1)} %maximum_select_fusion.refs_0_), channel_id=1, source_target_pairs={{0,4},{1,5},{2,6},{3,7},{4,0},{5,1},{6,2},{7,3},{8,12},{9,13},{10,... | collective-permute-start | bytes 1179656 | tf_op jit(solution)/shard_map/ppermute | solution.py:277
  40.4 2.8 %collective-permute-start.2 = (bf16[128,1536]{1,0:T(8,128)(2,1)S(1)}, bf16[128,1536]{1,0:T(8,128)(2,1)S(1)}, u32[]{:S(2)}, u32[]{:S(2)}) collective-permute-start(bf16[128,1536]{1,0:T(8,128)(2,1)S(1)} %maximum_select_fusion.refs_0_), channel_id=1, source_target_pairs={{0,2},{1,3},{2,4},{3,5},{4,6},{5,7},{6,0},{7,1},{8,10},{9,11},{10,... | collective-permute-start | bytes 1179656 | tf_op jit(solution)/shard_map/ppermute | solution.py:278
  44.0 10.4 %collective-permute-done.refs_1_ = bf16[128,1536]{1,0:T(8,128)(2,1)S(1)} collective-permute-done((bf16[128,1536]{1,0:T(8,128)(2,1)S(1)}, bf16[128,1536]{1,0:T(8,128)(2,1)S(1)}, u32[]{:S(2)}, u32[]{:S(2)}) %collective-permute-start) | collective-permute-done | bytes 393248 | tf_op jit(solution)/shard_map/ppermute | solution.py:276
  55.9 4.1 %collective-permute-done.2.refs_3_ = bf16[128,1536]{1,0:T(8,128)(2,1)S(1)} collective-permute-done((bf16[128,1536]{1,0:T(8,128)(2,1)S(1)}, bf16[128,1536]{1,0:T(8,128)(2,1)S(1)}, u32[]{:S(2)}, u32[]{:S(2)}) %collective-permute-start.2) | collective-permute-done | bytes 393248 | tf_op jit(solution)/shard_map/ppermute | solution.py:278
  65.5 1.9 %collective-permute-start.3 = (bf16[512,1536]{1,0:T(8,128)(2,1)S(1)}, bf16[512,1536]{1,0:T(8,128)(2,1)}, u32[]{:S(2)}, u32[]{:S(2)}) collective-permute-start(bf16[512,1536]{1,0:T(8,128)(2,1)S(1)} %by_place.1.own), channel_id=1, source_target_pairs={{0,1},{1,0},{2,3},{3,2},{4,5},{5,4},{6,7},{7,6},{8,9},{9,8},{10,11... | collective-permute-start | bytes 4718600 | tf_op jit(solution)/shard_map/ppermute | solution.py:281
  67.5 10.9 %collective-permute-start.4 = (bf16[384,768]{1,0:T(8,128)(2,1)S(1)}, bf16[384,768]{1,0:T(8,128)(2,1)S(1)}, u32[]{:S(2)}, u32[]{:S(2)}) collective-permute-start(bf16[384,768]{1,0:T(8,128)(2,1)S(1)} %bitcast.12), channel_id=1, source_target_pairs={{0,448},{8,456},{16,464},{24,472},{32,480},{40,488},{48,496},{56,5... | collective-permute-start | bytes 1769480 | tf_op jit(solution)/shard_map/ppermute | solution.py:283
  78.4 1.9 %collective-permute-start.5 = (bf16[384,768]{1,0:T(8,128)(2,1)S(1)}, bf16[384,768]{1,0:T(8,128)(2,1)S(1)}, u32[]{:S(2)}, u32[]{:S(2)}) collective-permute-start(bf16[384,768]{1,0:T(8,128)(2,1)S(1)} %bitcast.13), channel_id=1, source_target_pairs={{0,64},{8,72},{16,80},{24,88},{32,96},{40,104},{48,112},{56,120},{... | collective-permute-start | bytes 1769480 | tf_op jit(solution)/shard_map/ppermute | solution.py:284
  80.4 11.3 %collective-permute-done.4.u1.a = bf16[384,768]{1,0:T(8,128)(2,1)S(1)} collective-permute-done((bf16[384,768]{1,0:T(8,128)(2,1)S(1)}, bf16[384,768]{1,0:T(8,128)(2,1)S(1)}, u32[]{:S(2)}, u32[]{:S(2)}) %collective-permute-start.4) | collective-permute-done | bytes 589856 | tf_op jit(solution)/shard_map/ppermute | solution.py:283
  92.4 5.6 %collective-permute-start.6 = (bf16[192,768]{1,0:T(8,128)(2,1)}, bf16[192,768]{1,0:T(8,128)(2,1)}, u32[]{:S(2)}, u32[]{:S(2)}) collective-permute-start(bf16[192,768]{1,0:T(8,128)(2,1)} %half.2), channel_id=1, source_target_pairs={{0,448},{8,456},{16,464},{24,472},{32,480},{40,488},{48,496},{56,5... | collective-permute-start | bytes 884744 | tf_op jit(solution)/shard_map/ppermute | solution.py:286
  99.0 1.9 %collective-permute-start.7 = (bf16[192,768]{1,0:T(8,128)(2,1)}, bf16[192,768]{1,0:T(8,128)(2,1)}, u32[]{:S(2)}, u32[]{:S(2)}) collective-permute-start(bf16[192,768]{1,0:T(8,128)(2,1)} %half.3), channel_id=1, source_target_pairs={{0,64},{8,72},{16,80},{24,88},{32,96},{40,104},{48,112},{56,120},{... | collective-permute-start | bytes 884744 | tf_op jit(solution)/shard_map/ppermute | solution.py:287
  101.0 2.1 %collective-permute-start.10 = (bf16[384,768]{1,0:T(8,128)(2,1)S(1)}, bf16[384,768]{1,0:T(8,128)(2,1)S(1)}, u32[]{:S(2)}, u32[]{:S(2)}) collective-permute-start(bf16[384,768]{1,0:T(8,128)(2,1)S(1)} %get-tuple-element.7), channel_id=1, source_target_pairs={{0,64},{8,72},{16,80},{24,88},{32,96},{40,104},{48,112},{56,120},{... | collective-permute-start | bytes 1769480 | tf_op jit(solution)/shard_map/ppermute | solution.py:293
  103.1 5.1 %collective-permute-start.9 = (bf16[384,768]{1,0:T(8,128)(2,1)S(1)}, bf16[384,768]{1,0:T(8,128)(2,1)S(1)}, u32[]{:S(2)}, u32[]{:S(2)}) collective-permute-start(bf16[384,768]{1,0:T(8,128)(2,1)S(1)} %get-tuple-element.7), channel_id=1, source_target_pairs={{0,448},{8,456},{16,464},{24,472},{32,480},{40,488},{48,496},{56,5... | collective-permute-start | bytes 1769480 | tf_op jit(solution)/shard_map/ppermute | solution.py:293
  108.3 4.3 %early.1 = bf16[1024,1152]{1,0:T(8,128)(2,1)S(1)} custom-call(bf16[512,1536]{1,0:T(8,128)(2,1)} %collective-permute-done.3.other, bf16[512,1536]{1,0:T(8,128)(2,1)S(1)} %by_place.1.own, bf16[384,768]{1,0:T(8,128)(2,1)S(1)} %bitcast.14, bf16[384,768]{1,0:T(8,128)(2,1)S(1)} %copy-done.1, bf16[384,768]{1,0:T(8,128)(2,1)S(1)} %copy-done.3), custom_call_target="tpu_custom_call" | custom-call | flops 1811939328 | bytes 4915200 | tf_op jit(solution)/shard_map/early/pallas_call | solution.py:188
  112.6 2.7 %late.1 = bf16[1024,768]{1,0:T(8,128)(2,1)S(1)} custom-call(bf16[1024,1152]{1,0:T(8,128)(2,1)S(1)} %early.1, bf16[192,768]{1,0:T(8,128)(2,1)} %collective-permute-done.6.u2_top, bf16[192,768]{1,0:T(8,128)(2,1)} %collective-permute-done.7.u2_bottom, f32[1,768]{1,0:T(1,128)S(1)} %copy-done.12), custom_call_target="tpu_custom_call" | custom-call | flops 603979776 | bytes 4521984 | tf_op jit(solution)/shard_map/late/pallas_call | solution.py:240
  116.1 1.9 %collective-permute-start.12 = (bf16[512,768]{1,0:T(8,128)(2,1)S(1)}, bf16[512,768]{1,0:T(8,128)(2,1)S(1)}, u32[]{:S(2)}, u32[]{:S(2)}) collective-permute-start(bf16[512,768]{1,0:T(8,128)(2,1)S(1)} %convolution_convert_fusion), channel_id=1, source_target_pairs={{0,1},{1,0},{2,3},{3,2},{4,5},{5,4},{6,7},{7,6},{8,9},{9,8},{10,11... | collective-permute-start | bytes 2359304 | tf_op jit(solution)/shard_map/ppermute | solution.py:305
  118.0 5.1 %collective-permute-done.10 = bf16[384,768]{1,0:T(8,128)(2,1)S(1)} collective-permute-done((bf16[384,768]{1,0:T(8,128)(2,1)S(1)}, bf16[384,768]{1,0:T(8,128)(2,1)S(1)}, u32[]{:S(2)}, u32[]{:S(2)}) %collective-permute-start.10) | collective-permute-done | bytes 589856 | tf_op jit(solution)/shard_map/ppermute | solution.py:293
  123.3 1.7 %convolution_convert_fusion.1 = bf16[512,768]{1,0:T(8,128)(2,1)} fusion(bf16[768,768]{1,0:T(8,128)(2,1)S(1)} %pad_maximum_fusion, bf16[1024,768]{1,0:T(8,128)(2,1)S(1)} %late.1), kind=kOutput, calls=%fused_computation.3 | convolution fusion | flops 604372992 | bytes 2752512 | tf_op jit(solution)/shard_map/dot_general | solution.py:302
  125.0 1.9 %collective-permute-start.11 = (bf16[512,768]{1,0:T(8,128)(2,1)}, bf16[512,768]{1,0:T(8,128)(2,1)}, u32[]{:S(2)}, u32[]{:S(2)}) collective-permute-start(bf16[512,768]{1,0:T(8,128)(2,1)} %convolution_convert_fusion.1), channel_id=1, source_target_pairs={{0,1},{1,0},{2,3},{3,2},{4,5},{5,4},{6,7},{7,6},{8,9},{9,8},{10,11... | collective-permute-start | bytes 2359304 | tf_op jit(solution)/shard_map/ppermute | solution.py:305
  126.9 1.7 %add_convert_fusion = bf16[512,768]{1,0:T(8,128)(2,1)} fusion(bf16[512,768]{1,0:T(8,128)(2,1)S(1)} %collective-permute-done.12, bf16[768,768]{1,0:T(8,128)(2,1)S(1)} %get-tuple-element.8, bf16[1024,768]{1,0:T(8,128)(2,1)S(1)} %late.1), kind=kOutput, calls=%fused_computation | convolution fusion | flops 605159424 | bytes 3538944 | tf_op jit(solution)/shard_map/dot_general | solution.py:302
  128.6 3.5 %all-to-all-start.3 = ((bf16[4,128,768]{2,1,0:T(8,128)(2,1)}), bf16[4,128,768]{2,1,0:T(8,128)(2,1)S(1)}, u32[]{:S(2)}, u32[]{:S(2)}) async-start(bf16[4,128,768]{2,1,0:T(8,128)(2,1)} %bitcast.16), calls=%async_computation.3 | async-start | bytes 1572864 | tf_op jit(solution)/shard_map/all_to_all | solution.py:36
  132.1 2.8 %add_convert_fusion.1 = bf16[512,768]{1,0:T(8,128)(2,1)} fusion(bf16[512,768]{1,0:T(8,128)(2,1)} %collective-permute-done.11, bf16[768,768]{1,0:T(8,128)(2,1)S(1)} %pad_maximum_fusion, bf16[1024,768]{1,0:T(8,128)(2,1)S(1)} %late.1), kind=kOutput, calls=%fused_computation.1 | convolution fusion | flops 605159424 | bytes 3538944 | tf_op jit(solution)/shard_map/dot_general | solution.py:302
  134.9 10.4 %all-to-all-done.3 = bf16[4,128,768]{2,1,0:T(8,128)(2,1)S(1)} async-done(((bf16[4,128,768]{2,1,0:T(8,128)(2,1)}), bf16[4,128,768]{2,1,0:T(8,128)(2,1)S(1)}, u32[]{:S(2)}, u32[]{:S(2)}) %all-to-all-start.3) | async-done | bytes 786464 | tf_op jit(solution)/shard_map/all_to_all | solution.py:36
  145.3 3.5 %all-to-all-start.2 = ((bf16[4,128,768]{2,1,0:T(8,128)(2,1)}), bf16[4,128,768]{2,1,0:T(8,128)(2,1)S(1)}, u32[]{:S(2)}, u32[]{:S(2)}) async-start(bf16[4,128,768]{2,1,0:T(8,128)(2,1)} %bitcast.15), calls=%async_computation.2 | async-start | bytes 1572864 | tf_op jit(solution)/shard_map/all_to_all | solution.py:36
  149.0 12.2 %all-to-all-done.2 = bf16[4,128,768]{2,1,0:T(8,128)(2,1)S(1)} async-done(((bf16[4,128,768]{2,1,0:T(8,128)(2,1)}), bf16[4,128,768]{2,1,0:T(8,128)(2,1)S(1)}, u32[]{:S(2)}, u32[]{:S(2)}) %all-to-all-start.2) | async-done | bytes 786464 | tf_op jit(solution)/shard_map/all_to_all | solution.py:36
  (66 shorter events, 15.4 us)
Async XLA Ops:
  0.0 0.9 copy-start.13
  0.9 10.1 %copy-start.16 = (f32[768,48]{0,1:T(8,128)S(1)}, f32[768,48]{0,1:T(8,128)}, u32[]{:S(2)}) copy-start(f32[768,48]{0,1:T(8,128)} %param.10) | copy-start | bytes 442372
  0.9 10.1 %copy-start.18 = (f32[1,48]{1,0:T(1,128)S(1)}, f32[1,48]{1,0:T(1,128)}, u32[]{:S(2)}) copy-start(f32[1,48]{1,0:T(1,128)} %param.11) | copy-start | bytes 580
  0.9 14.6 %copy-start.14 = (bf16[128,1536]{1,0:T(8,128)(2,1)S(1)}, bf16[128,1536]{1,0:T(8,128)(2,1)}, u32[]{:S(2)}) copy-start(bf16[128,1536]{1,0:T(8,128)(2,1)} %param.6) | copy-start | bytes 1179652
  0.9 14.8 %copy-start.17 = (f32[1536]{0:T(1024)S(1)}, f32[1536]{0:T(1024)}, u32[]{:S(2)}) copy-start(f32[1536]{0:T(1024)} %param.7) | copy-start | bytes 18436
  1.8 25.0 %all-to-all-start = ((bf16[8,48,768]{2,1,0:T(8,128)(2,1)}), bf16[8,48,768]{2,1,0:T(8,128)(2,1)S(1)}, u32[]{:S(2)}, u32[]{:S(2)}) async-start(bf16[8,48,768]{2,1,0:T(8,128)(2,1)} %bitcast.1), calls=%async_computation | async-start | bytes 1179648 | tf_op jit(solution)/shard_map/all_to_all | solution.py:36
  11.1 11.6 %collective-permute-start.8 = (bf16[48,768]{1,0:T(8,128)(2,1)S(1)}, bf16[48,768]{1,0:T(8,128)(2,1)S(1)}, u32[]{:S(2)}, u32[]{:S(2)}) collective-permute-start(bf16[48,768]{1,0:T(8,128)(2,1)S(1)} %fusion.7.refs_0_), channel_id=1, source_target_pairs={{0,128},{8,136},{16,144},{24,152},{32,160},{40,168},{48,176},{56,1... | collective-permute-start | bytes 221192 | tf_op jit(solution)/shard_map/ppermute | solution.py:267
  17.3 14.4 %copy-start.15 = (bf16[128,384]{1,0:T(8,128)(2,1)S(1)}, bf16[128,384]{1,0:T(8,128)(2,1)}, u32[]{:S(2)}) copy-start(bf16[128,384]{1,0:T(8,128)(2,1)} %get-tuple-element.11) | copy-start | bytes 294916
  26.8 74.1 %all-to-all-start.1 = ((bf16[8,2,48,768]{3,2,1,0:T(8,128)(2,1)}), bf16[8,2,48,768]{3,2,1,0:T(8,128)(2,1)S(1)}, u32[]{:S(2)}, u32[]{:S(2)}) async-start(bf16[8,2,48,768]{3,2,1,0:T(8,128)(2,1)} %copies.3), calls=%async_computation.1 | async-start | bytes 2359296 | tf_op jit(solution)/shard_map/all_to_all | solution.py:36
  33.0 21.4 %collective-permute-start = (bf16[128,1536]{1,0:T(8,128)(2,1)S(1)}, bf16[128,1536]{1,0:T(8,128)(2,1)S(1)}, u32[]{:S(2)}, u32[]{:S(2)}) collective-permute-start(bf16[128,1536]{1,0:T(8,128)(2,1)S(1)} %maximum_select_fusion.refs_0_), channel_id=1, source_target_pairs={{0,6},{1,7},{2,0},{3,1},{4,2},{5,3},{6,4},{7,5},{8,14},{9,15},{10,... | collective-permute-start | bytes 1179656 | tf_op jit(solution)/shard_map/ppermute | solution.py:276
  37.7 17.4 %collective-permute-start.1 = (bf16[128,1536]{1,0:T(8,128)(2,1)S(1)}, bf16[128,1536]{1,0:T(8,128)(2,1)S(1)}, u32[]{:S(2)}, u32[]{:S(2)}) collective-permute-start(bf16[128,1536]{1,0:T(8,128)(2,1)S(1)} %maximum_select_fusion.refs_0_), channel_id=1, source_target_pairs={{0,4},{1,5},{2,6},{3,7},{4,0},{5,1},{6,2},{7,3},{8,12},{9,13},{10,... | collective-permute-start | bytes 1179656 | tf_op jit(solution)/shard_map/ppermute | solution.py:277
  40.4 19.6 %collective-permute-start.2 = (bf16[128,1536]{1,0:T(8,128)(2,1)S(1)}, bf16[128,1536]{1,0:T(8,128)(2,1)S(1)}, u32[]{:S(2)}, u32[]{:S(2)}) collective-permute-start(bf16[128,1536]{1,0:T(8,128)(2,1)S(1)} %maximum_select_fusion.refs_0_), channel_id=1, source_target_pairs={{0,2},{1,3},{2,4},{3,5},{4,6},{5,7},{6,0},{7,1},{8,10},{9,11},{10,... | collective-permute-start | bytes 1179656 | tf_op jit(solution)/shard_map/ppermute | solution.py:278
  60.8 1.0 copy-start.5
  61.8 1.0 copy-start.7
  62.7 1.0 copy-start.9
  63.7 1.0 copy-start.11
  65.5 42.7 %collective-permute-start.3 = (bf16[512,1536]{1,0:T(8,128)(2,1)S(1)}, bf16[512,1536]{1,0:T(8,128)(2,1)}, u32[]{:S(2)}, u32[]{:S(2)}) collective-permute-start(bf16[512,1536]{1,0:T(8,128)(2,1)S(1)} %by_place.1.own), channel_id=1, source_target_pairs={{0,1},{1,0},{2,3},{3,2},{4,5},{5,4},{6,7},{7,6},{8,9},{9,8},{10,11... | collective-permute-start | bytes 4718600 | tf_op jit(solution)/shard_map/ppermute | solution.py:281
  67.5 24.2 %collective-permute-start.4 = (bf16[384,768]{1,0:T(8,128)(2,1)S(1)}, bf16[384,768]{1,0:T(8,128)(2,1)S(1)}, u32[]{:S(2)}, u32[]{:S(2)}) collective-permute-start(bf16[384,768]{1,0:T(8,128)(2,1)S(1)} %bitcast.12), channel_id=1, source_target_pairs={{0,448},{8,456},{16,464},{24,472},{32,480},{40,488},{48,496},{56,5... | collective-permute-start | bytes 1769480 | tf_op jit(solution)/shard_map/ppermute | solution.py:283
  78.4 19.6 %collective-permute-start.5 = (bf16[384,768]{1,0:T(8,128)(2,1)S(1)}, bf16[384,768]{1,0:T(8,128)(2,1)S(1)}, u32[]{:S(2)}, u32[]{:S(2)}) collective-permute-start(bf16[384,768]{1,0:T(8,128)(2,1)S(1)} %bitcast.13), channel_id=1, source_target_pairs={{0,64},{8,72},{16,80},{24,88},{32,96},{40,104},{48,112},{56,120},{... | collective-permute-start | bytes 1769480 | tf_op jit(solution)/shard_map/ppermute | solution.py:284
  91.6 7.2 %copy-start = (bf16[384,768]{1,0:T(8,128)(2,1)}, bf16[384,768]{1,0:T(8,128)(2,1)S(1)}, u32[]{:S(2)}) copy-start(bf16[384,768]{1,0:T(8,128)(2,1)S(1)} %collective-permute-done.4.u1.a) | copy-start | bytes 1769476
  92.4 20.1 %collective-permute-start.6 = (bf16[192,768]{1,0:T(8,128)(2,1)}, bf16[192,768]{1,0:T(8,128)(2,1)}, u32[]{:S(2)}, u32[]{:S(2)}) collective-permute-start(bf16[192,768]{1,0:T(8,128)(2,1)} %half.2), channel_id=1, source_target_pairs={{0,448},{8,456},{16,464},{24,472},{32,480},{40,488},{48,496},{56,5... | collective-permute-start | bytes 884744 | tf_op jit(solution)/shard_map/ppermute | solution.py:286
  98.0 0.9 copy-start.2
  99.0 13.6 %collective-permute-start.7 = (bf16[192,768]{1,0:T(8,128)(2,1)}, bf16[192,768]{1,0:T(8,128)(2,1)}, u32[]{:S(2)}, u32[]{:S(2)}) collective-permute-start(bf16[192,768]{1,0:T(8,128)(2,1)} %half.3), channel_id=1, source_target_pairs={{0,64},{8,72},{16,80},{24,88},{32,96},{40,104},{48,112},{56,120},{... | collective-permute-start | bytes 884744 | tf_op jit(solution)/shard_map/ppermute | solution.py:287
  100.9 7.4 %copy-start.1 = (bf16[384,768]{1,0:T(8,128)(2,1)S(1)}, bf16[384,768]{1,0:T(8,128)(2,1)}, u32[]{:S(2)}) copy-start(bf16[384,768]{1,0:T(8,128)(2,1)} %copy-done) | copy-start | bytes 1769476
  100.9 7.4 %copy-start.3 = (bf16[384,768]{1,0:T(8,128)(2,1)S(1)}, bf16[384,768]{1,0:T(8,128)(2,1)}, u32[]{:S(2)}) copy-start(bf16[384,768]{1,0:T(8,128)(2,1)} %copy-done.2) | copy-start | bytes 1769476
  101.0 11.6 %copy-start.12 = (f32[1,768]{1,0:T(1,128)S(1)}, f32[1,768]{1,0:T(1,128)}, u32[]{:S(2)}) copy-start(f32[1,768]{1,0:T(1,128)} %scale.1) | copy-start | bytes 9220
  101.0 22.1 %collective-permute-start.10 = (bf16[384,768]{1,0:T(8,128)(2,1)S(1)}, bf16[384,768]{1,0:T(8,128)(2,1)S(1)}, u32[]{:S(2)}, u32[]{:S(2)}) collective-permute-start(bf16[384,768]{1,0:T(8,128)(2,1)S(1)} %get-tuple-element.7), channel_id=1, source_target_pairs={{0,64},{8,72},{16,80},{24,88},{32,96},{40,104},{48,112},{56,120},{... | collective-permute-start | bytes 1769480 | tf_op jit(solution)/shard_map/ppermute | solution.py:293
  103.1 20.1 %collective-permute-start.9 = (bf16[384,768]{1,0:T(8,128)(2,1)S(1)}, bf16[384,768]{1,0:T(8,128)(2,1)S(1)}, u32[]{:S(2)}, u32[]{:S(2)}) collective-permute-start(bf16[384,768]{1,0:T(8,128)(2,1)S(1)} %get-tuple-element.7), channel_id=1, source_target_pairs={{0,448},{8,456},{16,464},{24,472},{32,480},{40,488},{48,496},{56,5... | collective-permute-start | bytes 1769480 | tf_op jit(solution)/shard_map/ppermute | solution.py:293
  116.1 10.8 %collective-permute-start.12 = (bf16[512,768]{1,0:T(8,128)(2,1)S(1)}, bf16[512,768]{1,0:T(8,128)(2,1)S(1)}, u32[]{:S(2)}, u32[]{:S(2)}) collective-permute-start(bf16[512,768]{1,0:T(8,128)(2,1)S(1)} %convolution_convert_fusion), channel_id=1, source_target_pairs={{0,1},{1,0},{2,3},{3,2},{4,5},{5,4},{6,7},{7,6},{8,9},{9,8},{10,11... | collective-permute-start | bytes 2359304 | tf_op jit(solution)/shard_map/ppermute | solution.py:305
  125.0 7.1 %collective-permute-start.11 = (bf16[512,768]{1,0:T(8,128)(2,1)}, bf16[512,768]{1,0:T(8,128)(2,1)}, u32[]{:S(2)}, u32[]{:S(2)}) collective-permute-start(bf16[512,768]{1,0:T(8,128)(2,1)} %convolution_convert_fusion.1), channel_id=1, source_target_pairs={{0,1},{1,0},{2,3},{3,2},{4,5},{5,4},{6,7},{7,6},{8,9},{9,8},{10,11... | collective-permute-start | bytes 2359304 | tf_op jit(solution)/shard_map/ppermute | solution.py:305
  128.6 16.7 %all-to-all-start.3 = ((bf16[4,128,768]{2,1,0:T(8,128)(2,1)}), bf16[4,128,768]{2,1,0:T(8,128)(2,1)S(1)}, u32[]{:S(2)}, u32[]{:S(2)}) async-start(bf16[4,128,768]{2,1,0:T(8,128)(2,1)} %bitcast.16), calls=%async_computation.3 | async-start | bytes 1572864 | tf_op jit(solution)/shard_map/all_to_all | solution.py:36
  145.3 15.8 %all-to-all-start.2 = ((bf16[4,128,768]{2,1,0:T(8,128)(2,1)}), bf16[4,128,768]{2,1,0:T(8,128)(2,1)S(1)}, u32[]{:S(2)}, u32[]{:S(2)}) async-start(bf16[4,128,768]{2,1,0:T(8,128)(2,1)} %bitcast.15), calls=%async_computation.2 | async-start | bytes 1572864 | tf_op jit(solution)/shard_map/all_to_all | solution.py:36
  (4 other events, 3.0 us)

commit v7 on v6

--- a/solution.py
+++ b/solution.py
@@ -142,6 +142,32 @@
         compiler_params=pltpu.CompilerParams(vmem_limit_bytes=1 << 20),
         name="half",
     )(a)
+
+
+def stacked_kernel(*refs):
+    *blocks, out, sems = refs
+    rows = blocks[0].shape[0]
+    fetches = [
+        pltpu.make_async_copy(block, out.at[pl.ds(k * rows, rows)], sems.at[k]) for k, block in enumerate(blocks)
+    ]
+    for fetch in fetches:
+        fetch.start()
+    for fetch in fetches:
+        fetch.wait()
+
+
+def stacked(blocks):
+    rows, columns = blocks[0].shape
+    return pl.pallas_call(
+        stacked_kernel,
+        out_shape=jax.ShapeDtypeStruct((len(blocks) * rows, columns), blocks[0].dtype),
+        in_specs=[HBM] * len(blocks),
+        out_specs=VMEM,
+        scratch_shapes=[pltpu.SemaphoreType.DMA((len(blocks),))],
+        cost_estimate=cost(1 << 28, *blocks, *blocks),
+        compiler_params=pltpu.CompilerParams(vmem_limit_bytes=4 << 20),
+        name="stacked",
+    )(*blocks)
 
 
 TILE = 256
@@ -289,10 +315,9 @@
 
     copies = copies_of([down_piece, down_two])
     down_own, down_a = split(swapped(copies, "fs", ROW_GROUPS))
-    down_b = jnp.concatenate(
-        [lax.ppermute(down_own, PLANE, FROM_NEXT), lax.ppermute(down_own, PLANE, FROM_LAST)], 0
+    down_b = stacked(
+        [lax.ppermute(down_own, PLANE, FROM_NEXT), lax.ppermute(down_own, PLANE, FROM_LAST)]
     )
-    down_b = lax.optimization_barrier(down_b)
 
     early = early_of(other, own, (up_own, up_next, up_last))
     hidden = late_of(early, up_two, up_scale)
@@ -303,7 +328,8 @@
 
     def chunk(down, for_other):
         arrived = lax.ppermute(for_other, "tp", OTHER_CORE)
-        pair = (terms(hidden_own, down) + arrived.astype(F32)).astype(BF16)
+        mine = lax.optimization_barrier(terms(hidden_own, down))
+        pair = (mine + arrived.astype(F32)).astype(BF16)
         arrived = swapped(pair.reshape(X, rows, -1), "tp", X_GROUPS)
         return arrived.astype(F32).sum(axis=0).astype(BF16)
 

time: 163 us -> 164 us (level)
  other arithmetic: 3.02 us -> 6.23 us
  matrix products: 7.04 us -> 4.13 us
    convert_element_type x0 -> x2, other arithmetic: none -> 3.28 us  [chunk(): pair = (mine + arrived.astype(F32)).astype(BF16)]
    dot_general x4, matrix products: 7.04 us -> 4.13 us  [terms(): lax.dot_general(hidden, down, (((1,), (1,)), ((), ())), preferred_element...]
  transfers between devices with their start and end apart: 17 -> 17, of which waited for: 8 -> 8; matrix products, arithmetic and copies ran while one was open for 6% -> 7% of each run, Pallas kernels for 7% -> 7%
where the time goes in v7:
time: 164 us; the launch traced here: 163 us
  starting transfers between devices  69 us (42%)
  waiting for transfers between devices  61.6 us (38%)
  Pallas kernels  11.7 us (7%)
  local copies, waits for them, and re-layouts  9.52 us (6%)
  other arithmetic  6.23 us (4%)
  matrix products  4.13 us (3%)
    all_to_all x4, waiting for transfers between devices, swapped(): lax.all_to_all(blocks, axis, 0, 0, axis_index_groups=groups, tiled=True)  25.3 us
    all_to_all x4, starting transfers between devices, swapped(): lax.all_to_all(blocks, axis, 0, 0, axis_index_groups=groups, tiled=True)  21.1 us
    ppermute x1, waiting for transfers between devices, body(): up_next = lax.ppermute(up_own, PLANE, FROM_NEXT)  11.3 us
    ppermute x1, starting transfers between devices, body(): up_next = lax.ppermute(up_own, PLANE, FROM_NEXT)  10.9 us
    ppermute x1, waiting for transfers between devices, body(): lax.ppermute(normed, 'tp', X_NEXT)  10.4 us
    unnamed x38, local copies, waits for them, and re-layouts  8.03 us
    ppermute x1, starting transfers between devices, body(): lax.ppermute(half_of(up_next, 0), PLANE, FROM_NEXT)  5.59 us
    ppermute x1, waiting for transfers between devices, body(): down_two = lax.ppermute(down_piece, PLANE, FROM_TWO)  5.36 us
  transfers between devices with their start and end apart: 17, of which 8 were waited for; matrix products, arithmetic and copies ran while one was open for 7% of the time, Pallas kernels for 7%

profile of v7, /device:TPU:8, one launch (start us, length us, event | category | flops | bytes accessed | tf_op | source)
XLA Modules:
  0.0 162.6 jit_solution(3433602196970522760)
XLA Ops:
  1.8 9.2 %all-to-all-start = ((bf16[8,48,768]{2,1,0:T(8,128)(2,1)}), bf16[8,48,768]{2,1,0:T(8,128)(2,1)S(1)}, u32[]{:S(2)}, u32[]{:S(2)}) async-start(bf16[8,48,768]{2,1,0:T(8,128)(2,1)} %bitcast.1), calls=%async_computation | async-start | bytes 1179648 | tf_op jit(solution)/shard_map/all_to_all | solution.py:36
  11.1 4.4 %collective-permute-start.8 = (bf16[48,768]{1,0:T(8,128)(2,1)S(1)}, bf16[48,768]{1,0:T(8,128)(2,1)S(1)}, u32[]{:S(2)}, u32[]{:S(2)}) collective-permute-start(bf16[48,768]{1,0:T(8,128)(2,1)S(1)} %fusion.9.refs_0_), channel_id=1, source_target_pairs={{0,128},{8,136},{16,144},{24,152},{32,160},{40,168},{48,176},{56,1... | collective-permute-start | bytes 221192 | tf_op jit(solution)/shard_map/ppermute | solution.py:293
  17.3 5.4 %collective-permute-done.8.refs_1_ = bf16[48,768]{1,0:T(8,128)(2,1)S(1)} collective-permute-done((bf16[48,768]{1,0:T(8,128)(2,1)S(1)}, bf16[48,768]{1,0:T(8,128)(2,1)S(1)}, u32[]{:S(2)}, u32[]{:S(2)}) %collective-permute-start.8) | collective-permute-done | bytes 73760 | tf_op jit(solution)/shard_map/ppermute | solution.py:293
  22.7 1.1 copies.3
  23.8 3.0 %all-to-all-done = bf16[8,48,768]{2,1,0:T(8,128)(2,1)S(1)} async-done(((bf16[8,48,768]{2,1,0:T(8,128)(2,1)}), bf16[8,48,768]{2,1,0:T(8,128)(2,1)S(1)}, u32[]{:S(2)}, u32[]{:S(2)}) %all-to-all-start) | async-done | bytes 589856 | tf_op jit(solution)/shard_map/all_to_all | solution.py:36
  26.8 4.9 %all-to-all-start.1 = ((bf16[8,2,48,768]{3,2,1,0:T(8,128)(2,1)}), bf16[8,2,48,768]{3,2,1,0:T(8,128)(2,1)S(1)}, u32[]{:S(2)}, u32[]{:S(2)}) async-start(bf16[8,2,48,768]{3,2,1,0:T(8,128)(2,1)} %copies.3), calls=%async_computation.1 | async-start | bytes 2359296 | tf_op jit(solution)/shard_map/all_to_all | solution.py:36
  31.7 1.3 maximum_select_fusion.refs_0_
  33.0 4.7 %collective-permute-start = (bf16[128,1536]{1,0:T(8,128)(2,1)S(1)}, bf16[128,1536]{1,0:T(8,128)(2,1)S(1)}, u32[]{:S(2)}, u32[]{:S(2)}) collective-permute-start(bf16[128,1536]{1,0:T(8,128)(2,1)S(1)} %maximum_select_fusion.refs_0_), channel_id=1, source_target_pairs={{0,6},{1,7},{2,0},{3,1},{4,2},{5,3},{6,4},{7,5},{8,14},{9,15},{10,... | collective-permute-start | bytes 1179656 | tf_op jit(solution)/shard_map/ppermute | solution.py:302
  37.7 2.7 %collective-permute-start.1 = (bf16[128,1536]{1,0:T(8,128)(2,1)S(1)}, bf16[128,1536]{1,0:T(8,128)(2,1)S(1)}, u32[]{:S(2)}, u32[]{:S(2)}) collective-permute-start(bf16[128,1536]{1,0:T(8,128)(2,1)S(1)} %maximum_select_fusion.refs_0_), channel_id=1, source_target_pairs={{0,4},{1,5},{2,6},{3,7},{4,0},{5,1},{6,2},{7,3},{8,12},{9,13},{10,... | collective-permute-start | bytes 1179656 | tf_op jit(solution)/shard_map/ppermute | solution.py:303
  40.4 2.8 %collective-permute-start.2 = (bf16[128,1536]{1,0:T(8,128)(2,1)S(1)}, bf16[128,1536]{1,0:T(8,128)(2,1)S(1)}, u32[]{:S(2)}, u32[]{:S(2)}) collective-permute-start(bf16[128,1536]{1,0:T(8,128)(2,1)S(1)} %maximum_select_fusion.refs_0_), channel_id=1, source_target_pairs={{0,2},{1,3},{2,4},{3,5},{4,6},{5,7},{6,0},{7,1},{8,10},{9,11},{10,... | collective-permute-start | bytes 1179656 | tf_op jit(solution)/shard_map/ppermute | solution.py:304
  44.0 10.4 %collective-permute-done.refs_1_ = bf16[128,1536]{1,0:T(8,128)(2,1)S(1)} collective-permute-done((bf16[128,1536]{1,0:T(8,128)(2,1)S(1)}, bf16[128,1536]{1,0:T(8,128)(2,1)S(1)}, u32[]{:S(2)}, u32[]{:S(2)}) %collective-permute-start) | collective-permute-done | bytes 393248 | tf_op jit(solution)/shard_map/ppermute | solution.py:302
  55.9 4.1 %collective-permute-done.2.refs_3_ = bf16[128,1536]{1,0:T(8,128)(2,1)S(1)} collective-permute-done((bf16[128,1536]{1,0:T(8,128)(2,1)S(1)}, bf16[128,1536]{1,0:T(8,128)(2,1)S(1)}, u32[]{:S(2)}, u32[]{:S(2)}) %collective-permute-start.2) | collective-permute-done | bytes 393248 | tf_op jit(solution)/shard_map/ppermute | solution.py:304
  65.5 1.9 %collective-permute-start.3 = (bf16[512,1536]{1,0:T(8,128)(2,1)S(1)}, bf16[512,1536]{1,0:T(8,128)(2,1)}, u32[]{:S(2)}, u32[]{:S(2)}) collective-permute-start(bf16[512,1536]{1,0:T(8,128)(2,1)S(1)} %by_place.1.own), channel_id=1, source_target_pairs={{0,1},{1,0},{2,3},{3,2},{4,5},{5,4},{6,7},{7,6},{8,9},{9,8},{10,11... | collective-permute-start | bytes 4718600 | tf_op jit(solution)/shard_map/ppermute | solution.py:307
  67.5 10.9 %collective-permute-start.4 = (bf16[384,768]{1,0:T(8,128)(2,1)S(1)}, bf16[384,768]{1,0:T(8,128)(2,1)S(1)}, u32[]{:S(2)}, u32[]{:S(2)}) collective-permute-start(bf16[384,768]{1,0:T(8,128)(2,1)S(1)} %bitcast.12), channel_id=1, source_target_pairs={{0,448},{8,456},{16,464},{24,472},{32,480},{40,488},{48,496},{56,5... | collective-permute-start | bytes 1769480 | tf_op jit(solution)/shard_map/ppermute | solution.py:309
  78.4 1.9 %collective-permute-start.5 = (bf16[384,768]{1,0:T(8,128)(2,1)S(1)}, bf16[384,768]{1,0:T(8,128)(2,1)S(1)}, u32[]{:S(2)}, u32[]{:S(2)}) collective-permute-start(bf16[384,768]{1,0:T(8,128)(2,1)S(1)} %bitcast.13), channel_id=1, source_target_pairs={{0,64},{8,72},{16,80},{24,88},{32,96},{40,104},{48,112},{56,120},{... | collective-permute-start | bytes 1769480 | tf_op jit(solution)/shard_map/ppermute | solution.py:310
  80.4 11.3 %collective-permute-done.4.u1.a = bf16[384,768]{1,0:T(8,128)(2,1)S(1)} collective-permute-done((bf16[384,768]{1,0:T(8,128)(2,1)S(1)}, bf16[384,768]{1,0:T(8,128)(2,1)S(1)}, u32[]{:S(2)}, u32[]{:S(2)}) %collective-permute-start.4) | collective-permute-done | bytes 589856 | tf_op jit(solution)/shard_map/ppermute | solution.py:309
  92.4 5.6 %collective-permute-start.6 = (bf16[192,768]{1,0:T(8,128)(2,1)}, bf16[192,768]{1,0:T(8,128)(2,1)}, u32[]{:S(2)}, u32[]{:S(2)}) collective-permute-start(bf16[192,768]{1,0:T(8,128)(2,1)} %half.2), channel_id=1, source_target_pairs={{0,448},{8,456},{16,464},{24,472},{32,480},{40,488},{48,496},{56,5... | collective-permute-start | bytes 884744 | tf_op jit(solution)/shard_map/ppermute | solution.py:312
  99.0 1.9 %collective-permute-start.7 = (bf16[192,768]{1,0:T(8,128)(2,1)}, bf16[192,768]{1,0:T(8,128)(2,1)}, u32[]{:S(2)}, u32[]{:S(2)}) collective-permute-start(bf16[192,768]{1,0:T(8,128)(2,1)} %half.3), channel_id=1, source_target_pairs={{0,64},{8,72},{16,80},{24,88},{32,96},{40,104},{48,112},{56,120},{... | collective-permute-start | bytes 884744 | tf_op jit(solution)/shard_map/ppermute | solution.py:313
  101.0 2.1 %collective-permute-start.10 = (bf16[384,768]{1,0:T(8,128)(2,1)S(1)}, bf16[384,768]{1,0:T(8,128)(2,1)S(1)}, u32[]{:S(2)}, u32[]{:S(2)}) collective-permute-start(bf16[384,768]{1,0:T(8,128)(2,1)S(1)} %get-tuple-element.7), channel_id=1, source_target_pairs={{0,64},{8,72},{16,80},{24,88},{32,96},{40,104},{48,112},{56,120},{... | collective-permute-start | bytes 1769480 | tf_op jit(solution)/shard_map/ppermute | solution.py:319
  103.1 5.1 %collective-permute-start.9 = (bf16[384,768]{1,0:T(8,128)(2,1)S(1)}, bf16[384,768]{1,0:T(8,128)(2,1)S(1)}, u32[]{:S(2)}, u32[]{:S(2)}) collective-permute-start(bf16[384,768]{1,0:T(8,128)(2,1)S(1)} %get-tuple-element.7), channel_id=1, source_target_pairs={{0,448},{8,456},{16,464},{24,472},{32,480},{40,488},{48,496},{56,5... | collective-permute-start | bytes 1769480 | tf_op jit(solution)/shard_map/ppermute | solution.py:319
  108.3 4.3 %early.1 = bf16[1024,1152]{1,0:T(8,128)(2,1)S(1)} custom-call(bf16[512,1536]{1,0:T(8,128)(2,1)} %collective-permute-done.3.other, bf16[512,1536]{1,0:T(8,128)(2,1)S(1)} %by_place.1.own, bf16[384,768]{1,0:T(8,128)(2,1)S(1)} %bitcast.14, bf16[384,768]{1,0:T(8,128)(2,1)S(1)} %copy-done.1, bf16[384,768]{1,0:T(8,128)(2,1)S(1)} %copy-done.3), custom_call_target="tpu_custom_call" | custom-call | flops 1811939328 | bytes 4915200 | tf_op jit(solution)/shard_map/early/pallas_call | solution.py:214
  112.6 2.7 %late.1 = bf16[1024,768]{1,0:T(8,128)(2,1)S(1)} custom-call(bf16[1024,1152]{1,0:T(8,128)(2,1)S(1)} %early.1, bf16[192,768]{1,0:T(8,128)(2,1)} %collective-permute-done.6.u2_top, bf16[192,768]{1,0:T(8,128)(2,1)} %collective-permute-done.7.u2_bottom, f32[1,768]{1,0:T(1,128)S(1)} %copy-done.12), custom_call_target="tpu_custom_call" | custom-call | flops 603979776 | bytes 4521984 | tf_op jit(solution)/shard_map/late/pallas_call | solution.py:266
  116.1 1.9 %collective-permute-start.12 = (bf16[512,768]{1,0:T(8,128)(2,1)S(1)}, bf16[512,768]{1,0:T(8,128)(2,1)S(1)}, u32[]{:S(2)}, u32[]{:S(2)}) collective-permute-start(bf16[512,768]{1,0:T(8,128)(2,1)S(1)} %convolution_convert_fusion), channel_id=1, source_target_pairs={{0,1},{1,0},{2,3},{3,2},{4,5},{5,4},{6,7},{7,6},{8,9},{9,8},{10,11... | collective-permute-start | bytes 2359304 | tf_op jit(solution)/shard_map/ppermute | solution.py:330
  118.0 5.1 %collective-permute-done.10.refs_1_ = bf16[384,768]{1,0:T(8,128)(2,1)S(1)} collective-permute-done((bf16[384,768]{1,0:T(8,128)(2,1)S(1)}, bf16[384,768]{1,0:T(8,128)(2,1)S(1)}, u32[]{:S(2)}, u32[]{:S(2)}) %collective-permute-start.10) | collective-permute-done | bytes 589856 | tf_op jit(solution)/shard_map/ppermute | solution.py:319
  123.4 1.7 %convolution_convert_fusion.1 = bf16[512,768]{1,0:T(8,128)(2,1)} fusion(bf16[768,768]{1,0:T(8,128)(2,1)S(1)} %stacked.1, bf16[1024,768]{1,0:T(8,128)(2,1)S(1)} %late.1), kind=kOutput, calls=%fused_computation.3 | convolution fusion | flops 604372992 | bytes 2752512 | tf_op jit(solution)/shard_map/dot_general | solution.py:327
  125.1 1.9 %collective-permute-start.11 = (bf16[512,768]{1,0:T(8,128)(2,1)}, bf16[512,768]{1,0:T(8,128)(2,1)}, u32[]{:S(2)}, u32[]{:S(2)}) collective-permute-start(bf16[512,768]{1,0:T(8,128)(2,1)} %convolution_convert_fusion.1), channel_id=1, source_target_pairs={{0,1},{1,0},{2,3},{3,2},{4,5},{5,4},{6,7},{7,6},{8,9},{9,8},{10,11... | collective-permute-start | bytes 2359304 | tf_op jit(solution)/shard_map/ppermute | solution.py:330
  127.9 1.1 add_convert_fusion
  128.9 3.5 %all-to-all-start.3 = ((bf16[4,128,768]{2,1,0:T(8,128)(2,1)}), bf16[4,128,768]{2,1,0:T(8,128)(2,1)S(1)}, u32[]{:S(2)}, u32[]{:S(2)}) async-start(bf16[4,128,768]{2,1,0:T(8,128)(2,1)} %bitcast.15), calls=%async_computation.3 | async-start | bytes 1572864 | tf_op jit(solution)/shard_map/all_to_all | solution.py:36
  133.3 2.2 %add_convert_fusion.1 = bf16[512,768]{1,0:T(8,128)(2,1)} fusion(f32[512,768]{1,0:T(8,128)S(1)} %fusion.7, bf16[512,768]{1,0:T(8,128)(2,1)} %collective-permute-done.11), kind=kLoop, calls=%fused_computation.1 | loop fusion | flops 1179648 | bytes 3145728 | tf_op jit(solution)/shard_map/convert_element_type | solution.py:332
  135.5 10.1 %all-to-all-done.3 = bf16[4,128,768]{2,1,0:T(8,128)(2,1)S(1)} async-done(((bf16[4,128,768]{2,1,0:T(8,128)(2,1)}), bf16[4,128,768]{2,1,0:T(8,128)(2,1)S(1)}, u32[]{:S(2)}, u32[]{:S(2)}) %all-to-all-start.3) | async-done | bytes 786464 | tf_op jit(solution)/shard_map/all_to_all | solution.py:36
  145.6 3.5 %all-to-all-start.2 = ((bf16[4,128,768]{2,1,0:T(8,128)(2,1)}), bf16[4,128,768]{2,1,0:T(8,128)(2,1)S(1)}, u32[]{:S(2)}, u32[]{:S(2)}) async-start(bf16[4,128,768]{2,1,0:T(8,128)(2,1)} %bitcast.5), calls=%async_computation.2 | async-start | bytes 1572864 | tf_op jit(solution)/shard_map/all_to_all | solution.py:36
  149.3 12.1 %all-to-all-done.2 = bf16[4,128,768]{2,1,0:T(8,128)(2,1)S(1)} async-done(((bf16[4,128,768]{2,1,0:T(8,128)(2,1)}), bf16[4,128,768]{2,1,0:T(8,128)(2,1)S(1)}, u32[]{:S(2)}, u32[]{:S(2)}) %all-to-all-start.2) | async-done | bytes 786464 | tf_op jit(solution)/shard_map/all_to_all | solution.py:36
  (68 shorter events, 17.2 us)
Async XLA Ops:
  0.0 0.9 copy-start.13
  0.9 10.1 %copy-start.16 = (f32[768,48]{0,1:T(8,128)S(1)}, f32[768,48]{0,1:T(8,128)}, u32[]{:S(2)}) copy-start(f32[768,48]{0,1:T(8,128)} %param.10) | copy-start | bytes 442372
  0.9 10.1 %copy-start.18 = (f32[1,48]{1,0:T(1,128)S(1)}, f32[1,48]{1,0:T(1,128)}, u32[]{:S(2)}) copy-start(f32[1,48]{1,0:T(1,128)} %param.11) | copy-start | bytes 580
  0.9 14.6 %copy-start.14 = (bf16[128,1536]{1,0:T(8,128)(2,1)S(1)}, bf16[128,1536]{1,0:T(8,128)(2,1)}, u32[]{:S(2)}) copy-start(bf16[128,1536]{1,0:T(8,128)(2,1)} %param.6) | copy-start | bytes 1179652
  0.9 14.8 %copy-start.17 = (f32[1536]{0:T(1024)S(1)}, f32[1536]{0:T(1024)}, u32[]{:S(2)}) copy-start(f32[1536]{0:T(1024)} %param.7) | copy-start | bytes 18436
  1.8 25.0 %all-to-all-start = ((bf16[8,48,768]{2,1,0:T(8,128)(2,1)}), bf16[8,48,768]{2,1,0:T(8,128)(2,1)S(1)}, u32[]{:S(2)}, u32[]{:S(2)}) async-start(bf16[8,48,768]{2,1,0:T(8,128)(2,1)} %bitcast.1), calls=%async_computation | async-start | bytes 1179648 | tf_op jit(solution)/shard_map/all_to_all | solution.py:36
  11.1 11.6 %collective-permute-start.8 = (bf16[48,768]{1,0:T(8,128)(2,1)S(1)}, bf16[48,768]{1,0:T(8,128)(2,1)S(1)}, u32[]{:S(2)}, u32[]{:S(2)}) collective-permute-start(bf16[48,768]{1,0:T(8,128)(2,1)S(1)} %fusion.9.refs_0_), channel_id=1, source_target_pairs={{0,128},{8,136},{16,144},{24,152},{32,160},{40,168},{48,176},{56,1... | collective-permute-start | bytes 221192 | tf_op jit(solution)/shard_map/ppermute | solution.py:293
  17.3 14.4 %copy-start.15 = (bf16[128,384]{1,0:T(8,128)(2,1)S(1)}, bf16[128,384]{1,0:T(8,128)(2,1)}, u32[]{:S(2)}) copy-start(bf16[128,384]{1,0:T(8,128)(2,1)} %get-tuple-element.11) | copy-start | bytes 294916
  26.8 74.1 %all-to-all-start.1 = ((bf16[8,2,48,768]{3,2,1,0:T(8,128)(2,1)}), bf16[8,2,48,768]{3,2,1,0:T(8,128)(2,1)S(1)}, u32[]{:S(2)}, u32[]{:S(2)}) async-start(bf16[8,2,48,768]{3,2,1,0:T(8,128)(2,1)} %copies.3), calls=%async_computation.1 | async-start | bytes 2359296 | tf_op jit(solution)/shard_map/all_to_all | solution.py:36
  33.0 21.4 %collective-permute-start = (bf16[128,1536]{1,0:T(8,128)(2,1)S(1)}, bf16[128,1536]{1,0:T(8,128)(2,1)S(1)}, u32[]{:S(2)}, u32[]{:S(2)}) collective-permute-start(bf16[128,1536]{1,0:T(8,128)(2,1)S(1)} %maximum_select_fusion.refs_0_), channel_id=1, source_target_pairs={{0,6},{1,7},{2,0},{3,1},{4,2},{5,3},{6,4},{7,5},{8,14},{9,15},{10,... | collective-permute-start | bytes 1179656 | tf_op jit(solution)/shard_map/ppermute | solution.py:302
  37.7 17.4 %collective-permute-start.1 = (bf16[128,1536]{1,0:T(8,128)(2,1)S(1)}, bf16[128,1536]{1,0:T(8,128)(2,1)S(1)}, u32[]{:S(2)}, u32[]{:S(2)}) collective-permute-start(bf16[128,1536]{1,0:T(8,128)(2,1)S(1)} %maximum_select_fusion.refs_0_), channel_id=1, source_target_pairs={{0,4},{1,5},{2,6},{3,7},{4,0},{5,1},{6,2},{7,3},{8,12},{9,13},{10,... | collective-permute-start | bytes 1179656 | tf_op jit(solution)/shard_map/ppermute | solution.py:303
  40.4 19.6 %collective-permute-start.2 = (bf16[128,1536]{1,0:T(8,128)(2,1)S(1)}, bf16[128,1536]{1,0:T(8,128)(2,1)S(1)}, u32[]{:S(2)}, u32[]{:S(2)}) collective-permute-start(bf16[128,1536]{1,0:T(8,128)(2,1)S(1)} %maximum_select_fusion.refs_0_), channel_id=1, source_target_pairs={{0,2},{1,3},{2,4},{3,5},{4,6},{5,7},{6,0},{7,1},{8,10},{9,11},{10,... | collective-permute-start | bytes 1179656 | tf_op jit(solution)/shard_map/ppermute | solution.py:304
  60.8 1.0 copy-start.5
  61.8 1.0 copy-start.7
  62.7 1.0 copy-start.9
  63.7 1.0 copy-start.11
  65.5 42.7 %collective-permute-start.3 = (bf16[512,1536]{1,0:T(8,128)(2,1)S(1)}, bf16[512,1536]{1,0:T(8,128)(2,1)}, u32[]{:S(2)}, u32[]{:S(2)}) collective-permute-start(bf16[512,1536]{1,0:T(8,128)(2,1)S(1)} %by_place.1.own), channel_id=1, source_target_pairs={{0,1},{1,0},{2,3},{3,2},{4,5},{5,4},{6,7},{7,6},{8,9},{9,8},{10,11... | collective-permute-start | bytes 4718600 | tf_op jit(solution)/shard_map/ppermute | solution.py:307
  67.5 24.2 %collective-permute-start.4 = (bf16[384,768]{1,0:T(8,128)(2,1)S(1)}, bf16[384,768]{1,0:T(8,128)(2,1)S(1)}, u32[]{:S(2)}, u32[]{:S(2)}) collective-permute-start(bf16[384,768]{1,0:T(8,128)(2,1)S(1)} %bitcast.12), channel_id=1, source_target_pairs={{0,448},{8,456},{16,464},{24,472},{32,480},{40,488},{48,496},{56,5... | collective-permute-start | bytes 1769480 | tf_op jit(solution)/shard_map/ppermute | solution.py:309
  78.4 19.6 %collective-permute-start.5 = (bf16[384,768]{1,0:T(8,128)(2,1)S(1)}, bf16[384,768]{1,0:T(8,128)(2,1)S(1)}, u32[]{:S(2)}, u32[]{:S(2)}) collective-permute-start(bf16[384,768]{1,0:T(8,128)(2,1)S(1)} %bitcast.13), channel_id=1, source_target_pairs={{0,64},{8,72},{16,80},{24,88},{32,96},{40,104},{48,112},{56,120},{... | collective-permute-start | bytes 1769480 | tf_op jit(solution)/shard_map/ppermute | solution.py:310
  91.6 7.2 %copy-start = (bf16[384,768]{1,0:T(8,128)(2,1)}, bf16[384,768]{1,0:T(8,128)(2,1)S(1)}, u32[]{:S(2)}) copy-start(bf16[384,768]{1,0:T(8,128)(2,1)S(1)} %collective-permute-done.4.u1.a) | copy-start | bytes 1769476
  92.4 20.1 %collective-permute-start.6 = (bf16[192,768]{1,0:T(8,128)(2,1)}, bf16[192,768]{1,0:T(8,128)(2,1)}, u32[]{:S(2)}, u32[]{:S(2)}) collective-permute-start(bf16[192,768]{1,0:T(8,128)(2,1)} %half.2), channel_id=1, source_target_pairs={{0,448},{8,456},{16,464},{24,472},{32,480},{40,488},{48,496},{56,5... | collective-permute-start | bytes 884744 | tf_op jit(solution)/shard_map/ppermute | solution.py:312
  98.0 0.9 copy-start.2
  99.0 13.6 %collective-permute-start.7 = (bf16[192,768]{1,0:T(8,128)(2,1)}, bf16[192,768]{1,0:T(8,128)(2,1)}, u32[]{:S(2)}, u32[]{:S(2)}) collective-permute-start(bf16[192,768]{1,0:T(8,128)(2,1)} %half.3), channel_id=1, source_target_pairs={{0,64},{8,72},{16,80},{24,88},{32,96},{40,104},{48,112},{56,120},{... | collective-permute-start | bytes 884744 | tf_op jit(solution)/shard_map/ppermute | solution.py:313
  100.9 7.4 %copy-start.1 = (bf16[384,768]{1,0:T(8,128)(2,1)S(1)}, bf16[384,768]{1,0:T(8,128)(2,1)}, u32[]{:S(2)}) copy-start(bf16[384,768]{1,0:T(8,128)(2,1)} %copy-done) | copy-start | bytes 1769476
  100.9 7.4 %copy-start.3 = (bf16[384,768]{1,0:T(8,128)(2,1)S(1)}, bf16[384,768]{1,0:T(8,128)(2,1)}, u32[]{:S(2)}) copy-start(bf16[384,768]{1,0:T(8,128)(2,1)} %copy-done.2) | copy-start | bytes 1769476
  101.0 11.6 %copy-start.12 = (f32[1,768]{1,0:T(1,128)S(1)}, f32[1,768]{1,0:T(1,128)}, u32[]{:S(2)}) copy-start(f32[1,768]{1,0:T(1,128)} %scale.1) | copy-start | bytes 9220
  101.0 22.1 %collective-permute-start.10 = (bf16[384,768]{1,0:T(8,128)(2,1)S(1)}, bf16[384,768]{1,0:T(8,128)(2,1)S(1)}, u32[]{:S(2)}, u32[]{:S(2)}) collective-permute-start(bf16[384,768]{1,0:T(8,128)(2,1)S(1)} %get-tuple-element.7), channel_id=1, source_target_pairs={{0,64},{8,72},{16,80},{24,88},{32,96},{40,104},{48,112},{56,120},{... | collective-permute-start | bytes 1769480 | tf_op jit(solution)/shard_map/ppermute | solution.py:319
  103.1 20.1 %collective-permute-start.9 = (bf16[384,768]{1,0:T(8,128)(2,1)S(1)}, bf16[384,768]{1,0:T(8,128)(2,1)S(1)}, u32[]{:S(2)}, u32[]{:S(2)}) collective-permute-start(bf16[384,768]{1,0:T(8,128)(2,1)S(1)} %get-tuple-element.7), channel_id=1, source_target_pairs={{0,448},{8,456},{16,464},{24,472},{32,480},{40,488},{48,496},{56,5... | collective-permute-start | bytes 1769480 | tf_op jit(solution)/shard_map/ppermute | solution.py:319
  116.1 11.8 %collective-permute-start.12 = (bf16[512,768]{1,0:T(8,128)(2,1)S(1)}, bf16[512,768]{1,0:T(8,128)(2,1)S(1)}, u32[]{:S(2)}, u32[]{:S(2)}) collective-permute-start(bf16[512,768]{1,0:T(8,128)(2,1)S(1)} %convolution_convert_fusion), channel_id=1, source_target_pairs={{0,1},{1,0},{2,3},{3,2},{4,5},{5,4},{6,7},{7,6},{8,9},{9,8},{10,11... | collective-permute-start | bytes 2359304 | tf_op jit(solution)/shard_map/ppermute | solution.py:330
  125.1 8.1 %collective-permute-start.11 = (bf16[512,768]{1,0:T(8,128)(2,1)}, bf16[512,768]{1,0:T(8,128)(2,1)}, u32[]{:S(2)}, u32[]{:S(2)}) collective-permute-start(bf16[512,768]{1,0:T(8,128)(2,1)} %convolution_convert_fusion.1), channel_id=1, source_target_pairs={{0,1},{1,0},{2,3},{3,2},{4,5},{5,4},{6,7},{7,6},{8,9},{9,8},{10,11... | collective-permute-start | bytes 2359304 | tf_op jit(solution)/shard_map/ppermute | solution.py:330
  128.9 16.7 %all-to-all-start.3 = ((bf16[4,128,768]{2,1,0:T(8,128)(2,1)}), bf16[4,128,768]{2,1,0:T(8,128)(2,1)S(1)}, u32[]{:S(2)}, u32[]{:S(2)}) async-start(bf16[4,128,768]{2,1,0:T(8,128)(2,1)} %bitcast.15), calls=%async_computation.3 | async-start | bytes 1572864 | tf_op jit(solution)/shard_map/all_to_all | solution.py:36
  145.6 15.8 %all-to-all-start.2 = ((bf16[4,128,768]{2,1,0:T(8,128)(2,1)}), bf16[4,128,768]{2,1,0:T(8,128)(2,1)S(1)}, u32[]{:S(2)}, u32[]{:S(2)}) async-start(bf16[4,128,768]{2,1,0:T(8,128)(2,1)} %bitcast.5), calls=%async_computation.2 | async-start | bytes 1572864 | tf_op jit(solution)/shard_map/all_to_all | solution.py:36
  (4 other events, 3.0 us)

commit v8 on v7

--- a/solution.py
+++ b/solution.py
@@ -170,7 +170,7 @@
     )(*blocks)
 
 
-TILE = 256
+TILE = 512
 
 
 def fetched(sources, target, sems):
@@ -214,7 +214,7 @@
     return pl.pallas_call(
         functools.partial(early_kernel, half),
         grid=(2 * half,),
-        out_shape=jax.ShapeDtypeStruct(shape, BF16),
+        out_shape=pltpu.HBM(shape, BF16),
         in_specs=[
             pl.BlockSpec((TILE, d), lambda i: (jnp.minimum(i, half - 1), 0)),
             pl.BlockSpec((TILE, d), lambda i: (jnp.maximum(i - half, 0), 0)),
@@ -277,7 +277,7 @@
         compiler_params=pltpu.CompilerParams(vmem_limit_bytes=12 << 20),
         cost_estimate=cost(4 * early.shape[0] * width * columns, early, *halves, out),
         name="late",
-    )(early, *halves, scale)
+    )(pltpu.with_memory_space_constraint(early, pltpu.HBM), *halves, scale)
 
 
 def body(tokens, norm_gain, up_weight, up_scale, down_weight, down_scale):

time: 164 us -> 164 us (level)
  no operation moved by 1% of the time
where the time goes in v8:
time: 164 us; the launch traced here: 163 us
  starting transfers between devices  69 us (42%)
  waiting for transfers between devices  60.6 us (37%)
  Pallas kernels  12.7 us (8%)
  local copies, waits for them, and re-layouts  9.5 us (6%)
  other arithmetic  6.23 us (4%)
  matrix products  4.12 us (3%)
    all_to_all x4, waiting for transfers between devices, swapped(): lax.all_to_all(blocks, axis, 0, 0, axis_index_groups=groups, tiled=True)  25.3 us
    all_to_all x4, starting transfers between devices, swapped(): lax.all_to_all(blocks, axis, 0, 0, axis_index_groups=groups, tiled=True)  21.1 us
    ppermute x1, waiting for transfers between devices, body(): up_next = lax.ppermute(up_own, PLANE, FROM_NEXT)  11.3 us
    ppermute x1, starting transfers between devices, body(): up_next = lax.ppermute(up_own, PLANE, FROM_NEXT)  10.9 us
    ppermute x1, waiting for transfers between devices, body(): lax.ppermute(normed, 'tp', X_NEXT)  10.4 us
    unnamed x38, local copies, waits for them, and re-layouts  8.01 us
    ppermute x1, starting transfers between devices, body(): lax.ppermute(half_of(up_next, 0), PLANE, FROM_NEXT)  5.59 us
    ppermute x1, waiting for transfers between devices, body(): down_two = lax.ppermute(down_piece, PLANE, FROM_TWO)  5.36 us
  transfers between devices with their start and end apart: 17, of which 8 were waited for; matrix products, arithmetic and copies ran while one was open for 7% of the time, Pallas kernels for 7%

profile of v8, /device:TPU:8, one launch (start us, length us, event | category | flops | bytes accessed | tf_op | source)
XLA Modules:
  0.0 162.6 jit_solution(18240546523039016132)
XLA Ops:
  1.8 9.2 %all-to-all-start = ((bf16[8,48,768]{2,1,0:T(8,128)(2,1)}), bf16[8,48,768]{2,1,0:T(8,128)(2,1)S(1)}, u32[]{:S(2)}, u32[]{:S(2)}) async-start(bf16[8,48,768]{2,1,0:T(8,128)(2,1)} %bitcast.1), calls=%async_computation | async-start | bytes 1179648 | tf_op jit(solution)/shard_map/all_to_all | solution.py:36
  11.1 4.4 %collective-permute-start.8 = (bf16[48,768]{1,0:T(8,128)(2,1)S(1)}, bf16[48,768]{1,0:T(8,128)(2,1)S(1)}, u32[]{:S(2)}, u32[]{:S(2)}) collective-permute-start(bf16[48,768]{1,0:T(8,128)(2,1)S(1)} %fusion.9.refs_0_), channel_id=1, source_target_pairs={{0,128},{8,136},{16,144},{24,152},{32,160},{40,168},{48,176},{56,1... | collective-permute-start | bytes 221192 | tf_op jit(solution)/shard_map/ppermute | solution.py:293
  17.3 5.4 %collective-permute-done.8.refs_1_ = bf16[48,768]{1,0:T(8,128)(2,1)S(1)} collective-permute-done((bf16[48,768]{1,0:T(8,128)(2,1)S(1)}, bf16[48,768]{1,0:T(8,128)(2,1)S(1)}, u32[]{:S(2)}, u32[]{:S(2)}) %collective-permute-start.8) | collective-permute-done | bytes 73760 | tf_op jit(solution)/shard_map/ppermute | solution.py:293
  22.7 1.1 copies.3
  23.8 3.0 %all-to-all-done = bf16[8,48,768]{2,1,0:T(8,128)(2,1)S(1)} async-done(((bf16[8,48,768]{2,1,0:T(8,128)(2,1)}), bf16[8,48,768]{2,1,0:T(8,128)(2,1)S(1)}, u32[]{:S(2)}, u32[]{:S(2)}) %all-to-all-start) | async-done | bytes 589856 | tf_op jit(solution)/shard_map/all_to_all | solution.py:36
  26.8 4.9 %all-to-all-start.1 = ((bf16[8,2,48,768]{3,2,1,0:T(8,128)(2,1)}), bf16[8,2,48,768]{3,2,1,0:T(8,128)(2,1)S(1)}, u32[]{:S(2)}, u32[]{:S(2)}) async-start(bf16[8,2,48,768]{3,2,1,0:T(8,128)(2,1)} %copies.3), calls=%async_computation.1 | async-start | bytes 2359296 | tf_op jit(solution)/shard_map/all_to_all | solution.py:36
  31.7 1.3 maximum_select_fusion.refs_0_
  33.0 4.7 %collective-permute-start = (bf16[128,1536]{1,0:T(8,128)(2,1)S(1)}, bf16[128,1536]{1,0:T(8,128)(2,1)S(1)}, u32[]{:S(2)}, u32[]{:S(2)}) collective-permute-start(bf16[128,1536]{1,0:T(8,128)(2,1)S(1)} %maximum_select_fusion.refs_0_), channel_id=1, source_target_pairs={{0,6},{1,7},{2,0},{3,1},{4,2},{5,3},{6,4},{7,5},{8,14},{9,15},{10,... | collective-permute-start | bytes 1179656 | tf_op jit(solution)/shard_map/ppermute | solution.py:302
  37.7 2.7 %collective-permute-start.1 = (bf16[128,1536]{1,0:T(8,128)(2,1)S(1)}, bf16[128,1536]{1,0:T(8,128)(2,1)S(1)}, u32[]{:S(2)}, u32[]{:S(2)}) collective-permute-start(bf16[128,1536]{1,0:T(8,128)(2,1)S(1)} %maximum_select_fusion.refs_0_), channel_id=1, source_target_pairs={{0,4},{1,5},{2,6},{3,7},{4,0},{5,1},{6,2},{7,3},{8,12},{9,13},{10,... | collective-permute-start | bytes 1179656 | tf_op jit(solution)/shard_map/ppermute | solution.py:303
  40.4 2.8 %collective-permute-start.2 = (bf16[128,1536]{1,0:T(8,128)(2,1)S(1)}, bf16[128,1536]{1,0:T(8,128)(2,1)S(1)}, u32[]{:S(2)}, u32[]{:S(2)}) collective-permute-start(bf16[128,1536]{1,0:T(8,128)(2,1)S(1)} %maximum_select_fusion.refs_0_), channel_id=1, source_target_pairs={{0,2},{1,3},{2,4},{3,5},{4,6},{5,7},{6,0},{7,1},{8,10},{9,11},{10,... | collective-permute-start | bytes 1179656 | tf_op jit(solution)/shard_map/ppermute | solution.py:304
  44.0 10.4 %collective-permute-done.refs_1_ = bf16[128,1536]{1,0:T(8,128)(2,1)S(1)} collective-permute-done((bf16[128,1536]{1,0:T(8,128)(2,1)S(1)}, bf16[128,1536]{1,0:T(8,128)(2,1)S(1)}, u32[]{:S(2)}, u32[]{:S(2)}) %collective-permute-start) | collective-permute-done | bytes 393248 | tf_op jit(solution)/shard_map/ppermute | solution.py:302
  55.9 4.1 %collective-permute-done.2.refs_3_ = bf16[128,1536]{1,0:T(8,128)(2,1)S(1)} collective-permute-done((bf16[128,1536]{1,0:T(8,128)(2,1)S(1)}, bf16[128,1536]{1,0:T(8,128)(2,1)S(1)}, u32[]{:S(2)}, u32[]{:S(2)}) %collective-permute-start.2) | collective-permute-done | bytes 393248 | tf_op jit(solution)/shard_map/ppermute | solution.py:304
  65.5 1.9 %collective-permute-start.3 = (bf16[512,1536]{1,0:T(8,128)(2,1)S(1)}, bf16[512,1536]{1,0:T(8,128)(2,1)}, u32[]{:S(2)}, u32[]{:S(2)}) collective-permute-start(bf16[512,1536]{1,0:T(8,128)(2,1)S(1)} %by_place.1.own), channel_id=1, source_target_pairs={{0,1},{1,0},{2,3},{3,2},{4,5},{5,4},{6,7},{7,6},{8,9},{9,8},{10,11... | collective-permute-start | bytes 4718600 | tf_op jit(solution)/shard_map/ppermute | solution.py:307
  67.5 10.9 %collective-permute-start.4 = (bf16[384,768]{1,0:T(8,128)(2,1)S(1)}, bf16[384,768]{1,0:T(8,128)(2,1)S(1)}, u32[]{:S(2)}, u32[]{:S(2)}) collective-permute-start(bf16[384,768]{1,0:T(8,128)(2,1)S(1)} %bitcast.12), channel_id=1, source_target_pairs={{0,448},{8,456},{16,464},{24,472},{32,480},{40,488},{48,496},{56,5... | collective-permute-start | bytes 1769480 | tf_op jit(solution)/shard_map/ppermute | solution.py:309
  78.4 1.9 %collective-permute-start.5 = (bf16[384,768]{1,0:T(8,128)(2,1)S(1)}, bf16[384,768]{1,0:T(8,128)(2,1)S(1)}, u32[]{:S(2)}, u32[]{:S(2)}) collective-permute-start(bf16[384,768]{1,0:T(8,128)(2,1)S(1)} %bitcast.13), channel_id=1, source_target_pairs={{0,64},{8,72},{16,80},{24,88},{32,96},{40,104},{48,112},{56,120},{... | collective-permute-start | bytes 1769480 | tf_op jit(solution)/shard_map/ppermute | solution.py:310
  80.4 11.3 %collective-permute-done.4.u1.a = bf16[384,768]{1,0:T(8,128)(2,1)S(1)} collective-permute-done((bf16[384,768]{1,0:T(8,128)(2,1)S(1)}, bf16[384,768]{1,0:T(8,128)(2,1)S(1)}, u32[]{:S(2)}, u32[]{:S(2)}) %collective-permute-start.4) | collective-permute-done | bytes 589856 | tf_op jit(solution)/shard_map/ppermute | solution.py:309
  92.4 5.6 %collective-permute-start.6 = (bf16[192,768]{1,0:T(8,128)(2,1)}, bf16[192,768]{1,0:T(8,128)(2,1)}, u32[]{:S(2)}, u32[]{:S(2)}) collective-permute-start(bf16[192,768]{1,0:T(8,128)(2,1)} %half.2), channel_id=1, source_target_pairs={{0,448},{8,456},{16,464},{24,472},{32,480},{40,488},{48,496},{56,5... | collective-permute-start | bytes 884744 | tf_op jit(solution)/shard_map/ppermute | solution.py:312
  99.0 1.9 %collective-permute-start.7 = (bf16[192,768]{1,0:T(8,128)(2,1)}, bf16[192,768]{1,0:T(8,128)(2,1)}, u32[]{:S(2)}, u32[]{:S(2)}) collective-permute-start(bf16[192,768]{1,0:T(8,128)(2,1)} %half.3), channel_id=1, source_target_pairs={{0,64},{8,72},{16,80},{24,88},{32,96},{40,104},{48,112},{56,120},{... | collective-permute-start | bytes 884744 | tf_op jit(solution)/shard_map/ppermute | solution.py:313
  101.0 2.1 %collective-permute-start.10 = (bf16[384,768]{1,0:T(8,128)(2,1)S(1)}, bf16[384,768]{1,0:T(8,128)(2,1)S(1)}, u32[]{:S(2)}, u32[]{:S(2)}) collective-permute-start(bf16[384,768]{1,0:T(8,128)(2,1)S(1)} %get-tuple-element.7), channel_id=1, source_target_pairs={{0,64},{8,72},{16,80},{24,88},{32,96},{40,104},{48,112},{56,120},{... | collective-permute-start | bytes 1769480 | tf_op jit(solution)/shard_map/ppermute | solution.py:319
  103.1 5.1 %collective-permute-start.9 = (bf16[384,768]{1,0:T(8,128)(2,1)S(1)}, bf16[384,768]{1,0:T(8,128)(2,1)S(1)}, u32[]{:S(2)}, u32[]{:S(2)}) collective-permute-start(bf16[384,768]{1,0:T(8,128)(2,1)S(1)} %get-tuple-element.7), channel_id=1, source_target_pairs={{0,448},{8,456},{16,464},{24,472},{32,480},{40,488},{48,496},{56,5... | collective-permute-start | bytes 1769480 | tf_op jit(solution)/shard_map/ppermute | solution.py:319
  108.3 5.2 %early.1 = bf16[1024,1152]{1,0:T(8,128)(2,1)} custom-call(bf16[512,1536]{1,0:T(8,128)(2,1)} %collective-permute-done.3.other, bf16[512,1536]{1,0:T(8,128)(2,1)S(1)} %by_place.1.own, bf16[384,768]{1,0:T(8,128)(2,1)S(1)} %bitcast.14, bf16[384,768]{1,0:T(8,128)(2,1)S(1)} %copy-done.1, bf16[384,768]{1,0:T(8,128)(2,1)S(1)} %copy-done.3), custom_call_target="tpu_custom_call" | custom-call | flops 1811939328 | bytes 4915200 | tf_op jit(solution)/shard_map/early/pallas_call | solution.py:214
  113.5 2.7 %late.1 = bf16[1024,768]{1,0:T(8,128)(2,1)S(1)} custom-call(bf16[1024,1152]{1,0:T(8,128)(2,1)} %early.1, bf16[192,768]{1,0:T(8,128)(2,1)} %collective-permute-done.6.u2_top, bf16[192,768]{1,0:T(8,128)(2,1)} %collective-permute-done.7.u2_bottom, f32[1,768]{1,0:T(1,128)S(1)} %copy-done.12), custom_call_target="tpu_custom_call" | custom-call | flops 603979776 | bytes 4521984 | tf_op jit(solution)/shard_map/late/pallas_call | solution.py:266
  117.1 1.9 %collective-permute-start.12 = (bf16[512,768]{1,0:T(8,128)(2,1)S(1)}, bf16[512,768]{1,0:T(8,128)(2,1)S(1)}, u32[]{:S(2)}, u32[]{:S(2)}) collective-permute-start(bf16[512,768]{1,0:T(8,128)(2,1)S(1)} %convolution_convert_fusion), channel_id=1, source_target_pairs={{0,1},{1,0},{2,3},{3,2},{4,5},{5,4},{6,7},{7,6},{8,9},{9,8},{10,11... | collective-permute-start | bytes 2359304 | tf_op jit(solution)/shard_map/ppermute | solution.py:330
  119.0 4.2 %collective-permute-done.10.refs_1_ = bf16[384,768]{1,0:T(8,128)(2,1)S(1)} collective-permute-done((bf16[384,768]{1,0:T(8,128)(2,1)S(1)}, bf16[384,768]{1,0:T(8,128)(2,1)S(1)}, u32[]{:S(2)}, u32[]{:S(2)}) %collective-permute-start.10) | collective-permute-done | bytes 589856 | tf_op jit(solution)/shard_map/ppermute | solution.py:319
  123.4 1.7 %convolution_convert_fusion.1 = bf16[512,768]{1,0:T(8,128)(2,1)} fusion(bf16[768,768]{1,0:T(8,128)(2,1)S(1)} %stacked.1, bf16[1024,768]{1,0:T(8,128)(2,1)S(1)} %late.1), kind=kOutput, calls=%fused_computation.3 | convolution fusion | flops 604372992 | bytes 2752512 | tf_op jit(solution)/shard_map/dot_general | solution.py:327
  125.1 1.9 %collective-permute-start.11 = (bf16[512,768]{1,0:T(8,128)(2,1)}, bf16[512,768]{1,0:T(8,128)(2,1)}, u32[]{:S(2)}, u32[]{:S(2)}) collective-permute-start(bf16[512,768]{1,0:T(8,128)(2,1)} %convolution_convert_fusion.1), channel_id=1, source_target_pairs={{0,1},{1,0},{2,3},{3,2},{4,5},{5,4},{6,7},{7,6},{8,9},{9,8},{10,11... | collective-permute-start | bytes 2359304 | tf_op jit(solution)/shard_map/ppermute | solution.py:330
  127.9 1.1 add_convert_fusion
  128.9 3.5 %all-to-all-start.3 = ((bf16[4,128,768]{2,1,0:T(8,128)(2,1)}), bf16[4,128,768]{2,1,0:T(8,128)(2,1)S(1)}, u32[]{:S(2)}, u32[]{:S(2)}) async-start(bf16[4,128,768]{2,1,0:T(8,128)(2,1)} %bitcast.15), calls=%async_computation.3 | async-start | bytes 1572864 | tf_op jit(solution)/shard_map/all_to_all | solution.py:36
  133.3 2.2 %add_convert_fusion.1 = bf16[512,768]{1,0:T(8,128)(2,1)} fusion(f32[512,768]{1,0:T(8,128)S(1)} %fusion.7, bf16[512,768]{1,0:T(8,128)(2,1)} %collective-permute-done.11), kind=kLoop, calls=%fused_computation.1 | loop fusion | flops 1179648 | bytes 3145728 | tf_op jit(solution)/shard_map/convert_element_type | solution.py:332
  135.5 10.1 %all-to-all-done.3 = bf16[4,128,768]{2,1,0:T(8,128)(2,1)S(1)} async-done(((bf16[4,128,768]{2,1,0:T(8,128)(2,1)}), bf16[4,128,768]{2,1,0:T(8,128)(2,1)S(1)}, u32[]{:S(2)}, u32[]{:S(2)}) %all-to-all-start.3) | async-done | bytes 786464 | tf_op jit(solution)/shard_map/all_to_all | solution.py:36
  145.6 3.5 %all-to-all-start.2 = ((bf16[4,128,768]{2,1,0:T(8,128)(2,1)}), bf16[4,128,768]{2,1,0:T(8,128)(2,1)S(1)}, u32[]{:S(2)}, u32[]{:S(2)}) async-start(bf16[4,128,768]{2,1,0:T(8,128)(2,1)} %bitcast.5), calls=%async_computation.2 | async-start | bytes 1572864 | tf_op jit(solution)/shard_map/all_to_all | solution.py:36
  149.3 12.2 %all-to-all-done.2 = bf16[4,128,768]{2,1,0:T(8,128)(2,1)S(1)} async-done(((bf16[4,128,768]{2,1,0:T(8,128)(2,1)}), bf16[4,128,768]{2,1,0:T(8,128)(2,1)S(1)}, u32[]{:S(2)}, u32[]{:S(2)}) %all-to-all-start.2) | async-done | bytes 786464 | tf_op jit(solution)/shard_map/all_to_all | solution.py:36
  (68 shorter events, 17.2 us)
Async XLA Ops:
  0.0 0.9 copy-start.13
  0.9 10.1 %copy-start.16 = (f32[768,48]{0,1:T(8,128)S(1)}, f32[768,48]{0,1:T(8,128)}, u32[]{:S(2)}) copy-start(f32[768,48]{0,1:T(8,128)} %param.10) | copy-start | bytes 442372
  0.9 10.1 %copy-start.18 = (f32[1,48]{1,0:T(1,128)S(1)}, f32[1,48]{1,0:T(1,128)}, u32[]{:S(2)}) copy-start(f32[1,48]{1,0:T(1,128)} %param.11) | copy-start | bytes 580
  0.9 14.6 %copy-start.14 = (bf16[128,1536]{1,0:T(8,128)(2,1)S(1)}, bf16[128,1536]{1,0:T(8,128)(2,1)}, u32[]{:S(2)}) copy-start(bf16[128,1536]{1,0:T(8,128)(2,1)} %param.6) | copy-start | bytes 1179652
  0.9 14.8 %copy-start.17 = (f32[1536]{0:T(1024)S(1)}, f32[1536]{0:T(1024)}, u32[]{:S(2)}) copy-start(f32[1536]{0:T(1024)} %param.7) | copy-start | bytes 18436
  1.8 25.0 %all-to-all-start = ((bf16[8,48,768]{2,1,0:T(8,128)(2,1)}), bf16[8,48,768]{2,1,0:T(8,128)(2,1)S(1)}, u32[]{:S(2)}, u32[]{:S(2)}) async-start(bf16[8,48,768]{2,1,0:T(8,128)(2,1)} %bitcast.1), calls=%async_computation | async-start | bytes 1179648 | tf_op jit(solution)/shard_map/all_to_all | solution.py:36
  11.1 11.6 %collective-permute-start.8 = (bf16[48,768]{1,0:T(8,128)(2,1)S(1)}, bf16[48,768]{1,0:T(8,128)(2,1)S(1)}, u32[]{:S(2)}, u32[]{:S(2)}) collective-permute-start(bf16[48,768]{1,0:T(8,128)(2,1)S(1)} %fusion.9.refs_0_), channel_id=1, source_target_pairs={{0,128},{8,136},{16,144},{24,152},{32,160},{40,168},{48,176},{56,1... | collective-permute-start | bytes 221192 | tf_op jit(solution)/shard_map/ppermute | solution.py:293
  17.3 14.4 %copy-start.15 = (bf16[128,384]{1,0:T(8,128)(2,1)S(1)}, bf16[128,384]{1,0:T(8,128)(2,1)}, u32[]{:S(2)}) copy-start(bf16[128,384]{1,0:T(8,128)(2,1)} %get-tuple-element.11) | copy-start | bytes 294916
  26.8 74.1 %all-to-all-start.1 = ((bf16[8,2,48,768]{3,2,1,0:T(8,128)(2,1)}), bf16[8,2,48,768]{3,2,1,0:T(8,128)(2,1)S(1)}, u32[]{:S(2)}, u32[]{:S(2)}) async-start(bf16[8,2,48,768]{3,2,1,0:T(8,128)(2,1)} %copies.3), calls=%async_computation.1 | async-start | bytes 2359296 | tf_op jit(solution)/shard_map/all_to_all | solution.py:36
  33.0 21.4 %collective-permute-start = (bf16[128,1536]{1,0:T(8,128)(2,1)S(1)}, bf16[128,1536]{1,0:T(8,128)(2,1)S(1)}, u32[]{:S(2)}, u32[]{:S(2)}) collective-permute-start(bf16[128,1536]{1,0:T(8,128)(2,1)S(1)} %maximum_select_fusion.refs_0_), channel_id=1, source_target_pairs={{0,6},{1,7},{2,0},{3,1},{4,2},{5,3},{6,4},{7,5},{8,14},{9,15},{10,... | collective-permute-start | bytes 1179656 | tf_op jit(solution)/shard_map/ppermute | solution.py:302
  37.7 17.4 %collective-permute-start.1 = (bf16[128,1536]{1,0:T(8,128)(2,1)S(1)}, bf16[128,1536]{1,0:T(8,128)(2,1)S(1)}, u32[]{:S(2)}, u32[]{:S(2)}) collective-permute-start(bf16[128,1536]{1,0:T(8,128)(2,1)S(1)} %maximum_select_fusion.refs_0_), channel_id=1, source_target_pairs={{0,4},{1,5},{2,6},{3,7},{4,0},{5,1},{6,2},{7,3},{8,12},{9,13},{10,... | collective-permute-start | bytes 1179656 | tf_op jit(solution)/shard_map/ppermute | solution.py:303
  40.4 19.6 %collective-permute-start.2 = (bf16[128,1536]{1,0:T(8,128)(2,1)S(1)}, bf16[128,1536]{1,0:T(8,128)(2,1)S(1)}, u32[]{:S(2)}, u32[]{:S(2)}) collective-permute-start(bf16[128,1536]{1,0:T(8,128)(2,1)S(1)} %maximum_select_fusion.refs_0_), channel_id=1, source_target_pairs={{0,2},{1,3},{2,4},{3,5},{4,6},{5,7},{6,0},{7,1},{8,10},{9,11},{10,... | collective-permute-start | bytes 1179656 | tf_op jit(solution)/shard_map/ppermute | solution.py:304
  60.8 1.0 copy-start.5
  61.8 1.0 copy-start.7
  62.8 1.0 copy-start.9
  63.8 1.0 copy-start.11
  65.5 42.7 %collective-permute-start.3 = (bf16[512,1536]{1,0:T(8,128)(2,1)S(1)}, bf16[512,1536]{1,0:T(8,128)(2,1)}, u32[]{:S(2)}, u32[]{:S(2)}) collective-permute-start(bf16[512,1536]{1,0:T(8,128)(2,1)S(1)} %by_place.1.own), channel_id=1, source_target_pairs={{0,1},{1,0},{2,3},{3,2},{4,5},{5,4},{6,7},{7,6},{8,9},{9,8},{10,11... | collective-permute-start | bytes 4718600 | tf_op jit(solution)/shard_map/ppermute | solution.py:307
  67.5 24.2 %collective-permute-start.4 = (bf16[384,768]{1,0:T(8,128)(2,1)S(1)}, bf16[384,768]{1,0:T(8,128)(2,1)S(1)}, u32[]{:S(2)}, u32[]{:S(2)}) collective-permute-start(bf16[384,768]{1,0:T(8,128)(2,1)S(1)} %bitcast.12), channel_id=1, source_target_pairs={{0,448},{8,456},{16,464},{24,472},{32,480},{40,488},{48,496},{56,5... | collective-permute-start | bytes 1769480 | tf_op jit(solution)/shard_map/ppermute | solution.py:309
  78.4 19.6 %collective-permute-start.5 = (bf16[384,768]{1,0:T(8,128)(2,1)S(1)}, bf16[384,768]{1,0:T(8,128)(2,1)S(1)}, u32[]{:S(2)}, u32[]{:S(2)}) collective-permute-start(bf16[384,768]{1,0:T(8,128)(2,1)S(1)} %bitcast.13), channel_id=1, source_target_pairs={{0,64},{8,72},{16,80},{24,88},{32,96},{40,104},{48,112},{56,120},{... | collective-permute-start | bytes 1769480 | tf_op jit(solution)/shard_map/ppermute | solution.py:310
  91.7 7.2 %copy-start = (bf16[384,768]{1,0:T(8,128)(2,1)}, bf16[384,768]{1,0:T(8,128)(2,1)S(1)}, u32[]{:S(2)}) copy-start(bf16[384,768]{1,0:T(8,128)(2,1)S(1)} %collective-permute-done.4.u1.a) | copy-start | bytes 1769476
  92.4 21.1 %collective-permute-start.6 = (bf16[192,768]{1,0:T(8,128)(2,1)}, bf16[192,768]{1,0:T(8,128)(2,1)}, u32[]{:S(2)}, u32[]{:S(2)}) collective-permute-start(bf16[192,768]{1,0:T(8,128)(2,1)} %half.2), channel_id=1, source_target_pairs={{0,448},{8,456},{16,464},{24,472},{32,480},{40,488},{48,496},{56,5... | collective-permute-start | bytes 884744 | tf_op jit(solution)/shard_map/ppermute | solution.py:312
  98.0 0.9 copy-start.2
  99.0 14.5 %collective-permute-start.7 = (bf16[192,768]{1,0:T(8,128)(2,1)}, bf16[192,768]{1,0:T(8,128)(2,1)}, u32[]{:S(2)}, u32[]{:S(2)}) collective-permute-start(bf16[192,768]{1,0:T(8,128)(2,1)} %half.3), channel_id=1, source_target_pairs={{0,64},{8,72},{16,80},{24,88},{32,96},{40,104},{48,112},{56,120},{... | collective-permute-start | bytes 884744 | tf_op jit(solution)/shard_map/ppermute | solution.py:313
  100.9 7.4 %copy-start.1 = (bf16[384,768]{1,0:T(8,128)(2,1)S(1)}, bf16[384,768]{1,0:T(8,128)(2,1)}, u32[]{:S(2)}) copy-start(bf16[384,768]{1,0:T(8,128)(2,1)} %copy-done) | copy-start | bytes 1769476
  100.9 7.4 %copy-start.3 = (bf16[384,768]{1,0:T(8,128)(2,1)S(1)}, bf16[384,768]{1,0:T(8,128)(2,1)}, u32[]{:S(2)}) copy-start(bf16[384,768]{1,0:T(8,128)(2,1)} %copy-done.2) | copy-start | bytes 1769476
  101.0 12.5 %copy-start.12 = (f32[1,768]{1,0:T(1,128)S(1)}, f32[1,768]{1,0:T(1,128)}, u32[]{:S(2)}) copy-start(f32[1,768]{1,0:T(1,128)} %scale.1) | copy-start | bytes 9220
  101.0 22.1 %collective-permute-start.10 = (bf16[384,768]{1,0:T(8,128)(2,1)S(1)}, bf16[384,768]{1,0:T(8,128)(2,1)S(1)}, u32[]{:S(2)}, u32[]{:S(2)}) collective-permute-start(bf16[384,768]{1,0:T(8,128)(2,1)S(1)} %get-tuple-element.7), channel_id=1, source_target_pairs={{0,64},{8,72},{16,80},{24,88},{32,96},{40,104},{48,112},{56,120},{... | collective-permute-start | bytes 1769480 | tf_op jit(solution)/shard_map/ppermute | solution.py:319
  103.1 20.1 %collective-permute-start.9 = (bf16[384,768]{1,0:T(8,128)(2,1)S(1)}, bf16[384,768]{1,0:T(8,128)(2,1)S(1)}, u32[]{:S(2)}, u32[]{:S(2)}) collective-permute-start(bf16[384,768]{1,0:T(8,128)(2,1)S(1)} %get-tuple-element.7), channel_id=1, source_target_pairs={{0,448},{8,456},{16,464},{24,472},{32,480},{40,488},{48,496},{56,5... | collective-permute-start | bytes 1769480 | tf_op jit(solution)/shard_map/ppermute | solution.py:319
  117.1 10.8 %collective-permute-start.12 = (bf16[512,768]{1,0:T(8,128)(2,1)S(1)}, bf16[512,768]{1,0:T(8,128)(2,1)S(1)}, u32[]{:S(2)}, u32[]{:S(2)}) collective-permute-start(bf16[512,768]{1,0:T(8,128)(2,1)S(1)} %convolution_convert_fusion), channel_id=1, source_target_pairs={{0,1},{1,0},{2,3},{3,2},{4,5},{5,4},{6,7},{7,6},{8,9},{9,8},{10,11... | collective-permute-start | bytes 2359304 | tf_op jit(solution)/shard_map/ppermute | solution.py:330
  125.1 8.1 %collective-permute-start.11 = (bf16[512,768]{1,0:T(8,128)(2,1)}, bf16[512,768]{1,0:T(8,128)(2,1)}, u32[]{:S(2)}, u32[]{:S(2)}) collective-permute-start(bf16[512,768]{1,0:T(8,128)(2,1)} %convolution_convert_fusion.1), channel_id=1, source_target_pairs={{0,1},{1,0},{2,3},{3,2},{4,5},{5,4},{6,7},{7,6},{8,9},{9,8},{10,11... | collective-permute-start | bytes 2359304 | tf_op jit(solution)/shard_map/ppermute | solution.py:330
  128.9 16.7 %all-to-all-start.3 = ((bf16[4,128,768]{2,1,0:T(8,128)(2,1)}), bf16[4,128,768]{2,1,0:T(8,128)(2,1)S(1)}, u32[]{:S(2)}, u32[]{:S(2)}) async-start(bf16[4,128,768]{2,1,0:T(8,128)(2,1)} %bitcast.15), calls=%async_computation.3 | async-start | bytes 1572864 | tf_op jit(solution)/shard_map/all_to_all | solution.py:36
  145.6 15.8 %all-to-all-start.2 = ((bf16[4,128,768]{2,1,0:T(8,128)(2,1)}), bf16[4,128,768]{2,1,0:T(8,128)(2,1)S(1)}, u32[]{:S(2)}, u32[]{:S(2)}) async-start(bf16[4,128,768]{2,1,0:T(8,128)(2,1)} %bitcast.5), calls=%async_computation.2 | async-start | bytes 1572864 | tf_op jit(solution)/shard_map/all_to_all | solution.py:36
  (4 other events, 3.0 us)
